TPU v7x, 32 devices: a whole 2x2x4 slice. The times are simulated.
32 devices in a mesh: rep: 4 (over z), fs: 2 (over y), tp: 4 (over x, core).
Axes of the slice: x: 2, y: 2, z: 4, core: 2. Of those that a mesh axis runs over, the one named last changes fastest.
Arguments:
- tokens: bfloat16 [3072, 2048], P('rep', 'fs'), may hold values from -6 to 6
- gate_pre: bfloat16 [3072, 6144], P('rep', 'tp'), may hold values from -6 to 6
- up_pre: bfloat16 [3072, 6144], P('rep', 'tp'), may hold values from -6 to 6
- hidden_grad: bfloat16 [3072, 6144], P('rep', 'tp'), may hold values from -0.75 to 0.75
- gate_weight: bfloat16 [2048, 6144], P('fs', 'tp'), may hold values from -0.125 to 0.125
- up_weight: bfloat16 [2048, 6144], P('fs', 'tp'), may hold values from -0.125 to 0.125
- gate_taps: float32 [3, 6144], P(None, 'tp'), may hold values from -3.5 to 3.5
- up_taps: float32 [3, 6144], P(None, 'tp'), may hold values from -3.5 to 3.5
- gate_bias: float32 [6144], P('tp'), may hold values from -4 to 4
- up_bias: float32 [6144], P('tp'), may hold values from -4 to 4
Outputs:
- input_grad: bfloat16 [3072, 2048], P('rep', 'fs')
- gate_weight_grad: float32 [2048, 6144], P('fs', 'tp')
- up_weight_grad: float32 [2048, 6144], P('fs', 'tp')
- gate_taps_grad: float32 [3, 6144], P(None, 'tp')
- up_taps_grad: float32 [3, 6144], P(None, 'tp')
- gate_bias_grad: float32 [6144], P('tp')
- up_bias_grad: float32 [6144], P('tp')
All inputs are finite; a program needn't handle non-finite values.
Results may differ from a plain program's by a relative error of at most 0.017.
Values may be sent and summed in bfloat16 or wider, within the bound.
No kernel may reach another device: no remote copies, remote signals or barrier semaphores. Data moves between devices by JAX's collectives and lax.ppermute only.
A program may use at most 64 MiB of HBM per device.

v0:
```python
import jax
import jax.numpy as jnp
from jax import lax
from jax.sharding import PartitionSpec as P


def causal_mix(signal, tap_weights):
    tap_count = tap_weights.shape[0]
    length = signal.shape[0]
    padded = jnp.pad(signal, ((tap_count - 1, 0), (0, 0)))
    mixed = padded[0:length] * tap_weights[0]
    for offset in range(1, tap_count):
        mixed = mixed + padded[offset : offset + length] * tap_weights[offset]
    return mixed


def mix_back(signal, tap_weights):
    tap_count = tap_weights.shape[0]
    length = signal.shape[0]
    padded = jnp.pad(signal, ((0, tap_count - 1), (0, 0)))
    begin = tap_count - 1
    mixed = padded[begin : begin + length] * tap_weights[0]
    for offset in range(1, tap_count):
        begin = tap_count - 1 - offset
        mixed = mixed + padded[begin : begin + length] * tap_weights[offset]
    return mixed


def tap_terms(grad_signal, signal, tap_count):
    length = signal.shape[0]
    padded = jnp.pad(signal, ((tap_count - 1, 0), (0, 0)))
    return jnp.stack(
        [
            jnp.sum(grad_signal * padded[offset : offset + length], axis=0)
            for offset in range(tap_count)
        ]
    )


def backward_terms(gate_pre, up_pre, hidden_grad, gate_taps, up_taps, gate_bias, up_bias):
    gate_float = gate_pre.astype(jnp.float32)
    up_float = up_pre.astype(jnp.float32)
    gate_mixed = causal_mix(gate_float, gate_taps) + gate_bias
    up_mixed = causal_mix(up_float, up_taps) + up_bias
    logistic = jax.nn.sigmoid(gate_mixed)
    cotangent = hidden_grad.astype(jnp.float32)
    gate_delta = cotangent * up_mixed * logistic * (1.0 + gate_mixed * (1.0 - logistic))
    up_delta = cotangent * gate_mixed * logistic
    gate_back = mix_back(gate_delta, gate_taps).astype(jnp.bfloat16)
    up_back = mix_back(up_delta, up_taps).astype(jnp.bfloat16)
    tap_count = gate_taps.shape[0]
    return (
        gate_back,
        up_back,
        tap_terms(gate_delta, gate_float, tap_count),
        tap_terms(up_delta, up_float, tap_count),
        jnp.sum(gate_delta, axis=0),
        jnp.sum(up_delta, axis=0),
    )


def per_device(
    tokens,
    gate_pre,
    up_pre,
    hidden_grad,
    gate_weight,
    up_weight,
    gate_taps,
    up_taps,
    gate_bias,
    up_bias,
):
    gate_back, up_back, gate_tap_part, up_tap_part, gate_bias_part, up_bias_part = backward_terms(
        gate_pre, up_pre, hidden_grad, gate_taps, up_taps, gate_bias, up_bias
    )
    feature_dims = (((1,), (1,)), ((), ()))
    token_dims = (((0,), (0,)), ((), ()))
    full_partial = lax.dot_general(
        gate_back, gate_weight, feature_dims, preferred_element_type=jnp.float32
    ) + lax.dot_general(up_back, up_weight, feature_dims, preferred_element_type=jnp.float32)
    own_columns = lax.psum_scatter(
        full_partial.astype(jnp.bfloat16), "tp", scatter_dimension=1, tiled=True
    )
    result = lax.all_gather(own_columns, "tp", axis=1, tiled=True)
    gate_local = lax.dot_general(tokens, gate_back, token_dims, preferred_element_type=jnp.float32)
    up_local = lax.dot_general(tokens, up_back, token_dims, preferred_element_type=jnp.float32)
    summed_grads = (
        lax.psum(gate_local.astype(jnp.bfloat16), "rep").astype(jnp.float32),
        lax.psum(up_local.astype(jnp.bfloat16), "rep").astype(jnp.float32),
        lax.psum(gate_tap_part.astype(jnp.bfloat16), "rep").astype(jnp.float32),
        lax.psum(up_tap_part.astype(jnp.bfloat16), "rep").astype(jnp.float32),
        lax.psum(gate_bias_part.astype(jnp.bfloat16), "rep").astype(jnp.float32),
        lax.psum(up_bias_part.astype(jnp.bfloat16), "rep").astype(jnp.float32),
    )
    gate_weight_grad, up_weight_grad, gate_taps_grad, up_taps_grad, gate_bias_grad, up_bias_grad = (
        summed_grads
    )
    return (
        result,
        gate_weight_grad,
        up_weight_grad,
        gate_taps_grad,
        up_taps_grad,
        gate_bias_grad,
        up_bias_grad,
    )


def solution(mesh):
    return jax.shard_map(
        per_device,
        mesh=mesh,
        in_specs=(
            P("rep", "fs"),
            P("rep", "tp"),
            P("rep", "tp"),
            P("rep", "tp"),
            P("fs", "tp"),
            P("fs", "tp"),
            P(None, "tp"),
            P(None, "tp"),
            P("tp"),
            P("tp"),
        ),
        out_specs=(
            P("rep", "fs"),
            P("fs", "tp"),
            P("fs", "tp"),
            P(None, "tp"),
            P(None, "tp"),
            P("tp"),
            P("tp"),
        ),
        check_vma=False,
    )
```

profile of v0, /device:TPU:0, one launch (start us, length us, event | category | flops | bytes accessed | tf_op | source)
XLA Modules:
  0.0 329.4 jit_solution(4718363927047613101)
XLA Ops:
  8.0 0.0 copy-start
  8.0 0.0 reduce-scatter.2.cloned.1.call-start
  8.1 0.0 copy-start.3
  8.1 1.0 slice_reduce_fusion.2
  9.1 1.0 slice_reduce_fusion.5
  10.0 2.3 convert_element_type.66
  12.3 0.0 copy-done.3
  12.4 0.0 copy-start.2
  12.4 0.0 copy-start.7
  12.4 0.6 convert_element_type.65
  13.0 1.0 copy-done.2
  14.0 0.0 copy-done.7
  14.0 0.0 copy-start.8
  14.0 5.8 %fusion.5 = (bf16[1536]{0:T(1024)(128)(2,1)S(1)}, bf16[1536]{0:T(1024)(128)(2,1)S(1)}, bf16[1536]{0:T(1024)(128)(2,1)S(1)}, bf16[1536]{0:T(1024)(128)(2,1)S(1)},...) fusion(bf16[768,1536]{1,0:T(8,128)(2,1)S(1)} %copy-done.3, f32[768,1536]{1,0:T(8,128)S(1)} %convert_element_type.65, ...), kind=kLoop, calls=%fused_computation.32 | loop fusion | flops 23586816 | bytes 23629824 | tf_op jit(solution)/shard_map/reduce_sum | solution.py:58
  19.8 0.0 copy-done.8
  19.8 10.3 %fusion.6 = (bf16[1536]{0:T(1024)(128)(2,1)S(1)}, bf16[1536]{0:T(1024)(128)(2,1)S(1)}, bf16[1536]{0:T(1024)(128)(2,1)S(1)}, bf16[1536]{0:T(1024)(128)(2,1)S(1)},...) fusion(bf16[768,1536]{1,0:T(8,128)(2,1)} %param.11, f32[768,1536]{1,0:T(8,128)S(1)} %convert_element_type.66, ...), kind=kLoop, calls=%fused_computation.33 | loop fusion | flops 35383296 | bytes 30707712 | tf_op jit(solution)/shard_map/reduce_sum | solution.py:57
  30.1 5.9 %add_convert_fusion.1 = bf16[768,1536]{1,0:T(8,128)(2,1)S(1)} fusion(f32[768,1536]{1,0:T(8,128)} %get-tuple-element.40, f32[1536]{0:T(1024)S(1)} %get-tuple-element.30, f32[1536]{0:T(1024)S(1)} %get-tuple-element.31, f32[1536]{0:T(1024)S(1)} %get-tuple-element.29), kind=kLoop, calls=%fused_computation.12 | loop fusion | flops 7077888 | bytes 7096320 | tf_op jit(solution)/shard_map/convert_element_type | solution.py:49
  36.1 0.0 copy-done
  36.1 0.0 copy-start.6
  36.1 0.0 copy-start.4
  36.1 0.0 copy-start.9
  36.1 2.6 fusion.9
  38.7 0.0 copy-done.6
  38.7 0.0 copy-done.4
  38.8 0.8 copy-done.9
  39.5 3.7 %add_convert_fusion.2 = bf16[768,1024]{1,0:T(8,128)(2,1)} fusion(f32[768,1024]{1,0:T(8,128)S(1)} %fusion.9, bf16[768,1536]{1,0:T(8,128)(2,1)S(1)} %copy-done.4, bf16[1024,1536]{1,0:T(8,128)(2,1)S(1)} %copy-done.9), kind=kOutput, calls=%fused_computation.23 | convolution fusion | flops 2417491968 | bytes 10223616 | tf_op jit(solution)/shard_map/dot_general | solution.py:81
  43.2 0.0 reduce-scatter.2.cloned.1.call-update
  43.3 0.0 all-gather.2.cloned.1.call-start
  43.3 30.9 %reduce-scatter.2.cloned.1.call-done = bf16[768,256]{1,0:T(8,128)(2,1)} async-done(((bf16[768,1024]{1,0:T(8,128)(2,1)}), bf16[768,256]{1,0:T(8,128)(2,1)}) %reduce-scatter.2.cloned.1.call-update) | async-done | bytes 393232 | tf_op jit(solution)/shard_map/reduce_scatter | solution.py:82
  74.2 0.0 all-gather.2.cloned.1.call-update
  74.2 0.0 copy-start.5
  74.2 0.0 all-reduce.8.cloned.1.call-start
  74.3 0.0 copy-start.10
  74.3 6.6 %fusion.3 = bf16[1024,1536]{0,1:T(8,128)(2,1)} fusion(bf16[768,1536]{1,0:T(8,128)(2,1)} %copy-done.6, bf16[768,1024]{1,0:T(8,128)(2,1)} %param.10), kind=kOutput, calls=%fused_computation.21 | convolution fusion | flops 2417491968 | bytes 7077888 | tf_op jit(solution)/shard_map/dot_general | solution.py:86
  80.9 0.0 copy-done.5
  80.9 0.0 copy-done.10
  80.9 4.0 %fusion.4 = bf16[1024,1536]{0,1:T(8,128)(2,1)} fusion(bf16[768,1536]{1,0:T(8,128)(2,1)S(1)} %copy-done.5, bf16[768,1024]{1,0:T(8,128)(2,1)S(1)} %copy-done.10), kind=kOutput, calls=%fused_computation.22 | convolution fusion | flops 2417491968 | bytes 7077888 | tf_op jit(solution)/shard_map/dot_general | solution.py:87
  84.9 0.0 all-reduce.8.cloned.1.call-update
  85.0 0.1 pad_maximum_fusion
  85.1 21.1 %all-reduce.4 = (bf16[3,1536]{1,0:T(4,128)(2,1)S(1)}, bf16[3,1536]{1,0:T(4,128)(2,1)S(1)}, bf16[1536]{0:T(1024)(128)(2,1)S(1)}, bf16[1536]{0:T(1024)(128)(2,1)S(1)}) all-reduce(bf16[3,1536]{1,0:T(4,128)(2,1)S(1)} %get-tuple-element.42, bf16[3,1536]{1,0:T(4,128)(2,1)S(1)} %get-tuple-element.43, ...), channel_id=1, replica_groups=mesh['rep'=4,'fs'=2,'tp'=4] {'rep'}, use_global_device_ids=true, to_apply=%region_6.7 | all-reduce | flops 12288 | bytes 49152 | tf_op jit(solution)/shard_map/psum | solution.py:91
  106.2 0.6 convert_element_type.79
  106.8 0.6 convert_element_type.81
  107.4 0.6 convert_element_type.76
  108.0 0.6 convert_element_type.77
  108.6 0.0 all-gather.2.cloned.1.call-done
  108.6 199.7 %all-reduce.8.cloned.1.call-done = (bf16[1024,1536]{0,1:T(8,128)(2,1)}, bf16[1024,1536]{0,1:T(8,128)(2,1)}) async-done(((bf16[1024,1536]{0,1:T(8,128)(2,1)}, bf16[1024,1536]{0,1:T(8,128)(2,1)}), (bf16[1024,1536]{0,1:T(8,128)(2,1)}, bf16[1024,1536]{0,1:T(8,128)(2,1)})) %all-reduce.8.cloned.1.call-update) | async-done | bytes 6291472 | tf_op jit(solution)/shard_map/psum | solution.py:89
  308.3 5.4 %copy.17 = f32[1024,1536]{1,0:T(8,128)} copy(bf16[1024,1536]{0,1:T(8,128)(2,1)} %get-tuple-element.36) | data formatting | bytes 9437184
  313.7 0.0 copy-start.1
  313.7 5.5 %copy.18 = f32[1024,1536]{1,0:T(8,128)} copy(bf16[1024,1536]{0,1:T(8,128)(2,1)} %get-tuple-element.37) | data formatting | bytes 9437184
  319.2 2.7 copy.22
  321.9 0.0 copy-done.1
  (6 shorter events, 0.0 us)
Async XLA Ops:
  8.0 28.1 %copy-start = (bf16[1024,1536]{1,0:T(8,128)(2,1)S(1)}, bf16[1024,1536]{1,0:T(8,128)(2,1)}, u32[]{:S(2)}) copy-start(bf16[1024,1536]{1,0:T(8,128)(2,1)} %param.14) | copy-start | bytes 9437188
  8.0 66.2 %reduce-scatter.2.cloned.1.call-start = ((), (), s32[]{:S(2)}) async-start(), calls=%async_computation.1 | async-start | bytes 1966080 | tf_op jit(solution)/shard_map/reduce_scatter | solution.py:82
  8.1 4.3 %copy-start.3 = (bf16[768,1536]{1,0:T(8,128)(2,1)S(1)}, bf16[768,1536]{1,0:T(8,128)(2,1)}, u32[]{:S(2)}) copy-start(bf16[768,1536]{1,0:T(8,128)(2,1)} %param.12) | copy-start | bytes 7077892
  12.4 1.7 copy-start.2
  12.4 1.7 copy-start.7
  14.0 5.8 %copy-start.8 = (f32[1536]{0:T(1024)S(1)}, f32[1536]{0:T(1024)}, u32[]{:S(2)}) copy-start(f32[1536]{0:T(1024)} %param.19) | copy-start | bytes 18436
  36.1 2.7 copy-start.6
  36.1 2.7 copy-start.4
  36.1 3.4 %copy-start.9 = (bf16[1024,1536]{1,0:T(8,128)(2,1)S(1)}, bf16[1024,1536]{1,0:T(8,128)(2,1)}, u32[]{:S(2)}) copy-start(bf16[1024,1536]{1,0:T(8,128)(2,1)} %param.15) | copy-start | bytes 9437188
  43.3 65.4 %all-gather.2.cloned.1.call-start = ((), (), s32[]{:S(2)}) async-start(), calls=%async_computation.2 | async-start | bytes 1966080 | tf_op jit(solution)/shard_map/all_gather | solution.py:85
  74.2 6.7 %copy-start.5 = (bf16[768,1536]{1,0:T(8,128)(2,1)S(1)}, bf16[768,1536]{1,0:T(8,128)(2,1)}, u32[]{:S(2)}) copy-start(bf16[768,1536]{1,0:T(8,128)(2,1)} %get-tuple-element.41) | copy-start | bytes 7077892
  74.2 234.1 %all-reduce.8.cloned.1.call-start = ((), (), s32[]{:S(2)}) async-start(), calls=%async_computation.3 | async-start | bytes 12582912 | tf_op jit(solution)/shard_map/psum | solution.py:89
  74.3 6.6 %copy-start.10 = (bf16[768,1024]{1,0:T(8,128)(2,1)S(1)}, bf16[768,1024]{1,0:T(8,128)(2,1)}, u32[]{:S(2)}) copy-start(bf16[768,1024]{1,0:T(8,128)(2,1)} %param.10) | copy-start | bytes 4718596
  313.7 8.2 %copy-start.1 = (bf16[1024,1536]{1,0:T(8,128)(2,1)S(1)}, bf16[1024,1536]{1,0:T(8,128)(2,1)}, u32[]{:S(2)}) copy-start(bf16[1024,1536]{1,0:T(8,128)(2,1)} %param.14) | copy-start | bytes 9437188
Sparse Core Ops, SparseCore 0:
  43.4 30.7 reduce-scatter.1
  75.7 19.8 all-gather.1
Sparse Core Ops, SparseCore 1:
  85.0 223.3 all-reduce.7
where the time goes:
time: 330 us; the launch traced here: 329 us
  waiting for transfers between devices  231 us (70%)
  other arithmetic  27.4 us (8%)
  blocking collectives  21.1 us (6%)
  local copies, waits for them, and re-layouts  17.4 us (5%)
  matrix products  17 us (5%)
  between operations  15.7 us (5%)
    psum x1, waiting for transfers between devices, per_device(): lax.psum(gate_local.astype(jnp.bfloat16), 'rep').astype(jnp.float32)  200 us
    reduce_scatter x1, waiting for transfers between devices, per_device(): lax.psum_scatter(full_partial.astype(jnp.bfloat16), 'tp', scatter_dimensi...  30.9 us
    psum x1, blocking collectives, per_device(): lax.psum(gate_tap_part.astype(jnp.bfloat16), 'rep').astype(jnp.float32)  21.1 us
    unnamed x25, local copies, waits for them, and re-layouts  15.4 us
    reduce_sum x1, other arithmetic, backward_terms(): jnp.sum(gate_delta, axis=0)  10.3 us
  transfers between devices with their start and end apart: 3, of which 2 were waited for; matrix products, arithmetic and copies ran while one was open for 4% of the time, Pallas kernels for 0%

commit v1 on v0

v1 whole, which is shorter than its diff:
```python
import functools

import jax
import jax.numpy as jnp
from jax import lax
from jax.experimental import pallas as pl
from jax.experimental.pallas import tpu as pltpu
from jax.sharding import PartitionSpec as P


BLOCK = 128
STRIP = 64
ROWS = 8
MIB = 1 << 20


def params(mib):
    return pltpu.CompilerParams(vmem_limit_bytes=mib * MIB)


def on_chip(x):
    return pltpu.with_memory_space_constraint(x, pltpu.VMEM)


def off_chip(x):
    return pltpu.with_memory_space_constraint(x, pltpu.HBM)


VMEM = pl.BlockSpec(memory_space=pltpu.VMEM)
HBM = pl.BlockSpec(memory_space=pltpu.HBM)
SMEM = pl.BlockSpec(memory_space=pltpu.SMEM)


def start_loads(index, sources, targets, sems):
    copies = []
    for k, (source, target) in enumerate(zip(sources, targets)):
        columns = slice(index * BLOCK, (index + 1) * BLOCK)
        copies.append(pltpu.make_async_copy(source.at[:, columns], target, sems.at[k]))
        copies[k].start()
    return copies


def turn_kernel(flags_ref, in_ref, gate_ref, up_ref, grad_ref, out_ref, gate_in, up_in, grad_in, sems):
    del flags_ref
    copies = start_loads(0, (gate_ref, up_ref, grad_ref), (gate_in, up_in, grad_in), sems)
    out_ref[...] = in_ref[...].T
    for copy in copies:
        copy.wait()


def turn(flags, tokens, signals):
    length, features = tokens.shape
    return pl.pallas_call(
        turn_kernel,
        in_specs=[SMEM, VMEM, HBM, HBM, HBM],
        out_specs=[VMEM] * 4,
        out_shape=[pltpu.VMEM((features, length), tokens.dtype)]
        + [pltpu.VMEM((length, BLOCK), tokens.dtype)] * 3,
        scratch_shapes=[pltpu.SemaphoreType.DMA((3,))],
        compiler_params=params(6),
        name="turn",
    )(flags, off_chip(tokens), *(off_chip(x) for x in signals))


def block_kernel(
    index,
    last,
    tokens_ref,
    gate_pre_ref,
    up_pre_ref,
    grad_ref,
    gate_in,
    up_in,
    grad_in,
    gate_taps_ref,
    up_taps_ref,
    gate_bias_ref,
    up_bias_ref,
    *rest,
):
    gate_pad, up_pad, gate_delta, up_delta, back_ref, sems = rest[-6:]
    outs = rest[: -6] if index == 0 else rest[2:-6]
    chunk_ref, extra_ref, gate_back_ref, up_back_ref = outs[:4]
    copies = []
    if not last:
        copies = start_loads(index + 1, (gate_pre_ref, up_pre_ref, grad_ref), outs[4:], sems)
    length, width = gate_in.shape
    taps = gate_taps_ref.shape[0]
    columns = slice(index * width, (index + 1) * width)
    lead = 8
    zeros = jnp.zeros((lead, width), jnp.float32)
    gate_pad[0:lead, :] = zeros
    up_pad[0:lead, :] = zeros
    gate_delta[length:, :] = zeros
    up_delta[length:, :] = zeros
    gate_pad[lead:, :] = gate_in[...].astype(jnp.float32)
    up_pad[lead:, :] = up_in[...].astype(jnp.float32)
    gate_w = [gate_taps_ref[k : k + 1, columns] for k in range(taps)]
    up_w = [up_taps_ref[k : k + 1, columns] for k in range(taps)]
    gate_b = gate_bias_ref[columns].reshape(1, width)
    up_b = up_bias_ref[columns].reshape(1, width)

    def fold(x):
        return jnp.sum(x.reshape(STRIP // 8, 8, width), axis=0)

    def strip(i, sums):
        base = pl.multiple_of(length - (i + 1) * STRIP, STRIP)
        first = lead - (taps - 1)
        gates = [gate_pad[pl.ds(base + first + k, STRIP), :] for k in range(taps)]
        ups = [up_pad[pl.ds(base + first + k, STRIP), :] for k in range(taps)]
        gate_mixed = gates[0] * gate_w[0]
        up_mixed = ups[0] * up_w[0]
        for k in range(1, taps):
            gate_mixed = gate_mixed + gates[k] * gate_w[k]
            up_mixed = up_mixed + ups[k] * up_w[k]
        gate_mixed = gate_mixed + gate_b
        up_mixed = up_mixed + up_b
        grad = grad_in[pl.ds(base, STRIP), :].astype(jnp.float32)
        s = jax.nn.sigmoid(gate_mixed)
        scaled = grad * s
        g_delta = scaled * up_mixed * (1.0 + gate_mixed * (1.0 - s))
        u_delta = scaled * gate_mixed
        gate_delta[pl.ds(base, STRIP), :] = g_delta
        up_delta[pl.ds(base, STRIP), :] = u_delta
        g_back = g_delta * gate_w[taps - 1]
        u_back = u_delta * up_w[taps - 1]
        for k in range(1, taps):
            g_back = g_back + gate_delta[pl.ds(base + k, STRIP), :] * gate_w[taps - 1 - k]
            u_back = u_back + up_delta[pl.ds(base + k, STRIP), :] * up_w[taps - 1 - k]
        back_ref[pl.ds(base, STRIP), 0:width] = g_back.astype(jnp.bfloat16)
        back_ref[pl.ds(base, STRIP), width:] = u_back.astype(jnp.bfloat16)
        terms = [fold(g_delta * gates[k]) for k in range(taps)]
        terms.append(fold(g_delta))
        terms.extend(fold(u_delta * ups[k]) for k in range(taps))
        terms.append(fold(u_delta))
        return tuple(a + b for a, b in zip(sums, terms))

    start = tuple(jnp.zeros((8, width), jnp.float32) for _ in range(2 * taps + 2))
    sums = lax.fori_loop(0, length // STRIP, strip, start)
    rows = [jnp.sum(x, axis=0, keepdims=True) for x in sums]
    pad = jnp.zeros((ROWS - taps - 1, width), jnp.float32)
    gate_rows = jnp.concatenate(rows[: taps + 1] + [pad], axis=0)
    up_rows = jnp.concatenate(rows[taps + 1 :] + [pad], axis=0)
    extra_ref[:, 0:width] = gate_rows
    extra_ref[:, width:] = up_rows
    gate_back_ref[:, columns] = back_ref[:, 0:width]
    up_back_ref[:, columns] = back_ref[:, width:]
    chunk_ref[...] = jnp.dot(
        tokens_ref[...], back_ref[...], preferred_element_type=jnp.float32
    ).astype(jnp.bfloat16)
    for copy in copies:
        copy.wait()


def make_block(index, backs, tokens_t, signals, ready, taps, biases):
    length, hidden = signals[0].shape
    features = tokens_t.shape[0]
    last = (index + 1) * BLOCK == hidden
    back = pltpu.VMEM((length, hidden), jnp.bfloat16)
    outs = [
        pltpu.VMEM((features, 2 * BLOCK), jnp.bfloat16),
        pltpu.VMEM((ROWS, 2 * BLOCK), jnp.float32),
        back,
        back,
    ]
    if not last:
        outs += [pltpu.VMEM((length, BLOCK), jnp.bfloat16)] * 3
    return pl.pallas_call(
        functools.partial(block_kernel, index, last),
        in_specs=[VMEM] + [HBM] * 3 + [VMEM] * (7 + len(backs)),
        out_specs=[VMEM] * len(outs),
        out_shape=outs,
        scratch_shapes=[pltpu.VMEM((length + 8, BLOCK), jnp.float32)] * 4
        + [pltpu.VMEM((length, 2 * BLOCK), jnp.bfloat16), pltpu.SemaphoreType.DMA((3,))],
        input_output_aliases={11: 2, 12: 3} if backs else {},
        compiler_params=params(6),
        cost_estimate=pl.CostEstimate(
            flops=2 * features * length * 2 * BLOCK + 60 * length * BLOCK,
            bytes_accessed=6 * length * BLOCK,
            transcendentals=length * BLOCK,
        ),
        name="block",
    )(
        on_chip(tokens_t),
        *(off_chip(x) for x in signals),
        *(on_chip(x) for x in ready),
        *taps,
        *biases,
        *(on_chip(x) for x in backs),
    )


def add_kernel(a_ref, b_ref, out_ref):
    out_ref[...] = (a_ref[...].astype(jnp.float32) + b_ref[...].astype(jnp.float32)).astype(out_ref.dtype)


def add_chunk(a, b):
    return pl.pallas_call(
        add_kernel,
        out_shape=pltpu.VMEM(a.shape, a.dtype),
        compiler_params=params(4),
        cost_estimate=pl.CostEstimate(flops=a.size, bytes_accessed=6 * a.size, transcendentals=0),
        name="add",
    )(on_chip(a), on_chip(b))


def store_kernel(flags_ref, got_ref, final_ref, *refs):
    gate_ref, up_ref = refs[-2:]
    width = gate_ref.shape[1]

    @pl.when(flags_ref[0] == 1)
    def _():
        gate_ref[...] = got_ref[:, 0:width].astype(jnp.float32)
        up_ref[...] = got_ref[:, width:].astype(jnp.float32)

    @pl.when(flags_ref[0] == 0)
    def _():
        gate_ref[...] = final_ref[:, 0:width].astype(jnp.float32)
        up_ref[...] = final_ref[:, width:].astype(jnp.float32)


def store_chunk(index, hidden, flags, got, final, outs):
    features = got.shape[0]
    whole = pl.BlockSpec((features, 2 * BLOCK), lambda i: (0, 0))
    block = pl.BlockSpec((features, BLOCK), lambda i: (0, index))
    grad = pltpu.HBM((features, hidden), jnp.float32)
    return pl.pallas_call(
        store_kernel,
        grid=(1,),
        in_specs=[pl.BlockSpec(memory_space=pltpu.SMEM), whole, whole]
        + [pl.BlockSpec(memory_space=pltpu.HBM)] * len(outs),
        out_specs=[block, block],
        out_shape=[grad, grad],
        input_output_aliases={3: 0, 4: 1} if outs else {},
        compiler_params=params(8),
        cost_estimate=pl.CostEstimate(flops=got.size, bytes_accessed=8 * got.size, transcendentals=0),
        name="store",
    )(flags, on_chip(got), on_chip(final), *(off_chip(x) for x in outs))


def gather_kernel(*refs):
    out_ref = refs[-1]
    count = len(refs) - 1
    for j in range(count):
        x = refs[j][...].astype(out_ref.dtype)
        out_ref[:, j * BLOCK : (j + 1) * BLOCK] = x[:, :BLOCK]
        out_ref[:, (count + j) * BLOCK : (count + j + 1) * BLOCK] = x[:, BLOCK:]


def gather(extras):
    return pl.pallas_call(
        gather_kernel,
        out_shape=pltpu.VMEM((ROWS, len(extras) * 2 * BLOCK), jnp.bfloat16),
        compiler_params=params(2),
        name="gather",
    )(*(on_chip(x) for x in extras))


def small_kernel(flags_ref, got_ref, final_ref, *refs):
    hidden = refs[0].shape[1]
    taps = refs[0].shape[0]
    is_end = jnp.full(got_ref.shape, flags_ref[0], jnp.int32) == 1
    x = jnp.where(is_end, got_ref[...].astype(jnp.float32), final_ref[...].astype(jnp.float32))
    refs[0][...] = x[:taps, :hidden]
    refs[1][...] = x[:taps, hidden:]
    refs[2][...] = x[taps, :hidden]
    refs[3][...] = x[taps, hidden:]


def small_outs(flags, got, final, taps):
    hidden = got.shape[1] // 2
    shapes = [(taps, hidden), (taps, hidden), (hidden,), (hidden,)]
    return pl.pallas_call(
        small_kernel,
        in_specs=[SMEM, VMEM, VMEM],
        out_specs=[VMEM] * 4,
        out_shape=[jax.ShapeDtypeStruct(x, jnp.float32) for x in shapes],
        compiler_params=params(2),
        name="small",
    )(flags, on_chip(got), on_chip(final))


PIECES = 3


def feature_kernel(piece, *refs):
    flags_ref, gate_back_ref, up_back_ref, gate_ref, up_ref = refs[:5]
    width = gate_ref.shape[1]
    columns = slice(piece * width, (piece + 1) * width)
    dims = (((1,), (1,)), ((), ()))
    term = lax.dot_general(
        gate_back_ref[:, columns], gate_ref[...], dims, preferred_element_type=jnp.float32
    ) + lax.dot_general(up_back_ref[:, columns], up_ref[...], dims, preferred_element_type=jnp.float32)
    if piece > 0:
        term = term + refs[5][...]
    if piece < PIECES - 1:
        refs[-1][...] = term
        return
    send_ref, keep_ref = refs[-2:]
    half = send_ref.shape[1]
    low = term[:, :half].astype(send_ref.dtype)
    high = term[:, half:].astype(send_ref.dtype)

    @pl.when(flags_ref[1] == 1)
    def _():
        send_ref[...] = low
        keep_ref[...] = high

    @pl.when(flags_ref[1] == 0)
    def _():
        send_ref[...] = high
        keep_ref[...] = low


def feature_piece(piece, flags, gate_back, up_back, gate_weight, up_weight, total):
    length, hidden = gate_back.shape
    features = gate_weight.shape[0]
    width = hidden // PIECES
    weight = pl.BlockSpec((features, width), lambda i: (0, piece))
    whole = pl.BlockSpec((length, hidden), lambda i: (0, 0))
    full = pl.BlockSpec((length, features), lambda i: (0, 0))
    half = pl.BlockSpec((length, features // 2), lambda i: (0, 0))
    last = piece == PIECES - 1
    if last:
        out_specs, outs = [half, half], [pltpu.VMEM((length, features // 2), jnp.bfloat16)] * 2
    else:
        out_specs, outs = [full], [pltpu.VMEM((length, features), jnp.float32)]
    return pl.pallas_call(
        functools.partial(feature_kernel, piece),
        grid=(1,),
        in_specs=[SMEM, whole, whole, weight, weight] + [full] * len(total),
        out_specs=out_specs,
        out_shape=outs,
        input_output_aliases={5: 0} if total and not last else {},
        compiler_params=params(20),
        cost_estimate=pl.CostEstimate(
            flops=4 * length * width * features, bytes_accessed=4 * width * features, transcendentals=0
        ),
        name="feature",
    )(flags, on_chip(gate_back), on_chip(up_back), off_chip(gate_weight), off_chip(up_weight), *total)


def join_kernel(flags_ref, own_ref, other_ref, out_ref):
    half = own_ref.shape[1]

    @pl.when(flags_ref[1] == 1)
    def _():
        out_ref[:, half:] = own_ref[...]
        out_ref[:, :half] = other_ref[...]

    @pl.when(flags_ref[1] == 0)
    def _():
        out_ref[:, :half] = own_ref[...]
        out_ref[:, half:] = other_ref[...]


def join(flags, own, other):
    return pl.pallas_call(
        join_kernel,
        in_specs=[SMEM, VMEM, VMEM],
        out_specs=VMEM,
        out_shape=jax.ShapeDtypeStruct((own.shape[0], 2 * own.shape[1]), own.dtype),
        compiler_params=params(8),
        name="join",
    )(flags, on_chip(own), on_chip(other))


INWARD = [(0, 1), (3, 2)]
OUTWARD = [(1, 0), (2, 3)]
MIDDLE = [(1, 2), (2, 1)]


def line_chunk(part, add):
    got = lax.ppermute(part, "rep", INWARD)
    pair = add(part, got)
    other = lax.ppermute(pair, "rep", MIDDLE)
    final = add(pair, other)
    got = lax.ppermute(final, "rep", OUTWARD)
    return got, final


NEAR = [(0, 1), (1, 0), (2, 3), (3, 2)]
FAR = [(0, 2), (2, 0), (1, 3), (3, 1)]


def sum_over_four(flags, send, keep):
    got = lax.ppermute(send, "tp", NEAR)
    own = add_chunk(keep, got)
    got = lax.ppermute(own, "tp", FAR)
    own = add_chunk(own, got)
    other = lax.ppermute(own, "tp", NEAR)
    return join(flags, own, other)


def per_device(
    tokens,
    gate_pre,
    up_pre,
    hidden_grad,
    gate_weight,
    up_weight,
    gate_taps,
    up_taps,
    gate_bias,
    up_bias,
):
    taps, hidden = gate_taps.shape
    count = hidden // BLOCK
    plane = lax.axis_index("rep")
    is_end = (plane == 0) | (plane == 3)
    flags = jnp.stack([is_end.astype(jnp.int32), lax.axis_index("tp") % 2])
    signals = (gate_pre, up_pre, hidden_grad)
    biases = (gate_bias, up_bias)
    tokens_t, *ready = turn(flags, tokens, signals)
    chunks, extras, backs_at, backs = [], [], [], ()
    for j in range(count):
        chunk, extra, *more = make_block(
            j, backs, tokens_t, signals, ready, (gate_taps, up_taps), biases
        )
        backs, ready = more[:2], more[2:] or ready
        backs_at.append(backs)
        chunks.append(chunk)
        extras.append(extra)
    total = ()
    for piece in range(PIECES):
        total = feature_piece(piece, flags, *backs, gate_weight, up_weight, total)
    send, keep = total
    if lax.axis_size("tp") == 4:
        result = sum_over_four(flags, send, keep)
    else:
        odd = flags[1] == 1
        partial = jnp.where(
            odd, jnp.concatenate([send, keep], axis=1), jnp.concatenate([keep, send], axis=1)
        )
        own = lax.psum_scatter(partial, "tp", scatter_dimension=1, tiled=True)
        result = lax.all_gather(own, "tp", axis=1, tiled=True)
    extra = gather(extras)
    if lax.axis_size("rep") == 4:
        outs = ()
        for j in range(count):
            got, final = line_chunk(chunks[j], add_chunk)
            outs = store_chunk(j, hidden, flags, got, final, outs)
        gate, up = outs
        got, final = line_chunk(extra, add_chunk)
    else:
        sums = [lax.psum(c, "rep") for c in chunks]
        gate = jnp.concatenate([c[:, :BLOCK] for c in sums], axis=1).astype(jnp.float32)
        up = jnp.concatenate([c[:, BLOCK:] for c in sums], axis=1).astype(jnp.float32)
        got = final = lax.psum(extra, "rep")
    gate_taps_grad, up_taps_grad, gate_bias_grad, up_bias_grad = small_outs(flags, got, final, taps)
    return (
        result,
        gate,
        up,
        gate_taps_grad,
        up_taps_grad,
        gate_bias_grad,
        up_bias_grad,
    )


def solution(mesh):
    return jax.shard_map(
        per_device,
        mesh=mesh,
        in_specs=(
            P("rep", "fs"),
            P("rep", "tp"),
            P("rep", "tp"),
            P("rep", "tp"),
            P("fs", "tp"),
            P("fs", "tp"),
            P(None, "tp"),
            P(None, "tp"),
            P("tp"),
            P("tp"),
        ),
        out_specs=(
            P("rep", "fs"),
            P("fs", "tp"),
            P("fs", "tp"),
            P(None, "tp"),
            P(None, "tp"),
            P("tp"),
            P("tp"),
        ),
        check_vma=False,
    )
```

time: 330 us -> 369 us (1.12)
  Pallas kernels: 0 us -> 58.1 us
  starting transfers between devices: 0.12 us -> 57.8 us
  other arithmetic: 27.4 us -> 0.08 us
  blocking collectives: 21.1 us -> 0 us
  waiting for transfers between devices: 231 us -> 251 us
  local copies, waits for them, and re-layouts: 17.4 us -> 0.01 us
  matrix products: 17 us -> 0 us
  between operations: 15.7 us -> 1.45 us
    ppermute x0 -> x42, waiting for transfers between devices: none -> 251 us  [the longest x13 173 us: line_chunk(): got = lax.ppermute(final, 'rep', OUTWARD)]
    psum x1 -> x0, waiting for transfers between devices: 200 us -> none  [per_device(): lax.psum(gate_local.astype(jnp.bfloat16), 'rep').astype(jnp.float32)]
    pallas_call x0 -> x59, Pallas kernels: none -> 58.1 us  [the longest x12 19.4 us: make_block(): pl.pallas_call(functools.partial(block_kernel, index, last), in_specs=[VM...]
    ppermute x0 -> x42, starting transfers between devices: none -> 57.8 us  [the longest x13 30.6 us: line_chunk(): got = lax.ppermute(part, 'rep', INWARD)]
    reduce_scatter x1 -> x0, waiting for transfers between devices: 30.9 us -> none  [per_device(): lax.psum_scatter(full_partial.astype(jnp.bfloat16), 'tp', scatter_dimensi...]
    psum x1 -> x0, blocking collectives: 21.1 us -> none  [per_device(): lax.psum(gate_tap_part.astype(jnp.bfloat16), 'rep').astype(jnp.float32)]
    dot_general x4 -> x0, matrix products: 17 us -> none  [the longest x1 6.58 us: per_device(): lax.dot_general(tokens, gate_back, token_dims, preferred_element_type=jnp...]
    reduce_sum x2 -> x0, other arithmetic: 16.1 us -> none  [the longest x1 10.3 us: backward_terms(): jnp.sum(gate_delta, axis=0)]
  transfers between devices with their start and end apart: 3 -> 42, of which waited for: 2 -> 20; matrix products, arithmetic and copies ran while one was open for 4% -> 0% of each run, Pallas kernels for 0% -> 14%
where the time goes in v1:
time: 369 us; the launch traced here: 368 us
  waiting for transfers between devices  251 us (68%)
  Pallas kernels  58.1 us (16%)
  starting transfers between devices  57.8 us (16%)
    ppermute x13, waiting for transfers between devices, line_chunk(): got = lax.ppermute(final, 'rep', OUTWARD)  173 us
    ppermute x13, waiting for transfers between devices, line_chunk(): got = lax.ppermute(part, 'rep', INWARD)  77.9 us
    ppermute x13, starting transfers between devices, line_chunk(): got = lax.ppermute(part, 'rep', INWARD)  30.6 us
    pallas_call x12, Pallas kernels, make_block(): pl.pallas_call(functools.partial(block_kernel, index, last), in_specs=[VM...  19.4 us
    pallas_call x12, Pallas kernels, store_chunk(): pl.pallas_call(store_kernel, grid=(1,), in_specs=[pl.BlockSpec(memory_spa...  19.1 us
    ppermute x13, starting transfers between devices, line_chunk(): got = lax.ppermute(final, 'rep', OUTWARD)  16.7 us
    pallas_call x3, Pallas kernels, feature_piece(): pl.pallas_call(functools.partial(feature_kernel, piece), grid=(1,), in_sp...  10.5 us
    ppermute x13, starting transfers between devices, line_chunk(): other = lax.ppermute(pair, 'rep', MIDDLE)  8.95 us
  transfers between devices with their start and end apart: 42, of which 20 were waited for; matrix products, arithmetic and copies ran while one was open for 0% of the time, Pallas kernels for 14%

profile of v1, /device:TPU:0, one launch (start us, length us, event | category | flops | bytes accessed | tf_op | source)
XLA Modules:
  0.0 368.1 jit_solution(4391955096507132322)
XLA Ops:
  0.7 2.6 turn.1
  3.4 1.6 block.12
  5.0 5.0 %collective-permute-start.36 = (bf16[1024,256]{1,0:T(8,128)(2,1)S(1)}, bf16[1024,256]{1,0:T(8,128)(2,1)S(1)}, u32[]{:S(2)}, u32[]{:S(2)}) collective-permute-start(bf16[1024,256]{1,0:T(8,128)(2,1)S(1)} %get-tuple-element.196.a_ref), channel_id=1, source_target_pairs={{0,8},{24,16},{1,9},{25,17},{2,10},{26,18},{3,11},{27,19},{4,12},{... | collective-permute-start | bytes 1572872 | tf_op jit(solution)/shard_map/ppermute | solution.py:374
  10.0 1.6 block.13
  11.6 1.3 collective-permute-start.33
  13.0 1.6 block.14
  14.6 1.3 collective-permute-start.30
  15.9 1.6 block.15
  17.5 1.3 collective-permute-start.27
  18.9 1.6 block.16
  20.5 1.6 block.17
  22.1 1.6 block.18
  23.7 1.6 block.19
  25.4 1.6 block.20
  27.0 1.6 block.21
  28.6 1.6 block.22
  30.2 1.6 block.23
  31.9 1.3 collective-permute-start.39
  33.2 22.7 %collective-permute-done.39.b_ref = bf16[8,3072]{1,0:T(8,128)(2,1)S(1)} collective-permute-done((bf16[8,3072]{1,0:T(8,128)(2,1)S(1)}, bf16[8,3072]{1,0:T(8,128)(2,1)S(1)}, u32[]{:S(2)}, u32[]{:S(2)}) %collective-permute-start.39) | collective-permute-done | bytes 49184 | tf_op jit(solution)/shard_map/ppermute | solution.py:374
  57.9 9.8 %collective-permute-done.41.got_ref = bf16[8,3072]{1,0:T(8,128)(2,1)S(1)} collective-permute-done((bf16[8,3072]{1,0:T(8,128)(2,1)S(1)}, bf16[8,3072]{1,0:T(8,128)(2,1)S(1)}, u32[]{:S(2)}, u32[]{:S(2)}) %collective-permute-start.41) | collective-permute-done | bytes 49184 | tf_op jit(solution)/shard_map/ppermute | solution.py:378
  67.8 1.6 collective-permute-start.24
  69.4 1.3 collective-permute-start.21
  70.7 1.3 collective-permute-start.18
  72.1 3.4 feature.3.refs_5_
  75.5 1.3 collective-permute-start.15
  76.8 1.5 collective-permute-start.12
  78.3 3.5 feature.4.refs_5_
  81.8 3.6 feature.5
  85.6 7.3 %collective-permute-done.21.b_ref = bf16[1024,256]{1,0:T(8,128)(2,1)S(1)} collective-permute-done((bf16[1024,256]{1,0:T(8,128)(2,1)S(1)}, bf16[1024,256]{1,0:T(8,128)(2,1)S(1)}, u32[]{:S(2)}, u32[]{:S(2)}) %collective-permute-start.21) | collective-permute-done | bytes 524320 | tf_op jit(solution)/shard_map/ppermute | solution.py:374
  92.9 4.4 %collective-permute-start.9 = (bf16[1024,256]{1,0:T(8,128)(2,1)S(1)}, bf16[1024,256]{1,0:T(8,128)(2,1)S(1)}, u32[]{:S(2)}, u32[]{:S(2)}) collective-permute-start(bf16[1024,256]{1,0:T(8,128)(2,1)S(1)} %get-tuple-element.187.a_ref), channel_id=1, source_target_pairs={{0,8},{24,16},{1,9},{25,17},{2,10},{26,18},{3,11},{27,19},{4,12},{... | collective-permute-start | bytes 1572872 | tf_op jit(solution)/shard_map/ppermute | solution.py:374
  97.3 6.8 %collective-permute-done.18.b_ref = bf16[1024,256]{1,0:T(8,128)(2,1)S(1)} collective-permute-done((bf16[1024,256]{1,0:T(8,128)(2,1)S(1)}, bf16[1024,256]{1,0:T(8,128)(2,1)S(1)}, u32[]{:S(2)}, u32[]{:S(2)}) %collective-permute-start.18) | collective-permute-done | bytes 524320 | tf_op jit(solution)/shard_map/ppermute | solution.py:374
  104.1 4.4 %collective-permute-start.6 = (bf16[1024,256]{1,0:T(8,128)(2,1)S(1)}, bf16[1024,256]{1,0:T(8,128)(2,1)S(1)}, u32[]{:S(2)}, u32[]{:S(2)}) collective-permute-start(bf16[1024,256]{1,0:T(8,128)(2,1)S(1)} %get-tuple-element.186.a_ref), channel_id=1, source_target_pairs={{0,8},{24,16},{1,9},{25,17},{2,10},{26,18},{3,11},{27,19},{4,12},{... | collective-permute-start | bytes 1572872 | tf_op jit(solution)/shard_map/ppermute | solution.py:374
  108.5 6.8 %collective-permute-done.15.b_ref = bf16[1024,256]{1,0:T(8,128)(2,1)S(1)} collective-permute-done((bf16[1024,256]{1,0:T(8,128)(2,1)S(1)}, bf16[1024,256]{1,0:T(8,128)(2,1)S(1)}, u32[]{:S(2)}, u32[]{:S(2)}) %collective-permute-start.15) | collective-permute-done | bytes 524320 | tf_op jit(solution)/shard_map/ppermute | solution.py:374
  115.3 4.4 %collective-permute-start.3 = (bf16[1024,256]{1,0:T(8,128)(2,1)S(1)}, bf16[1024,256]{1,0:T(8,128)(2,1)S(1)}, u32[]{:S(2)}, u32[]{:S(2)}) collective-permute-start(bf16[1024,256]{1,0:T(8,128)(2,1)S(1)} %get-tuple-element.185.a_ref), channel_id=1, source_target_pairs={{0,8},{24,16},{1,9},{25,17},{2,10},{26,18},{3,11},{27,19},{4,12},{... | collective-permute-start | bytes 1572872 | tf_op jit(solution)/shard_map/ppermute | solution.py:374
  119.9 6.7 %collective-permute-done.12.b_ref = bf16[1024,256]{1,0:T(8,128)(2,1)S(1)} collective-permute-done((bf16[1024,256]{1,0:T(8,128)(2,1)S(1)}, bf16[1024,256]{1,0:T(8,128)(2,1)S(1)}, u32[]{:S(2)}, u32[]{:S(2)}) %collective-permute-start.12) | collective-permute-done | bytes 524320 | tf_op jit(solution)/shard_map/ppermute | solution.py:374
  127.4 10.4 %collective-permute-done.9.b_ref = bf16[1024,256]{1,0:T(8,128)(2,1)S(1)} collective-permute-done((bf16[1024,256]{1,0:T(8,128)(2,1)S(1)}, bf16[1024,256]{1,0:T(8,128)(2,1)S(1)}, u32[]{:S(2)}, u32[]{:S(2)}) %collective-permute-start.9) | collective-permute-done | bytes 524320 | tf_op jit(solution)/shard_map/ppermute | solution.py:374
  138.6 10.4 %collective-permute-done.6.b_ref = bf16[1024,256]{1,0:T(8,128)(2,1)S(1)} collective-permute-done((bf16[1024,256]{1,0:T(8,128)(2,1)S(1)}, bf16[1024,256]{1,0:T(8,128)(2,1)S(1)}, u32[]{:S(2)}, u32[]{:S(2)}) %collective-permute-start.6) | collective-permute-done | bytes 524320 | tf_op jit(solution)/shard_map/ppermute | solution.py:374
  149.9 6.7 %collective-permute-done.3.b_ref = bf16[1024,256]{1,0:T(8,128)(2,1)S(1)} collective-permute-done((bf16[1024,256]{1,0:T(8,128)(2,1)S(1)}, bf16[1024,256]{1,0:T(8,128)(2,1)S(1)}, u32[]{:S(2)}, u32[]{:S(2)}) %collective-permute-start.3) | collective-permute-done | bytes 524320 | tf_op jit(solution)/shard_map/ppermute | solution.py:374
  163.4 1.6 collective-permute-start.1
  170.2 1.3 collective-permute-start.29
  171.7 69.7 %collective-permute-done.38.got_ref = bf16[1024,256]{1,0:T(8,128)(2,1)S(1)} collective-permute-done((bf16[1024,256]{1,0:T(8,128)(2,1)S(1)}, bf16[1024,256]{1,0:T(8,128)(2,1)S(1)}, u32[]{:S(2)}, u32[]{:S(2)}) %collective-permute-start.38) | collective-permute-done | bytes 524320 | tf_op jit(solution)/shard_map/ppermute | solution.py:378
  242.8 9.8 %collective-permute-done.35.got_ref = bf16[1024,256]{1,0:T(8,128)(2,1)S(1)} collective-permute-done((bf16[1024,256]{1,0:T(8,128)(2,1)S(1)}, bf16[1024,256]{1,0:T(8,128)(2,1)S(1)}, u32[]{:S(2)}, u32[]{:S(2)}) %collective-permute-start.35) | collective-permute-done | bytes 524320 | tf_op jit(solution)/shard_map/ppermute | solution.py:378
  254.0 9.8 %collective-permute-done.32.got_ref = bf16[1024,256]{1,0:T(8,128)(2,1)S(1)} collective-permute-done((bf16[1024,256]{1,0:T(8,128)(2,1)S(1)}, bf16[1024,256]{1,0:T(8,128)(2,1)S(1)}, u32[]{:S(2)}, u32[]{:S(2)}) %collective-permute-start.32) | collective-permute-done | bytes 524320 | tf_op jit(solution)/shard_map/ppermute | solution.py:378
  266.8 11.0 %collective-permute-done.29.got_ref = bf16[1024,256]{1,0:T(8,128)(2,1)S(1)} collective-permute-done((bf16[1024,256]{1,0:T(8,128)(2,1)S(1)}, bf16[1024,256]{1,0:T(8,128)(2,1)S(1)}, u32[]{:S(2)}, u32[]{:S(2)}) %collective-permute-start.29) | collective-permute-done | bytes 524320 | tf_op jit(solution)/shard_map/ppermute | solution.py:378
  277.9 11.1 %collective-permute-done.26.got_ref = bf16[1024,256]{1,0:T(8,128)(2,1)S(1)} collective-permute-done((bf16[1024,256]{1,0:T(8,128)(2,1)S(1)}, bf16[1024,256]{1,0:T(8,128)(2,1)S(1)}, u32[]{:S(2)}, u32[]{:S(2)}) %collective-permute-start.26) | collective-permute-done | bytes 524320 | tf_op jit(solution)/shard_map/ppermute | solution.py:378
  290.4 9.8 %collective-permute-done.23.got_ref = bf16[1024,256]{1,0:T(8,128)(2,1)S(1)} collective-permute-done((bf16[1024,256]{1,0:T(8,128)(2,1)S(1)}, bf16[1024,256]{1,0:T(8,128)(2,1)S(1)}, u32[]{:S(2)}, u32[]{:S(2)}) %collective-permute-start.23) | collective-permute-done | bytes 524320 | tf_op jit(solution)/shard_map/ppermute | solution.py:378
  301.7 9.8 %collective-permute-done.20.got_ref = bf16[1024,256]{1,0:T(8,128)(2,1)S(1)} collective-permute-done((bf16[1024,256]{1,0:T(8,128)(2,1)S(1)}, bf16[1024,256]{1,0:T(8,128)(2,1)S(1)}, u32[]{:S(2)}, u32[]{:S(2)}) %collective-permute-start.20) | collective-permute-done | bytes 524320 | tf_op jit(solution)/shard_map/ppermute | solution.py:378
  312.9 9.8 %collective-permute-done.17.got_ref = bf16[1024,256]{1,0:T(8,128)(2,1)S(1)} collective-permute-done((bf16[1024,256]{1,0:T(8,128)(2,1)S(1)}, bf16[1024,256]{1,0:T(8,128)(2,1)S(1)}, u32[]{:S(2)}, u32[]{:S(2)}) %collective-permute-start.17) | collective-permute-done | bytes 524320 | tf_op jit(solution)/shard_map/ppermute | solution.py:378
  325.2 1.6 store.12
  326.7 1.6 store.13
  328.3 1.6 store.14
  329.9 1.6 store.15
  331.5 1.6 store.16
  333.1 1.6 store.17
  334.7 1.6 store.18
  336.3 1.6 store.19
  337.9 1.6 store.20
  339.5 5.7 %collective-permute-done.11.got_ref = bf16[1024,256]{1,0:T(8,128)(2,1)S(1)} collective-permute-done((bf16[1024,256]{1,0:T(8,128)(2,1)S(1)}, bf16[1024,256]{1,0:T(8,128)(2,1)S(1)}, u32[]{:S(2)}, u32[]{:S(2)}) %collective-permute-start.11) | collective-permute-done | bytes 524320 | tf_op jit(solution)/shard_map/ppermute | solution.py:378
  345.2 1.6 store.21
  346.8 9.6 %collective-permute-done.8.got_ref = bf16[1024,256]{1,0:T(8,128)(2,1)S(1)} collective-permute-done((bf16[1024,256]{1,0:T(8,128)(2,1)S(1)}, bf16[1024,256]{1,0:T(8,128)(2,1)S(1)}, u32[]{:S(2)}, u32[]{:S(2)}) %collective-permute-start.8) | collective-permute-done | bytes 524320 | tf_op jit(solution)/shard_map/ppermute | solution.py:378
  356.4 1.6 store.22
  358.0 6.7 %collective-permute-done.5.got_ref = bf16[1024,256]{1,0:T(8,128)(2,1)S(1)} collective-permute-done((bf16[1024,256]{1,0:T(8,128)(2,1)S(1)}, bf16[1024,256]{1,0:T(8,128)(2,1)S(1)}, u32[]{:S(2)}, u32[]{:S(2)}) %collective-permute-start.5) | collective-permute-done | bytes 524320 | tf_op jit(solution)/shard_map/ppermute | solution.py:378
  364.7 1.6 store.23
  366.3 1.8 join.1
  (88 shorter events, 29.3 us)
Async XLA Ops:
  0.7 2.6 copy-start
  0.7 2.6 copy-start.1
  0.7 2.7 copy-start.2
  0.7 2.7 copy-start.3
  5.0 64.4 %collective-permute-start.36 = (bf16[1024,256]{1,0:T(8,128)(2,1)S(1)}, bf16[1024,256]{1,0:T(8,128)(2,1)S(1)}, u32[]{:S(2)}, u32[]{:S(2)}) collective-permute-start(bf16[1024,256]{1,0:T(8,128)(2,1)S(1)} %get-tuple-element.196.a_ref), channel_id=1, source_target_pairs={{0,8},{24,16},{1,9},{25,17},{2,10},{26,18},{3,11},{27,19},{4,12},{... | collective-permute-start | bytes 1572872 | tf_op jit(solution)/shard_map/ppermute | solution.py:374
  11.6 59.1 %collective-permute-start.33 = (bf16[1024,256]{1,0:T(8,128)(2,1)S(1)}, bf16[1024,256]{1,0:T(8,128)(2,1)S(1)}, u32[]{:S(2)}, u32[]{:S(2)}) collective-permute-start(bf16[1024,256]{1,0:T(8,128)(2,1)S(1)} %get-tuple-element.195.a_ref), channel_id=1, source_target_pairs={{0,8},{24,16},{1,9},{25,17},{2,10},{26,18},{3,11},{27,19},{4,12},{... | collective-permute-start | bytes 1572872 | tf_op jit(solution)/shard_map/ppermute | solution.py:374
  14.6 60.9 %collective-permute-start.30 = (bf16[1024,256]{1,0:T(8,128)(2,1)S(1)}, bf16[1024,256]{1,0:T(8,128)(2,1)S(1)}, u32[]{:S(2)}, u32[]{:S(2)}) collective-permute-start(bf16[1024,256]{1,0:T(8,128)(2,1)S(1)} %get-tuple-element.194.a_ref), channel_id=1, source_target_pairs={{0,8},{24,16},{1,9},{25,17},{2,10},{26,18},{3,11},{27,19},{4,12},{... | collective-permute-start | bytes 1572872 | tf_op jit(solution)/shard_map/ppermute | solution.py:374
  17.5 59.3 %collective-permute-start.27 = (bf16[1024,256]{1,0:T(8,128)(2,1)S(1)}, bf16[1024,256]{1,0:T(8,128)(2,1)S(1)}, u32[]{:S(2)}, u32[]{:S(2)}) collective-permute-start(bf16[1024,256]{1,0:T(8,128)(2,1)S(1)} %get-tuple-element.193.a_ref), channel_id=1, source_target_pairs={{0,8},{24,16},{1,9},{25,17},{2,10},{26,18},{3,11},{27,19},{4,12},{... | collective-permute-start | bytes 1572872 | tf_op jit(solution)/shard_map/ppermute | solution.py:374
  31.9 24.0 %collective-permute-start.39 = (bf16[8,3072]{1,0:T(8,128)(2,1)S(1)}, bf16[8,3072]{1,0:T(8,128)(2,1)S(1)}, u32[]{:S(2)}, u32[]{:S(2)}) collective-permute-start(bf16[8,3072]{1,0:T(8,128)(2,1)S(1)} %gather.1.a_ref), channel_id=1, source_target_pairs={{0,8},{24,16},{1,9},{25,17},{2,10},{26,18},{3,11},{27,19},{4,12},{... | collective-permute-start | bytes 147464 | tf_op jit(solution)/shard_map/ppermute | solution.py:374
  55.9 0.7 collective-permute-start.40
  56.6 11.1 %collective-permute-start.41 = (bf16[8,3072]{1,0:T(8,128)(2,1)S(1)}, bf16[8,3072]{1,0:T(8,128)(2,1)S(1)}, u32[]{:S(2)}, u32[]{:S(2)}) collective-permute-start(bf16[8,3072]{1,0:T(8,128)(2,1)S(1)} %add.62.final_ref), channel_id=1, source_target_pairs={{8,0},{16,24},{9,1},{17,25},{10,2},{18,26},{11,3},{19,27},{12,4},{... | collective-permute-start | bytes 147464 | tf_op jit(solution)/shard_map/ppermute | solution.py:378
  67.8 17.7 %collective-permute-start.24 = (bf16[1024,256]{1,0:T(8,128)(2,1)S(1)}, bf16[1024,256]{1,0:T(8,128)(2,1)S(1)}, u32[]{:S(2)}, u32[]{:S(2)}) collective-permute-start(bf16[1024,256]{1,0:T(8,128)(2,1)S(1)} %get-tuple-element.192.a_ref), channel_id=1, source_target_pairs={{0,8},{24,16},{1,9},{25,17},{2,10},{26,18},{3,11},{27,19},{4,12},{... | collective-permute-start | bytes 1572872 | tf_op jit(solution)/shard_map/ppermute | solution.py:374
  69.4 23.5 %collective-permute-start.21 = (bf16[1024,256]{1,0:T(8,128)(2,1)S(1)}, bf16[1024,256]{1,0:T(8,128)(2,1)S(1)}, u32[]{:S(2)}, u32[]{:S(2)}) collective-permute-start(bf16[1024,256]{1,0:T(8,128)(2,1)S(1)} %get-tuple-element.191.a_ref), channel_id=1, source_target_pairs={{0,8},{24,16},{1,9},{25,17},{2,10},{26,18},{3,11},{27,19},{4,12},{... | collective-permute-start | bytes 1572872 | tf_op jit(solution)/shard_map/ppermute | solution.py:374
  70.7 33.4 %collective-permute-start.18 = (bf16[1024,256]{1,0:T(8,128)(2,1)S(1)}, bf16[1024,256]{1,0:T(8,128)(2,1)S(1)}, u32[]{:S(2)}, u32[]{:S(2)}) collective-permute-start(bf16[1024,256]{1,0:T(8,128)(2,1)S(1)} %get-tuple-element.190.a_ref), channel_id=1, source_target_pairs={{0,8},{24,16},{1,9},{25,17},{2,10},{26,18},{3,11},{27,19},{4,12},{... | collective-permute-start | bytes 1572872 | tf_op jit(solution)/shard_map/ppermute | solution.py:374
  75.5 39.9 %collective-permute-start.15 = (bf16[1024,256]{1,0:T(8,128)(2,1)S(1)}, bf16[1024,256]{1,0:T(8,128)(2,1)S(1)}, u32[]{:S(2)}, u32[]{:S(2)}) collective-permute-start(bf16[1024,256]{1,0:T(8,128)(2,1)S(1)} %get-tuple-element.189.a_ref), channel_id=1, source_target_pairs={{0,8},{24,16},{1,9},{25,17},{2,10},{26,18},{3,11},{27,19},{4,12},{... | collective-permute-start | bytes 1572872 | tf_op jit(solution)/shard_map/ppermute | solution.py:374
  76.8 49.8 %collective-permute-start.12 = (bf16[1024,256]{1,0:T(8,128)(2,1)S(1)}, bf16[1024,256]{1,0:T(8,128)(2,1)S(1)}, u32[]{:S(2)}, u32[]{:S(2)}) collective-permute-start(bf16[1024,256]{1,0:T(8,128)(2,1)S(1)} %get-tuple-element.188.a_ref), channel_id=1, source_target_pairs={{0,8},{24,16},{1,9},{25,17},{2,10},{26,18},{3,11},{27,19},{4,12},{... | collective-permute-start | bytes 1572872 | tf_op jit(solution)/shard_map/ppermute | solution.py:374
  85.5 71.9 %collective-permute-start = (bf16[768,512]{1,0:T(8,128)(2,1)S(1)}, bf16[768,512]{1,0:T(8,128)(2,1)S(1)}, u32[]{:S(2)}, u32[]{:S(2)}) collective-permute-start(bf16[768,512]{1,0:T(8,128)(2,1)S(1)} %get-tuple-element.184), channel_id=1, source_target_pairs={{0,1},{1,0},{2,3},{3,2},{4,5},{5,4},{6,7},{7,6},{8,9},{9,8},{10,11... | collective-permute-start | bytes 2359304 | tf_op jit(solution)/shard_map/ppermute | solution.py:387
  92.9 44.9 %collective-permute-start.9 = (bf16[1024,256]{1,0:T(8,128)(2,1)S(1)}, bf16[1024,256]{1,0:T(8,128)(2,1)S(1)}, u32[]{:S(2)}, u32[]{:S(2)}) collective-permute-start(bf16[1024,256]{1,0:T(8,128)(2,1)S(1)} %get-tuple-element.187.a_ref), channel_id=1, source_target_pairs={{0,8},{24,16},{1,9},{25,17},{2,10},{26,18},{3,11},{27,19},{4,12},{... | collective-permute-start | bytes 1572872 | tf_op jit(solution)/shard_map/ppermute | solution.py:374
  104.1 44.9 %collective-permute-start.6 = (bf16[1024,256]{1,0:T(8,128)(2,1)S(1)}, bf16[1024,256]{1,0:T(8,128)(2,1)S(1)}, u32[]{:S(2)}, u32[]{:S(2)}) collective-permute-start(bf16[1024,256]{1,0:T(8,128)(2,1)S(1)} %get-tuple-element.186.a_ref), channel_id=1, source_target_pairs={{0,8},{24,16},{1,9},{25,17},{2,10},{26,18},{3,11},{27,19},{4,12},{... | collective-permute-start | bytes 1572872 | tf_op jit(solution)/shard_map/ppermute | solution.py:374
  115.3 41.2 %collective-permute-start.3 = (bf16[1024,256]{1,0:T(8,128)(2,1)S(1)}, bf16[1024,256]{1,0:T(8,128)(2,1)S(1)}, u32[]{:S(2)}, u32[]{:S(2)}) collective-permute-start(bf16[1024,256]{1,0:T(8,128)(2,1)S(1)} %get-tuple-element.185.a_ref), channel_id=1, source_target_pairs={{0,8},{24,16},{1,9},{25,17},{2,10},{26,18},{3,11},{27,19},{4,12},{... | collective-permute-start | bytes 1572872 | tf_op jit(solution)/shard_map/ppermute | solution.py:374
  126.6 31.7 %collective-permute-start.37 = (bf16[1024,256]{1,0:T(8,128)(2,1)S(1)}, bf16[1024,256]{1,0:T(8,128)(2,1)S(1)}, u32[]{:S(2)}, u32[]{:S(2)}) collective-permute-start(bf16[1024,256]{1,0:T(8,128)(2,1)S(1)} %add.59.a_ref), channel_id=1, source_target_pairs={{8,16},{16,8},{9,17},{17,9},{10,18},{18,10},{11,19},{19,11},{12,20... | collective-permute-start | bytes 1572872 | tf_op jit(solution)/shard_map/ppermute | solution.py:376
  137.8 21.3 %collective-permute-start.34 = (bf16[1024,256]{1,0:T(8,128)(2,1)S(1)}, bf16[1024,256]{1,0:T(8,128)(2,1)S(1)}, u32[]{:S(2)}, u32[]{:S(2)}) collective-permute-start(bf16[1024,256]{1,0:T(8,128)(2,1)S(1)} %add.57.a_ref), channel_id=1, source_target_pairs={{8,16},{16,8},{9,17},{17,9},{10,18},{18,10},{11,19},{19,11},{12,20... | collective-permute-start | bytes 1572872 | tf_op jit(solution)/shard_map/ppermute | solution.py:376
  149.1 10.9 %collective-permute-start.31 = (bf16[1024,256]{1,0:T(8,128)(2,1)S(1)}, bf16[1024,256]{1,0:T(8,128)(2,1)S(1)}, u32[]{:S(2)}, u32[]{:S(2)}) collective-permute-start(bf16[1024,256]{1,0:T(8,128)(2,1)S(1)} %add.55.a_ref), channel_id=1, source_target_pairs={{8,16},{16,8},{9,17},{17,9},{10,18},{18,10},{11,19},{19,11},{12,20... | collective-permute-start | bytes 1572872 | tf_op jit(solution)/shard_map/ppermute | solution.py:376
  156.6 4.2 %collective-permute-start.28 = (bf16[1024,256]{1,0:T(8,128)(2,1)S(1)}, bf16[1024,256]{1,0:T(8,128)(2,1)S(1)}, u32[]{:S(2)}, u32[]{:S(2)}) collective-permute-start(bf16[1024,256]{1,0:T(8,128)(2,1)S(1)} %add.53.a_ref), channel_id=1, source_target_pairs={{8,16},{16,8},{9,17},{17,9},{10,18},{18,10},{11,19},{19,11},{12,20... | collective-permute-start | bytes 1572872 | tf_op jit(solution)/shard_map/ppermute | solution.py:376
  157.4 4.2 %collective-permute-start.25 = (bf16[1024,256]{1,0:T(8,128)(2,1)S(1)}, bf16[1024,256]{1,0:T(8,128)(2,1)S(1)}, u32[]{:S(2)}, u32[]{:S(2)}) collective-permute-start(bf16[1024,256]{1,0:T(8,128)(2,1)S(1)} %add.51.a_ref), channel_id=1, source_target_pairs={{8,16},{16,8},{9,17},{17,9},{10,18},{18,10},{11,19},{19,11},{12,20... | collective-permute-start | bytes 1572872 | tf_op jit(solution)/shard_map/ppermute | solution.py:376
  158.3 4.2 %collective-permute-start.22 = (bf16[1024,256]{1,0:T(8,128)(2,1)S(1)}, bf16[1024,256]{1,0:T(8,128)(2,1)S(1)}, u32[]{:S(2)}, u32[]{:S(2)}) collective-permute-start(bf16[1024,256]{1,0:T(8,128)(2,1)S(1)} %add.49.a_ref), channel_id=1, source_target_pairs={{8,16},{16,8},{9,17},{17,9},{10,18},{18,10},{11,19},{19,11},{12,20... | collective-permute-start | bytes 1572872 | tf_op jit(solution)/shard_map/ppermute | solution.py:376
  159.1 4.3 %collective-permute-start.19 = (bf16[1024,256]{1,0:T(8,128)(2,1)S(1)}, bf16[1024,256]{1,0:T(8,128)(2,1)S(1)}, u32[]{:S(2)}, u32[]{:S(2)}) collective-permute-start(bf16[1024,256]{1,0:T(8,128)(2,1)S(1)} %add.47.a_ref), channel_id=1, source_target_pairs={{8,16},{16,8},{9,17},{17,9},{10,18},{18,10},{11,19},{19,11},{12,20... | collective-permute-start | bytes 1572872 | tf_op jit(solution)/shard_map/ppermute | solution.py:376
  159.9 5.1 %collective-permute-start.16 = (bf16[1024,256]{1,0:T(8,128)(2,1)S(1)}, bf16[1024,256]{1,0:T(8,128)(2,1)S(1)}, u32[]{:S(2)}, u32[]{:S(2)}) collective-permute-start(bf16[1024,256]{1,0:T(8,128)(2,1)S(1)} %add.45.a_ref), channel_id=1, source_target_pairs={{8,16},{16,8},{9,17},{17,9},{10,18},{18,10},{11,19},{19,11},{12,20... | collective-permute-start | bytes 1572872 | tf_op jit(solution)/shard_map/ppermute | solution.py:376
  160.8 5.1 %collective-permute-start.13 = (bf16[1024,256]{1,0:T(8,128)(2,1)S(1)}, bf16[1024,256]{1,0:T(8,128)(2,1)S(1)}, u32[]{:S(2)}, u32[]{:S(2)}) collective-permute-start(bf16[1024,256]{1,0:T(8,128)(2,1)S(1)} %add.43.a_ref), channel_id=1, source_target_pairs={{8,16},{16,8},{9,17},{17,9},{10,18},{18,10},{11,19},{19,11},{12,20... | collective-permute-start | bytes 1572872 | tf_op jit(solution)/shard_map/ppermute | solution.py:376
  161.6 5.7 %collective-permute-start.10 = (bf16[1024,256]{1,0:T(8,128)(2,1)S(1)}, bf16[1024,256]{1,0:T(8,128)(2,1)S(1)}, u32[]{:S(2)}, u32[]{:S(2)}) collective-permute-start(bf16[1024,256]{1,0:T(8,128)(2,1)S(1)} %add.41.a_ref), channel_id=1, source_target_pairs={{8,16},{16,8},{9,17},{17,9},{10,18},{18,10},{11,19},{19,11},{12,20... | collective-permute-start | bytes 1572872 | tf_op jit(solution)/shard_map/ppermute | solution.py:376
  162.5 6.3 %collective-permute-start.7 = (bf16[1024,256]{1,0:T(8,128)(2,1)S(1)}, bf16[1024,256]{1,0:T(8,128)(2,1)S(1)}, u32[]{:S(2)}, u32[]{:S(2)}) collective-permute-start(bf16[1024,256]{1,0:T(8,128)(2,1)S(1)} %add.39.a_ref), channel_id=1, source_target_pairs={{8,16},{16,8},{9,17},{17,9},{10,18},{18,10},{11,19},{19,11},{12,20... | collective-permute-start | bytes 1572872 | tf_op jit(solution)/shard_map/ppermute | solution.py:376
  163.4 101.9 %collective-permute-start.1 = (bf16[768,512]{1,0:T(8,128)(2,1)S(1)}, bf16[768,512]{1,0:T(8,128)(2,1)S(1)}, u32[]{:S(2)}, u32[]{:S(2)}) collective-permute-start(bf16[768,512]{1,0:T(8,128)(2,1)S(1)} %add.35.a_ref), channel_id=1, source_target_pairs={{0,2},{2,0},{1,3},{3,1},{4,6},{6,4},{5,7},{7,5},{8,10},{10,8},{9,1... | collective-permute-start | bytes 2359304 | tf_op jit(solution)/shard_map/ppermute | solution.py:389
  165.1 5.2 %collective-permute-start.4 = (bf16[1024,256]{1,0:T(8,128)(2,1)S(1)}, bf16[1024,256]{1,0:T(8,128)(2,1)S(1)}, u32[]{:S(2)}, u32[]{:S(2)}) collective-permute-start(bf16[1024,256]{1,0:T(8,128)(2,1)S(1)} %add.37.a_ref), channel_id=1, source_target_pairs={{8,16},{16,8},{9,17},{17,9},{10,18},{18,10},{11,19},{19,11},{12,20... | collective-permute-start | bytes 1572872 | tf_op jit(solution)/shard_map/ppermute | solution.py:376
  165.9 75.5 %collective-permute-start.38 = (bf16[1024,256]{1,0:T(8,128)(2,1)S(1)}, bf16[1024,256]{1,0:T(8,128)(2,1)S(1)}, u32[]{:S(2)}, u32[]{:S(2)}) collective-permute-start(bf16[1024,256]{1,0:T(8,128)(2,1)S(1)} %add.60.final_ref), channel_id=1, source_target_pairs={{8,0},{16,24},{9,1},{17,25},{10,2},{18,26},{11,3},{19,27},{12,4},{... | collective-permute-start | bytes 1572872 | tf_op jit(solution)/shard_map/ppermute | solution.py:378
  167.4 85.2 %collective-permute-start.35 = (bf16[1024,256]{1,0:T(8,128)(2,1)S(1)}, bf16[1024,256]{1,0:T(8,128)(2,1)S(1)}, u32[]{:S(2)}, u32[]{:S(2)}) collective-permute-start(bf16[1024,256]{1,0:T(8,128)(2,1)S(1)} %add.58.final_ref), channel_id=1, source_target_pairs={{8,0},{16,24},{9,1},{17,25},{10,2},{18,26},{11,3},{19,27},{12,4},{... | collective-permute-start | bytes 1572872 | tf_op jit(solution)/shard_map/ppermute | solution.py:378
  168.8 95.0 %collective-permute-start.32 = (bf16[1024,256]{1,0:T(8,128)(2,1)S(1)}, bf16[1024,256]{1,0:T(8,128)(2,1)S(1)}, u32[]{:S(2)}, u32[]{:S(2)}) collective-permute-start(bf16[1024,256]{1,0:T(8,128)(2,1)S(1)} %add.56.final_ref), channel_id=1, source_target_pairs={{8,0},{16,24},{9,1},{17,25},{10,2},{18,26},{11,3},{19,27},{12,4},{... | collective-permute-start | bytes 1572872 | tf_op jit(solution)/shard_map/ppermute | solution.py:378
  170.2 107.5 %collective-permute-start.29 = (bf16[1024,256]{1,0:T(8,128)(2,1)S(1)}, bf16[1024,256]{1,0:T(8,128)(2,1)S(1)}, u32[]{:S(2)}, u32[]{:S(2)}) collective-permute-start(bf16[1024,256]{1,0:T(8,128)(2,1)S(1)} %add.54.final_ref), channel_id=1, source_target_pairs={{8,0},{16,24},{9,1},{17,25},{10,2},{18,26},{11,3},{19,27},{12,4},{... | collective-permute-start | bytes 1572872 | tf_op jit(solution)/shard_map/ppermute | solution.py:378
  241.4 47.6 %collective-permute-start.26 = (bf16[1024,256]{1,0:T(8,128)(2,1)S(1)}, bf16[1024,256]{1,0:T(8,128)(2,1)S(1)}, u32[]{:S(2)}, u32[]{:S(2)}) collective-permute-start(bf16[1024,256]{1,0:T(8,128)(2,1)S(1)} %add.52.final_ref), channel_id=1, source_target_pairs={{8,0},{16,24},{9,1},{17,25},{10,2},{18,26},{11,3},{19,27},{12,4},{... | collective-permute-start | bytes 1572872 | tf_op jit(solution)/shard_map/ppermute | solution.py:378
  252.6 47.6 %collective-permute-start.23 = (bf16[1024,256]{1,0:T(8,128)(2,1)S(1)}, bf16[1024,256]{1,0:T(8,128)(2,1)S(1)}, u32[]{:S(2)}, u32[]{:S(2)}) collective-permute-start(bf16[1024,256]{1,0:T(8,128)(2,1)S(1)} %add.50.final_ref), channel_id=1, source_target_pairs={{8,0},{16,24},{9,1},{17,25},{10,2},{18,26},{11,3},{19,27},{12,4},{... | collective-permute-start | bytes 1572872 | tf_op jit(solution)/shard_map/ppermute | solution.py:378
  263.8 47.6 %collective-permute-start.20 = (bf16[1024,256]{1,0:T(8,128)(2,1)S(1)}, bf16[1024,256]{1,0:T(8,128)(2,1)S(1)}, u32[]{:S(2)}, u32[]{:S(2)}) collective-permute-start(bf16[1024,256]{1,0:T(8,128)(2,1)S(1)} %add.48.final_ref), channel_id=1, source_target_pairs={{8,0},{16,24},{9,1},{17,25},{10,2},{18,26},{11,3},{19,27},{12,4},{... | collective-permute-start | bytes 1572872 | tf_op jit(solution)/shard_map/ppermute | solution.py:378
  265.3 57.4 %collective-permute-start.17 = (bf16[1024,256]{1,0:T(8,128)(2,1)S(1)}, bf16[1024,256]{1,0:T(8,128)(2,1)S(1)}, u32[]{:S(2)}, u32[]{:S(2)}) collective-permute-start(bf16[1024,256]{1,0:T(8,128)(2,1)S(1)} %add.46.final_ref), channel_id=1, source_target_pairs={{8,0},{16,24},{9,1},{17,25},{10,2},{18,26},{11,3},{19,27},{12,4},{... | collective-permute-start | bytes 1572872 | tf_op jit(solution)/shard_map/ppermute | solution.py:378
  277.8 88.5 %collective-permute-start.2 = (bf16[768,512]{1,0:T(8,128)(2,1)S(1)}, bf16[768,512]{1,0:T(8,128)(2,1)S(1)}, u32[]{:S(2)}, u32[]{:S(2)}) collective-permute-start(bf16[768,512]{1,0:T(8,128)(2,1)S(1)} %add.36.own_ref), channel_id=1, source_target_pairs={{0,1},{1,0},{2,3},{3,2},{4,5},{5,4},{6,7},{7,6},{8,9},{9,8},{10,11... | collective-permute-start | bytes 2359304 | tf_op jit(solution)/shard_map/ppermute | solution.py:391
  289.0 48.9 %collective-permute-start.14 = (bf16[1024,256]{1,0:T(8,128)(2,1)S(1)}, bf16[1024,256]{1,0:T(8,128)(2,1)S(1)}, u32[]{:S(2)}, u32[]{:S(2)}) collective-permute-start(bf16[1024,256]{1,0:T(8,128)(2,1)S(1)} %add.44.final_ref), channel_id=1, source_target_pairs={{8,0},{16,24},{9,1},{17,25},{10,2},{18,26},{11,3},{19,27},{12,4},{... | collective-permute-start | bytes 1572872 | tf_op jit(solution)/shard_map/ppermute | solution.py:378
  300.2 44.9 %collective-permute-start.11 = (bf16[1024,256]{1,0:T(8,128)(2,1)S(1)}, bf16[1024,256]{1,0:T(8,128)(2,1)S(1)}, u32[]{:S(2)}, u32[]{:S(2)}) collective-permute-start(bf16[1024,256]{1,0:T(8,128)(2,1)S(1)} %add.42.final_ref), channel_id=1, source_target_pairs={{8,0},{16,24},{9,1},{17,25},{10,2},{18,26},{11,3},{19,27},{12,4},{... | collective-permute-start | bytes 1572872 | tf_op jit(solution)/shard_map/ppermute | solution.py:378
  311.5 44.9 %collective-permute-start.8 = (bf16[1024,256]{1,0:T(8,128)(2,1)S(1)}, bf16[1024,256]{1,0:T(8,128)(2,1)S(1)}, u32[]{:S(2)}, u32[]{:S(2)}) collective-permute-start(bf16[1024,256]{1,0:T(8,128)(2,1)S(1)} %add.40.final_ref), channel_id=1, source_target_pairs={{8,0},{16,24},{9,1},{17,25},{10,2},{18,26},{11,3},{19,27},{12,4},{... | collective-permute-start | bytes 1572872 | tf_op jit(solution)/shard_map/ppermute | solution.py:378
  322.7 42.0 %collective-permute-start.5 = (bf16[1024,256]{1,0:T(8,128)(2,1)S(1)}, bf16[1024,256]{1,0:T(8,128)(2,1)S(1)}, u32[]{:S(2)}, u32[]{:S(2)}) collective-permute-start(bf16[1024,256]{1,0:T(8,128)(2,1)S(1)} %add.38.final_ref), channel_id=1, source_target_pairs={{8,0},{16,24},{9,1},{17,25},{10,2},{18,26},{11,3},{19,27},{12,4},{... | collective-permute-start | bytes 1572872 | tf_op jit(solution)/shard_map/ppermute | solution.py:378

commit v2 on v1

v2 whole, which is shorter than its diff:
```python
import functools

import jax
import jax.numpy as jnp
from jax import lax
from jax.experimental import pallas as pl
from jax.experimental.pallas import tpu as pltpu
from jax.sharding import PartitionSpec as P


BLOCK = 128
STRIP = 64
ROWS = 8
PIECES = 6
LAG = 4
MIB = 1 << 20


def on_end():
    plane = lax.axis_index("rep")
    return (plane == 0) | (plane == lax.axis_size("rep") - 1)


def on_second():
    return lax.axis_index("tp") % 2 == 1


def params(mib):
    return pltpu.CompilerParams(vmem_limit_bytes=mib * MIB)


def on_chip(x):
    return pltpu.with_memory_space_constraint(x, pltpu.VMEM)


def off_chip(x):
    return pltpu.with_memory_space_constraint(x, pltpu.HBM)


VMEM = pl.BlockSpec(memory_space=pltpu.VMEM)
HBM = pl.BlockSpec(memory_space=pltpu.HBM)
SMEM = pl.BlockSpec(memory_space=pltpu.SMEM)


def start_loads(index, sources, targets, sems):
    copies = []
    for k, (source, target) in enumerate(zip(sources, targets)):
        columns = slice(index * BLOCK, (index + 1) * BLOCK)
        copies.append(pltpu.make_async_copy(source.at[:, columns], target, sems.at[k]))
        copies[k].start()
    return copies


def turn_kernel(in_ref, gate_ref, up_ref, grad_ref, out_ref, gate_in, up_in, grad_in, sems):
    copies = start_loads(0, (gate_ref, up_ref, grad_ref), (gate_in, up_in, grad_in), sems)
    out_ref[...] = in_ref[...].T
    for copy in copies:
        copy.wait()


def turn(tokens, signals):
    length, features = tokens.shape
    return pl.pallas_call(
        turn_kernel,
        in_specs=[VMEM, HBM, HBM, HBM],
        out_specs=[VMEM] * 4,
        out_shape=[pltpu.VMEM((features, length), tokens.dtype)]
        + [pltpu.VMEM((length, BLOCK), tokens.dtype)] * 3,
        scratch_shapes=[pltpu.SemaphoreType.DMA((3,))],
        compiler_params=params(6),
        name="turn",
    )(off_chip(tokens), *(off_chip(x) for x in signals))


def block_kernel(
    index,
    last,
    aliased,
    tokens_ref,
    gate_pre_ref,
    up_pre_ref,
    grad_ref,
    gate_in,
    up_in,
    grad_in,
    gate_taps_ref,
    up_taps_ref,
    gate_bias_ref,
    up_bias_ref,
    *rest,
):
    gate_pad, up_pad, gate_delta, up_delta, back_ref, sems = rest[-6:]
    outs = rest[aliased:-6]
    top_ref, bottom_ref, extra_ref, gate_back_ref, up_back_ref = outs[:5]
    copies = []
    if not last:
        copies = start_loads(index + 1, (gate_pre_ref, up_pre_ref, grad_ref), outs[5:], sems)
    length, width = gate_in.shape
    taps = gate_taps_ref.shape[0]
    columns = slice(index * width, (index + 1) * width)
    lead = 8
    zeros = jnp.zeros((lead, width), jnp.float32)
    gate_pad[0:lead, :] = zeros
    up_pad[0:lead, :] = zeros
    gate_delta[length:, :] = zeros
    up_delta[length:, :] = zeros
    gate_pad[lead:, :] = gate_in[...].astype(jnp.float32)
    up_pad[lead:, :] = up_in[...].astype(jnp.float32)
    gate_w = [gate_taps_ref[k : k + 1, columns] for k in range(taps)]
    up_w = [up_taps_ref[k : k + 1, columns] for k in range(taps)]
    gate_b = gate_bias_ref[columns].reshape(1, width)
    up_b = up_bias_ref[columns].reshape(1, width)

    def fold(x):
        return jnp.sum(x.reshape(STRIP // 8, 8, width), axis=0)

    def strip(i, sums):
        base = pl.multiple_of(length - (i + 1) * STRIP, STRIP)
        first = lead - (taps - 1)
        gates = [gate_pad[pl.ds(base + first + k, STRIP), :] for k in range(taps)]
        ups = [up_pad[pl.ds(base + first + k, STRIP), :] for k in range(taps)]
        gate_mixed = gates[0] * gate_w[0]
        up_mixed = ups[0] * up_w[0]
        for k in range(1, taps):
            gate_mixed = gate_mixed + gates[k] * gate_w[k]
            up_mixed = up_mixed + ups[k] * up_w[k]
        gate_mixed = gate_mixed + gate_b
        up_mixed = up_mixed + up_b
        grad = grad_in[pl.ds(base, STRIP), :].astype(jnp.float32)
        s = jax.nn.sigmoid(gate_mixed)
        scaled = grad * s
        g_delta = scaled * up_mixed * (1.0 + gate_mixed * (1.0 - s))
        u_delta = scaled * gate_mixed
        gate_delta[pl.ds(base, STRIP), :] = g_delta
        up_delta[pl.ds(base, STRIP), :] = u_delta
        g_back = g_delta * gate_w[taps - 1]
        u_back = u_delta * up_w[taps - 1]
        for k in range(1, taps):
            g_back = g_back + gate_delta[pl.ds(base + k, STRIP), :] * gate_w[taps - 1 - k]
            u_back = u_back + up_delta[pl.ds(base + k, STRIP), :] * up_w[taps - 1 - k]
        back_ref[pl.ds(base, STRIP), 0:width] = g_back.astype(jnp.bfloat16)
        back_ref[pl.ds(base, STRIP), width:] = u_back.astype(jnp.bfloat16)
        terms = [fold(g_delta * gates[k]) for k in range(taps)]
        terms.append(fold(g_delta))
        terms.extend(fold(u_delta * ups[k]) for k in range(taps))
        terms.append(fold(u_delta))
        return tuple(a + b for a, b in zip(sums, terms))

    start = tuple(jnp.zeros((8, width), jnp.float32) for _ in range(2 * taps + 2))
    sums = lax.fori_loop(0, length // STRIP, strip, start)
    lines = [jnp.sum(x, axis=0, keepdims=True) for x in sums]
    pad = jnp.zeros((ROWS - taps - 1, width), jnp.float32)
    gate_rows = jnp.concatenate(lines[: taps + 1] + [pad], axis=0)
    up_rows = jnp.concatenate(lines[taps + 1 :] + [pad], axis=0)
    extra_ref[:, 0:width] = gate_rows
    extra_ref[:, width:] = up_rows
    begin = index * width % gate_back_ref.shape[1]
    gate_back_ref[:, begin : begin + width] = back_ref[:, 0:width]
    up_back_ref[:, begin : begin + width] = back_ref[:, width:]
    product = jnp.dot(
        tokens_ref[...], back_ref[...], preferred_element_type=jnp.float32
    ).astype(jnp.bfloat16)
    rows = top_ref.shape[0]
    top_ref[...] = product[:rows]
    bottom_ref[...] = product[rows:]
    for copy in copies:
        copy.wait()


def make_block(index, backs, tokens_t, signals, ready, taps, biases):
    length, hidden = signals[0].shape
    features = tokens_t.shape[0]
    last = (index + 1) * BLOCK == hidden
    back = pltpu.VMEM((length, max(hidden // PIECES, BLOCK)), jnp.bfloat16)
    half = pltpu.VMEM((features // 2, 2 * BLOCK), jnp.bfloat16)
    outs = [half, half, pltpu.VMEM((ROWS, 2 * BLOCK), jnp.float32), back, back]
    if not last:
        outs += [pltpu.VMEM((length, BLOCK), jnp.bfloat16)] * 3
    top, bottom, extra, *more = pl.pallas_call(
        functools.partial(block_kernel, index, last, len(backs)),
        in_specs=[VMEM] + [HBM] * 3 + [VMEM] * (7 + len(backs)),
        out_specs=[VMEM] * len(outs),
        out_shape=outs,
        scratch_shapes=[pltpu.VMEM((length + 8, BLOCK), jnp.float32)] * 4
        + [pltpu.VMEM((length, 2 * BLOCK), jnp.bfloat16), pltpu.SemaphoreType.DMA((3,))],
        input_output_aliases={11: 3, 12: 4} if backs else {},
        compiler_params=params(6),
        cost_estimate=pl.CostEstimate(
            flops=2 * features * length * 2 * BLOCK + 60 * length * BLOCK,
            bytes_accessed=6 * length * BLOCK,
            transcendentals=length * BLOCK,
        ),
        name="block",
    )(
        on_chip(tokens_t),
        *(off_chip(x) for x in signals),
        *(on_chip(x) for x in ready),
        *taps,
        *biases,
        *(on_chip(x) for x in backs),
    )
    return (top, bottom), extra, more[:2], more[2:]


def add_kernel(a_ref, b_ref, out_ref):
    out_ref[...] = (a_ref[...].astype(jnp.float32) + b_ref[...].astype(jnp.float32)).astype(out_ref.dtype)


def add_chunk(a, b):
    return pl.pallas_call(
        add_kernel,
        out_shape=pltpu.VMEM(a.shape, a.dtype),
        compiler_params=params(4),
        cost_estimate=pl.CostEstimate(flops=a.size, bytes_accessed=6 * a.size, transcendentals=0),
        name="add",
    )(on_chip(a), on_chip(b))


def turn_around_kernel(pair_ref, other_ref, *refs):
    out_ref = refs[-1]
    end = on_end()

    @pl.when(jnp.logical_not(end))
    def _():
        add_kernel(pair_ref, other_ref, out_ref)

    @pl.when(end)
    def _():
        out_ref[...] = refs[0][...]


def turn_around(pair, other, following):
    return pl.pallas_call(
        turn_around_kernel,
        in_specs=[VMEM, VMEM, VMEM],
        out_specs=VMEM,
        out_shape=pltpu.VMEM(pair.shape, pair.dtype),
        compiler_params=params(4),
        cost_estimate=pl.CostEstimate(flops=pair.size, bytes_accessed=6 * pair.size, transcendentals=0),
        name="around",
    )(on_chip(pair), on_chip(other), on_chip(following))


def store_kernel(blocks, *refs):
    halves = 2 * blocks
    gate_ref, up_ref = refs[-2:]
    rows = refs[0].shape[0]
    end = on_end()

    def write(sources):
        for i, source in enumerate(sources):
            piece = source[...].astype(jnp.float32)
            down = slice(i % 2 * rows, (i % 2 + 1) * rows)
            across = slice(i // 2 * BLOCK, (i // 2 + 1) * BLOCK)
            gate_ref[down, across] = piece[:, :BLOCK]
            up_ref[down, across] = piece[:, BLOCK:]

    @pl.when(end)
    def _():
        write(refs[:halves])

    @pl.when(jnp.logical_not(end))
    def _():
        write(refs[halves : 2 * halves])


def store_blocks(first, blocks, shape, came, sums, outs):
    rows = came[0].shape[0]
    whole = pl.BlockSpec((rows, 2 * BLOCK), lambda i: (0, 0))
    block = pl.BlockSpec((2 * rows, blocks * BLOCK), lambda i: (0, first // blocks))
    grad = pltpu.HBM(shape, jnp.float32)
    count = 4 * blocks
    return pl.pallas_call(
        functools.partial(store_kernel, blocks),
        grid=(1,),
        in_specs=[whole] * count + [HBM] * len(outs),
        out_specs=[block, block],
        out_shape=[grad, grad],
        input_output_aliases={count: 0, count + 1: 1} if outs else {},
        compiler_params=params(14),
        cost_estimate=pl.CostEstimate(
            flops=count * rows * BLOCK, bytes_accessed=8 * count * rows * BLOCK, transcendentals=0
        ),
        name="store",
    )(*(on_chip(x) for x in came), *(on_chip(x) for x in sums), *(off_chip(x) for x in outs))


def gather_kernel(*refs):
    out_ref = refs[-1]
    count = len(refs) - 1
    for j in range(count):
        x = refs[j][...].astype(out_ref.dtype)
        out_ref[:, j * BLOCK : (j + 1) * BLOCK] = x[:, :BLOCK]
        out_ref[:, (count + j) * BLOCK : (count + j + 1) * BLOCK] = x[:, BLOCK:]


def gather(extras):
    return pl.pallas_call(
        gather_kernel,
        out_shape=pltpu.VMEM((ROWS, len(extras) * 2 * BLOCK), jnp.bfloat16),
        compiler_params=params(2),
        name="gather",
    )(*(on_chip(x) for x in extras))


def small_kernel(got_ref, final_ref, *refs):
    hidden = refs[0].shape[1]
    taps = refs[0].shape[0]
    is_end = jnp.full(got_ref.shape, on_end().astype(jnp.int32)) == 1
    x = jnp.where(is_end, got_ref[...].astype(jnp.float32), final_ref[...].astype(jnp.float32))
    refs[0][...] = x[:taps, :hidden]
    refs[1][...] = x[:taps, hidden:]
    refs[2][...] = x[taps, :hidden]
    refs[3][...] = x[taps, hidden:]


def small_outs(got, final, taps):
    hidden = got.shape[1] // 2
    shapes = [(taps, hidden), (taps, hidden), (hidden,), (hidden,)]
    return pl.pallas_call(
        small_kernel,
        in_specs=[VMEM, VMEM],
        out_specs=[VMEM] * 4,
        out_shape=[jax.ShapeDtypeStruct(x, jnp.float32) for x in shapes],
        compiler_params=params(2),
        name="small",
    )(on_chip(got), on_chip(final))


def feature_kernel(piece, *refs):
    gate_back_ref, up_back_ref, gate_ref, up_ref = refs[:4]
    width = gate_back_ref.shape[1]
    columns = slice(piece * width, (piece + 1) * width)
    dims = (((1,), (1,)), ((), ()))
    term = lax.dot_general(
        gate_back_ref[...], gate_ref[:, columns], dims, preferred_element_type=jnp.float32
    ) + lax.dot_general(up_back_ref[...], up_ref[:, columns], dims, preferred_element_type=jnp.float32)
    if piece > 0:
        term = term + refs[4][...]
    if piece < PIECES - 1:
        refs[-1][...] = term
        return
    send_ref, keep_ref = refs[-2:]
    half = send_ref.shape[1]
    low = term[:, :half].astype(send_ref.dtype)
    high = term[:, half:].astype(send_ref.dtype)
    second = on_second()

    @pl.when(second)
    def _():
        send_ref[...] = low
        keep_ref[...] = high

    @pl.when(jnp.logical_not(second))
    def _():
        send_ref[...] = high
        keep_ref[...] = low


def feature_piece(piece, gate_back, up_back, gate_weight, up_weight, total):
    length, width = gate_back.shape
    features = gate_weight.shape[0]
    last = piece == PIECES - 1
    if last:
        outs = [pltpu.VMEM((length, features // 2), jnp.bfloat16)] * 2
    else:
        outs = [pltpu.VMEM((length, features), jnp.float32)]
    return pl.pallas_call(
        functools.partial(feature_kernel, piece),
        in_specs=[VMEM] * (4 + len(total)),
        out_specs=[VMEM] * len(outs),
        out_shape=outs,
        input_output_aliases={4: 0} if total and not last else {},
        compiler_params=params(8),
        cost_estimate=pl.CostEstimate(
            flops=4 * length * width * features, bytes_accessed=4 * width * features, transcendentals=0
        ),
        name="feature",
    )(*(on_chip(x) for x in (gate_back, up_back, gate_weight, up_weight, *total)))


def join_kernel(own_ref, other_ref, out_ref):
    half = own_ref.shape[1]
    second = on_second()

    @pl.when(second)
    def _():
        out_ref[:, half:] = own_ref[...]
        out_ref[:, :half] = other_ref[...]

    @pl.when(jnp.logical_not(second))
    def _():
        out_ref[:, :half] = own_ref[...]
        out_ref[:, half:] = other_ref[...]


def join(own, other):
    return pl.pallas_call(
        join_kernel,
        in_specs=[VMEM, VMEM],
        out_specs=VMEM,
        out_shape=jax.ShapeDtypeStruct((own.shape[0], 2 * own.shape[1]), own.dtype),
        compiler_params=params(8),
        name="join",
    )(on_chip(own), on_chip(other))


INWARD = [(0, 1), (3, 2)]
OUTWARD = [(1, 0), (2, 3)]
MIDDLE = [(1, 2), (2, 1)]


def line_chunk(part, add):
    got = lax.ppermute(part, "rep", INWARD)
    pair = add(part, got)
    other = lax.ppermute(pair, "rep", MIDDLE)
    final = add(pair, other)
    got = lax.ppermute(final, "rep", OUTWARD)
    return got, final


def line_sums(parts):
    count = len(parts)
    sums, came = [], []
    for j in range(count + LAG):
        if j < LAG:
            send, pairs = parts[j], INWARD
        else:
            send, pairs = sums[j - LAG], INWARD + OUTWARD
        got = lax.ppermute(send, "rep", pairs)
        came.append(got)
        if j < count:
            pair = add_chunk(parts[j], got)
            other = lax.ppermute(pair, "rep", MIDDLE)
            sums.append(turn_around(pair, other, parts[min(j + LAG, count - 1)]))
    return came[LAG:], sums


def store_groups(blocks):
    if blocks % 2:
        return [(j, 1) for j in range(blocks)]
    return [(j, 2) for j in range(0, blocks - 2, 2)] + [(blocks - 2, 1), (blocks - 1, 1)]


NEAR = [(0, 1), (1, 0), (2, 3), (3, 2)]
FAR = [(0, 2), (2, 0), (1, 3), (3, 1)]


def sum_over_four(send, keep):
    got = lax.ppermute(send, "tp", NEAR)
    own = add_chunk(keep, got)
    got = lax.ppermute(own, "tp", FAR)
    own = add_chunk(own, got)
    other = lax.ppermute(own, "tp", NEAR)
    return join(own, other)


def per_device(
    tokens,
    gate_pre,
    up_pre,
    hidden_grad,
    gate_weight,
    up_weight,
    gate_taps,
    up_taps,
    gate_bias,
    up_bias,
):
    taps, hidden = gate_taps.shape
    count = hidden // BLOCK
    per = max(count // PIECES, 1)
    signals = (gate_pre, up_pre, hidden_grad)
    tokens_t, *ready = turn(tokens, signals)
    chunks, extras, backs, backs_at = [], [], (), []
    for j in range(count):
        pair, extra, backs, ready = make_block(
            j, backs, tokens_t, signals, ready, (gate_taps, up_taps), (gate_bias, up_bias)
        )
        chunks.extend(pair)
        extras.append(extra)
        if (j + 1) % per == 0:
            backs_at.append(backs)
            backs = ()
    extra = gather(extras)
    if lax.axis_size("rep") == 4 and lax.axis_size("tp") == 4 and count % PIECES == 0:
        total = ()
        for piece in range(PIECES):
            total = feature_piece(piece, *backs_at[piece], gate_weight, up_weight, total)
        result = sum_over_four(*total)
        came, sums = line_sums(chunks)
        outs = ()
        for first, size in store_groups(count):
            mine = slice(2 * first, 2 * (first + size))
            outs = store_blocks(first, size, gate_weight.shape, came[mine], sums[mine], outs)
        gate, up = outs
        got, final = line_chunk(extra, add_chunk)
    else:
        dims = (((1,), (1,)), ((), ()))
        gate_back, up_back = (jnp.concatenate([b[k] for b in backs_at], axis=1) for k in range(2))
        partial = lax.dot_general(
            gate_back, gate_weight, dims, preferred_element_type=jnp.float32
        ) + lax.dot_general(up_back, up_weight, dims, preferred_element_type=jnp.float32)
        own = lax.psum_scatter(partial.astype(jnp.bfloat16), "tp", scatter_dimension=1, tiled=True)
        result = lax.all_gather(own, "tp", axis=1, tiled=True)
        sums = [lax.psum(c, "rep") for c in chunks]
        gate, up = (
            jnp.concatenate(
                [jnp.concatenate([c[:, k * BLOCK : (k + 1) * BLOCK] for c in sums[h::2]], axis=1) for h in range(2)],
                axis=0,
            ).astype(jnp.float32)
            for k in range(2)
        )
        got = final = lax.psum(extra, "rep")
    gate_taps_grad, up_taps_grad, gate_bias_grad, up_bias_grad = small_outs(got, final, taps)
    return (
        result,
        gate,
        up,
        gate_taps_grad,
        up_taps_grad,
        gate_bias_grad,
        up_bias_grad,
    )


def solution(mesh):
    return jax.shard_map(
        per_device,
        mesh=mesh,
        in_specs=(
            P("rep", "fs"),
            P("rep", "tp"),
            P("rep", "tp"),
            P("rep", "tp"),
            P("fs", "tp"),
            P("fs", "tp"),
            P(None, "tp"),
            P(None, "tp"),
            P("tp"),
            P("tp"),
        ),
        out_specs=(
            P("rep", "fs"),
            P("fs", "tp"),
            P("fs", "tp"),
            P(None, "tp"),
            P(None, "tp"),
            P("tp"),
            P("tp"),
        ),
        check_vma=False,
    )
```

time: 369 us -> 205 us (0.56)
  waiting for transfers between devices: 251 us -> 57.1 us
  starting transfers between devices: 57.8 us -> 103 us
  Pallas kernels: 58.1 us -> 42.2 us
    ppermute x13 -> x1, waiting for transfers between devices: 173 us -> 0.01 us  [line_chunk(): got = lax.ppermute(final, 'rep', OUTWARD)]
    ppermute x0 -> x52, starting transfers between devices: none -> 92.9 us  [the longest x28 76.5 us: line_sums(): got = lax.ppermute(send, 'rep', pairs)]
    ppermute x13 -> x1, waiting for transfers between devices: 77.9 us -> 0.01 us  [line_chunk(): got = lax.ppermute(part, 'rep', INWARD)]
    ppermute x0 -> x52, waiting for transfers between devices: none -> 57.1 us  [the longest x28 57 us: line_sums(): got = lax.ppermute(send, 'rep', pairs)]
    ppermute x13 -> x1, starting transfers between devices: 30.6 us -> 6.09 us  [line_chunk(): got = lax.ppermute(part, 'rep', INWARD)]
    ppermute x13 -> x1, starting transfers between devices: 16.7 us -> 1.29 us  [line_chunk(): got = lax.ppermute(final, 'rep', OUTWARD)]
    pallas_call x30 -> x52, Pallas kernels: 54.6 us -> 40.3 us  [the longest x12 19.3 us: make_block(): pl.pallas_call(functools.partial(block_kernel, index, last, len(backs)),...]
    ppermute x13 -> x1, starting transfers between devices: 8.95 us -> 0.66 us  [line_chunk(): other = lax.ppermute(pair, 'rep', MIDDLE)]
  transfers between devices with their start and end apart: 42 -> 58, of which waited for: 20 -> 20; matrix products, arithmetic and copies ran while one was open for 0% -> 0% of each run, Pallas kernels for 14% -> 18%
where the time goes in v2:
time: 205 us; the launch traced here: 204 us
  starting transfers between devices  103 us (50%)
  waiting for transfers between devices  57.1 us (28%)
  Pallas kernels  42.2 us (21%)
    ppermute x28, starting transfers between devices, line_sums(): got = lax.ppermute(send, 'rep', pairs)  76.5 us
    ppermute x28, waiting for transfers between devices, line_sums(): got = lax.ppermute(send, 'rep', pairs)  57 us
    pallas_call x12, Pallas kernels, make_block(): pl.pallas_call(functools.partial(block_kernel, index, last, len(backs)),...  19.3 us
    ppermute x24, starting transfers between devices, line_sums(): other = lax.ppermute(pair, 'rep', MIDDLE)  16.4 us
    pallas_call x7, Pallas kernels, store_blocks(): pl.pallas_call(functools.partial(store_kernel, blocks), grid=(1,), in_spe...  9.5 us
    pallas_call x6, Pallas kernels, feature_piece(): pl.pallas_call(functools.partial(feature_kernel, piece), in_specs=[VMEM]...  6.41 us
    ppermute x1, starting transfers between devices, line_chunk(): got = lax.ppermute(part, 'rep', INWARD)  6.09 us
  transfers between devices with their start and end apart: 58, of which 20 were waited for; matrix products, arithmetic and copies ran while one was open for 0% of the time, Pallas kernels for 18%

profile of v2, /device:TPU:0, one launch (start us, length us, event | category | flops | bytes accessed | tf_op | source)
XLA Modules:
  0.0 203.6 jit_solution(12655713492362084022)
XLA Ops:
  0.7 2.6 %turn.1 = (bf16[1024,768]{1,0:T(8,128)(2,1)S(1)}, bf16[768,128]{1,0:T(8,128)(2,1)S(1)}, bf16[768,128]{1,0:T(8,128)(2,1)S(1)}, bf16[768,128]{1,0:T(8,128)(2,1)S(1)}) custom-call(bf16[768,1024]{1,0:T(8,128)(2,1)} %in_ref.1, bf16[768,1536]{1,0:T(8,128)(2,1)} %gate_pre_ref.23, bf16[768,1536]{1,0:T(8,128)(2,1)} %up_pre_ref.23, bf16[768,1536]{1,0:T(8,128)(2,1)} %grad_ref.25), custom_call_target="tpu_custom_call" | custom-call | tf_op jit(solution)/shard_map/turn/pallas_call | solution.py:63
  3.3 1.6 block.12
  4.9 5.0 %collective-permute-start.29 = (bf16[512,256]{1,0:T(8,128)(2,1)S(1)}, bf16[512,256]{1,0:T(8,128)(2,1)S(1)}, u32[]{:S(2)}, u32[]{:S(2)}) collective-permute-start(bf16[512,256]{1,0:T(8,128)(2,1)S(1)} %get-tuple-element.204.a_ref), channel_id=1, source_target_pairs={{0,8},{24,16},{1,9},{25,17},{2,10},{26,18},{3,11},{27,19},{4,12},{... | collective-permute-start | bytes 786440 | tf_op jit(solution)/shard_map/ppermute | solution.py:430
  9.9 1.3 collective-permute-start.42
  11.2 1.6 block.13
  12.8 1.3 collective-permute-start.16
  14.1 1.3 collective-permute-start.3
  15.5 1.1 collective-permute-done.29.b_ref
  17.3 4.9 %collective-permute-done.42.b_ref = bf16[512,256]{1,0:T(8,128)(2,1)S(1)} collective-permute-done((bf16[512,256]{1,0:T(8,128)(2,1)S(1)}, bf16[512,256]{1,0:T(8,128)(2,1)S(1)}, u32[]{:S(2)}, u32[]{:S(2)}) %collective-permute-start.42) | collective-permute-done | bytes 262176 | tf_op jit(solution)/shard_map/ppermute | solution.py:430
  22.9 1.6 block.14
  24.5 1.6 block.15
  26.2 1.6 collective-permute-done.16.b_ref
  28.5 3.7 %collective-permute-done.3.b_ref = bf16[512,256]{1,0:T(8,128)(2,1)S(1)} collective-permute-done((bf16[512,256]{1,0:T(8,128)(2,1)S(1)}, bf16[512,256]{1,0:T(8,128)(2,1)S(1)}, u32[]{:S(2)}, u32[]{:S(2)}) %collective-permute-start.3) | collective-permute-done | bytes 262176 | tf_op jit(solution)/shard_map/ppermute | solution.py:430
  33.0 1.6 block.16
  34.7 1.6 block.17
  36.3 1.6 block.18
  37.9 1.6 block.19
  39.6 5.4 %collective-permute-start.31 = (bf16[512,256]{1,0:T(8,128)(2,1)S(1)}, bf16[512,256]{1,0:T(8,128)(2,1)S(1)}, u32[]{:S(2)}, u32[]{:S(2)}) collective-permute-start(bf16[512,256]{1,0:T(8,128)(2,1)S(1)} %around.36.refs_4_), channel_id=1, source_target_pairs={{0,8},{24,16},{8,0},{16,24},{1,9},{25,17},{9,1},{17,25},{2,10},{26... | collective-permute-start | bytes 786440 | tf_op jit(solution)/shard_map/ppermute | solution.py:430
  45.1 1.6 block.20
  46.7 1.6 block.21
  48.4 1.6 block.22
  50.0 2.1 %collective-permute-start.18 = (bf16[512,256]{1,0:T(8,128)(2,1)S(1)}, bf16[512,256]{1,0:T(8,128)(2,1)S(1)}, u32[]{:S(2)}, u32[]{:S(2)}) collective-permute-start(bf16[512,256]{1,0:T(8,128)(2,1)S(1)} %around.30.refs_7_), channel_id=1, source_target_pairs={{0,8},{24,16},{8,0},{16,24},{1,9},{25,17},{9,1},{17,25},{2,10},{26... | collective-permute-start | bytes 786440 | tf_op jit(solution)/shard_map/ppermute | solution.py:430
  54.4 3.4 %collective-permute-done.44.b_ref.refs_1_ = bf16[512,256]{1,0:T(8,128)(2,1)S(1)} collective-permute-done((bf16[512,256]{1,0:T(8,128)(2,1)S(1)}, bf16[512,256]{1,0:T(8,128)(2,1)S(1)}, u32[]{:S(2)}, u32[]{:S(2)}) %collective-permute-start.44) | collective-permute-done | bytes 262176 | tf_op jit(solution)/shard_map/ppermute | solution.py:430
  59.4 1.6 block.23
  62.1 1.3 collective-permute-done.18.b_ref.refs_3_
  64.1 2.9 %collective-permute-done.5.b_ref.refs_2_ = bf16[512,256]{1,0:T(8,128)(2,1)S(1)} collective-permute-done((bf16[512,256]{1,0:T(8,128)(2,1)S(1)}, bf16[512,256]{1,0:T(8,128)(2,1)S(1)}, u32[]{:S(2)}, u32[]{:S(2)}) %collective-permute-start.5) | collective-permute-done | bytes 262176 | tf_op jit(solution)/shard_map/ppermute | solution.py:430
  69.9 7.0 %collective-permute-start.46 = (bf16[512,256]{1,0:T(8,128)(2,1)S(1)}, bf16[512,256]{1,0:T(8,128)(2,1)S(1)}, u32[]{:S(2)}, u32[]{:S(2)}) collective-permute-start(bf16[512,256]{1,0:T(8,128)(2,1)S(1)} %around.43.refs_5_), channel_id=1, source_target_pairs={{0,8},{24,16},{8,0},{16,24},{1,9},{25,17},{9,1},{17,25},{2,10},{26... | collective-permute-start | bytes 786440 | tf_op jit(solution)/shard_map/ppermute | solution.py:430
  77.1 1.2 feature.11
  78.4 2.1 %collective-permute-start.20 = (bf16[512,256]{1,0:T(8,128)(2,1)S(1)}, bf16[512,256]{1,0:T(8,128)(2,1)S(1)}, u32[]{:S(2)}, u32[]{:S(2)}) collective-permute-start(bf16[512,256]{1,0:T(8,128)(2,1)S(1)} %around.31.refs_7_), channel_id=1, source_target_pairs={{0,8},{24,16},{8,0},{16,24},{1,9},{25,17},{9,1},{17,25},{2,10},{26... | collective-permute-start | bytes 786440 | tf_op jit(solution)/shard_map/ppermute | solution.py:430
  80.5 2.0 collective-permute-start.7
  83.2 3.1 %collective-permute-done.33.b_ref.refs_0_ = bf16[512,256]{1,0:T(8,128)(2,1)S(1)} collective-permute-done((bf16[512,256]{1,0:T(8,128)(2,1)S(1)}, bf16[512,256]{1,0:T(8,128)(2,1)S(1)}, u32[]{:S(2)}, u32[]{:S(2)}) %collective-permute-start.33) | collective-permute-done | bytes 262176 | tf_op jit(solution)/shard_map/ppermute | solution.py:430
  87.1 4.9 %collective-permute-done.20.b_ref.refs_3_ = bf16[512,256]{1,0:T(8,128)(2,1)S(1)} collective-permute-done((bf16[512,256]{1,0:T(8,128)(2,1)S(1)}, bf16[512,256]{1,0:T(8,128)(2,1)S(1)}, u32[]{:S(2)}, u32[]{:S(2)}) %collective-permute-start.20) | collective-permute-done | bytes 262176 | tf_op jit(solution)/shard_map/ppermute | solution.py:430
  92.7 2.6 %collective-permute-done.7.b_ref.refs_2_ = bf16[512,256]{1,0:T(8,128)(2,1)S(1)} collective-permute-done((bf16[512,256]{1,0:T(8,128)(2,1)S(1)}, bf16[512,256]{1,0:T(8,128)(2,1)S(1)}, u32[]{:S(2)}, u32[]{:S(2)}) %collective-permute-start.7) | collective-permute-done | bytes 262176 | tf_op jit(solution)/shard_map/ppermute | solution.py:430
  96.1 4.3 %collective-permute-start.48 = (bf16[512,256]{1,0:T(8,128)(2,1)S(1)}, bf16[512,256]{1,0:T(8,128)(2,1)S(1)}, u32[]{:S(2)}, u32[]{:S(2)}) collective-permute-start(bf16[512,256]{1,0:T(8,128)(2,1)S(1)} %around.44.refs_5_), channel_id=1, source_target_pairs={{0,8},{24,16},{8,0},{16,24},{1,9},{25,17},{9,1},{17,25},{2,10},{26... | collective-permute-start | bytes 786440 | tf_op jit(solution)/shard_map/ppermute | solution.py:430
  100.6 5.1 %collective-permute-start.22 = (bf16[512,256]{1,0:T(8,128)(2,1)S(1)}, bf16[512,256]{1,0:T(8,128)(2,1)S(1)}, u32[]{:S(2)}, u32[]{:S(2)}) collective-permute-start(bf16[512,256]{1,0:T(8,128)(2,1)S(1)} %around.32.refs_7_), channel_id=1, source_target_pairs={{0,8},{24,16},{8,0},{16,24},{1,9},{25,17},{9,1},{17,25},{2,10},{26... | collective-permute-start | bytes 786440 | tf_op jit(solution)/shard_map/ppermute | solution.py:430
  105.8 3.8 %collective-permute-start.9 = (bf16[512,256]{1,0:T(8,128)(2,1)S(1)}, bf16[512,256]{1,0:T(8,128)(2,1)S(1)}, u32[]{:S(2)}, u32[]{:S(2)}) collective-permute-start(bf16[512,256]{1,0:T(8,128)(2,1)S(1)} %around.26.refs_6_), channel_id=1, source_target_pairs={{0,8},{24,16},{8,0},{16,24},{1,9},{25,17},{9,1},{17,25},{2,10},{26... | collective-permute-start | bytes 786440 | tf_op jit(solution)/shard_map/ppermute | solution.py:430
  110.4 2.8 %collective-permute-done.35.b_ref.refs_0_ = bf16[512,256]{1,0:T(8,128)(2,1)S(1)} collective-permute-done((bf16[512,256]{1,0:T(8,128)(2,1)S(1)}, bf16[512,256]{1,0:T(8,128)(2,1)S(1)}, u32[]{:S(2)}, u32[]{:S(2)}) %collective-permute-start.35) | collective-permute-done | bytes 262176 | tf_op jit(solution)/shard_map/ppermute | solution.py:430
  114.2 1.6 collective-permute-start.1
  115.7 2.0 collective-permute-done.22.b_ref.refs_3_
  118.4 2.1 %collective-permute-done.9.b_ref.refs_2_ = bf16[512,256]{1,0:T(8,128)(2,1)S(1)} collective-permute-done((bf16[512,256]{1,0:T(8,128)(2,1)S(1)}, bf16[512,256]{1,0:T(8,128)(2,1)S(1)}, u32[]{:S(2)}, u32[]{:S(2)}) %collective-permute-start.9) | collective-permute-done | bytes 262176 | tf_op jit(solution)/shard_map/ppermute | solution.py:430
  121.3 4.9 %collective-permute-start.50 = (bf16[512,256]{1,0:T(8,128)(2,1)S(1)}, bf16[512,256]{1,0:T(8,128)(2,1)S(1)}, u32[]{:S(2)}, u32[]{:S(2)}) collective-permute-start(bf16[512,256]{1,0:T(8,128)(2,1)S(1)} %around.45.refs_5_), channel_id=1, source_target_pairs={{0,8},{24,16},{8,0},{16,24},{1,9},{25,17},{9,1},{17,25},{2,10},{26... | collective-permute-start | bytes 786440 | tf_op jit(solution)/shard_map/ppermute | solution.py:430
  126.6 5.6 %collective-permute-start.24 = (bf16[512,256]{1,0:T(8,128)(2,1)S(1)}, bf16[512,256]{1,0:T(8,128)(2,1)S(1)}, u32[]{:S(2)}, u32[]{:S(2)}) collective-permute-start(bf16[512,256]{1,0:T(8,128)(2,1)S(1)} %around.33.refs_7_), channel_id=1, source_target_pairs={{0,8},{24,16},{8,0},{16,24},{1,9},{25,17},{9,1},{17,25},{2,10},{26... | collective-permute-start | bytes 786440 | tf_op jit(solution)/shard_map/ppermute | solution.py:430
  132.2 3.0 %collective-permute-start.11 = (bf16[512,256]{1,0:T(8,128)(2,1)S(1)}, bf16[512,256]{1,0:T(8,128)(2,1)S(1)}, u32[]{:S(2)}, u32[]{:S(2)}) collective-permute-start(bf16[512,256]{1,0:T(8,128)(2,1)S(1)} %around.27.refs_6_), channel_id=1, source_target_pairs={{0,8},{24,16},{8,0},{16,24},{1,9},{25,17},{9,1},{17,25},{2,10},{26... | collective-permute-start | bytes 786440 | tf_op jit(solution)/shard_map/ppermute | solution.py:430
  135.9 3.0 %collective-permute-done.37.b_ref.refs_0_ = bf16[512,256]{1,0:T(8,128)(2,1)S(1)} collective-permute-done((bf16[512,256]{1,0:T(8,128)(2,1)S(1)}, bf16[512,256]{1,0:T(8,128)(2,1)S(1)}, u32[]{:S(2)}, u32[]{:S(2)}) %collective-permute-start.37) | collective-permute-done | bytes 262176 | tf_op jit(solution)/shard_map/ppermute | solution.py:430
  139.7 2.9 %collective-permute-done.24.b_ref.refs_3_ = bf16[512,256]{1,0:T(8,128)(2,1)S(1)} collective-permute-done((bf16[512,256]{1,0:T(8,128)(2,1)S(1)}, bf16[512,256]{1,0:T(8,128)(2,1)S(1)}, u32[]{:S(2)}, u32[]{:S(2)}) %collective-permute-start.24) | collective-permute-done | bytes 262176 | tf_op jit(solution)/shard_map/ppermute | solution.py:430
  143.4 2.1 %collective-permute-done.11.b_ref.refs_2_ = bf16[512,256]{1,0:T(8,128)(2,1)S(1)} collective-permute-done((bf16[512,256]{1,0:T(8,128)(2,1)S(1)}, bf16[512,256]{1,0:T(8,128)(2,1)S(1)}, u32[]{:S(2)}, u32[]{:S(2)}) %collective-permute-start.11) | collective-permute-done | bytes 262176 | tf_op jit(solution)/shard_map/ppermute | solution.py:430
  146.2 6.1 %collective-permute-start.55 = (bf16[8,3072]{1,0:T(8,128)(2,1)S(1)}, bf16[8,3072]{1,0:T(8,128)(2,1)S(1)}, u32[]{:S(2)}, u32[]{:S(2)}) collective-permute-start(bf16[8,3072]{1,0:T(8,128)(2,1)S(1)} %gather.1.a_ref), channel_id=1, source_target_pairs={{0,8},{24,16},{1,9},{25,17},{2,10},{26,18},{3,11},{27,19},{4,12},{... | collective-permute-start | bytes 147464 | tf_op jit(solution)/shard_map/ppermute | solution.py:414
  152.5 2.1 %collective-permute-start.39 = (bf16[512,256]{1,0:T(8,128)(2,1)S(1)}, bf16[512,256]{1,0:T(8,128)(2,1)S(1)}, u32[]{:S(2)}, u32[]{:S(2)}) collective-permute-start(bf16[512,256]{1,0:T(8,128)(2,1)S(1)} %around.40.refs_4_), channel_id=1, source_target_pairs={{0,8},{24,16},{8,0},{16,24},{1,9},{25,17},{9,1},{17,25},{2,10},{26... | collective-permute-start | bytes 786440 | tf_op jit(solution)/shard_map/ppermute | solution.py:430
  154.9 4.8 %collective-permute-start.26 = (bf16[512,256]{1,0:T(8,128)(2,1)S(1)}, bf16[512,256]{1,0:T(8,128)(2,1)S(1)}, u32[]{:S(2)}, u32[]{:S(2)}) collective-permute-start(bf16[512,256]{1,0:T(8,128)(2,1)S(1)} %around.34.refs_7_), channel_id=1, source_target_pairs={{0,8},{24,16},{8,0},{16,24},{1,9},{25,17},{9,1},{17,25},{2,10},{26... | collective-permute-start | bytes 786440 | tf_op jit(solution)/shard_map/ppermute | solution.py:430
  160.7 4.1 %collective-permute-done.39.b_ref.refs_0_ = bf16[512,256]{1,0:T(8,128)(2,1)S(1)} collective-permute-done((bf16[512,256]{1,0:T(8,128)(2,1)S(1)}, bf16[512,256]{1,0:T(8,128)(2,1)S(1)}, u32[]{:S(2)}, u32[]{:S(2)}) %collective-permute-start.39) | collective-permute-done | bytes 262176 | tf_op jit(solution)/shard_map/ppermute | solution.py:430
  165.5 4.5 %collective-permute-done.26.b_ref.refs_3_ = bf16[512,256]{1,0:T(8,128)(2,1)S(1)} collective-permute-done((bf16[512,256]{1,0:T(8,128)(2,1)S(1)}, bf16[512,256]{1,0:T(8,128)(2,1)S(1)}, u32[]{:S(2)}, u32[]{:S(2)}) %collective-permute-start.26) | collective-permute-done | bytes 262176 | tf_op jit(solution)/shard_map/ppermute | solution.py:430
  170.8 2.1 %collective-permute-done.13.b_ref.refs_2_ = bf16[512,256]{1,0:T(8,128)(2,1)S(1)} collective-permute-done((bf16[512,256]{1,0:T(8,128)(2,1)S(1)}, bf16[512,256]{1,0:T(8,128)(2,1)S(1)}, u32[]{:S(2)}, u32[]{:S(2)}) %collective-permute-start.13) | collective-permute-done | bytes 262176 | tf_op jit(solution)/shard_map/ppermute | solution.py:430
  174.3 1.3 collective-permute-start.57
  175.7 5.8 %collective-permute-start.54 = (bf16[512,256]{1,0:T(8,128)(2,1)S(1)}, bf16[512,256]{1,0:T(8,128)(2,1)S(1)}, u32[]{:S(2)}, u32[]{:S(2)}) collective-permute-start(bf16[512,256]{1,0:T(8,128)(2,1)S(1)} %around.47.refs_3_), channel_id=1, source_target_pairs={{0,8},{24,16},{8,0},{16,24},{1,9},{25,17},{9,1},{17,25},{2,10},{26... | collective-permute-start | bytes 786440 | tf_op jit(solution)/shard_map/ppermute | solution.py:430
  181.5 5.6 %collective-permute-start.41 = (bf16[512,256]{1,0:T(8,128)(2,1)S(1)}, bf16[512,256]{1,0:T(8,128)(2,1)S(1)}, u32[]{:S(2)}, u32[]{:S(2)}) collective-permute-start(bf16[512,256]{1,0:T(8,128)(2,1)S(1)} %around.41.refs_2_), channel_id=1, source_target_pairs={{0,8},{24,16},{8,0},{16,24},{1,9},{25,17},{9,1},{17,25},{2,10},{26... | collective-permute-start | bytes 786440 | tf_op jit(solution)/shard_map/ppermute | solution.py:430
  187.1 2.9 %collective-permute-start.28 = (bf16[512,256]{1,0:T(8,128)(2,1)S(1)}, bf16[512,256]{1,0:T(8,128)(2,1)S(1)}, u32[]{:S(2)}, u32[]{:S(2)}) collective-permute-start(bf16[512,256]{1,0:T(8,128)(2,1)S(1)} %around.35.refs_3_), channel_id=1, source_target_pairs={{0,8},{24,16},{8,0},{16,24},{1,9},{25,17},{9,1},{17,25},{2,10},{26... | collective-permute-start | bytes 786440 | tf_op jit(solution)/shard_map/ppermute | solution.py:430
  190.7 1.5 store.7
  192.2 1.5 store.8
  193.7 1.5 store.9
  195.2 1.5 store.10
  196.7 1.3 join.1
  197.9 1.5 store.11
  199.4 1.1 store.12
  200.5 2.1 %collective-permute-done.15.refs_0_ = bf16[512,256]{1,0:T(8,128)(2,1)S(1)} collective-permute-done((bf16[512,256]{1,0:T(8,128)(2,1)S(1)}, bf16[512,256]{1,0:T(8,128)(2,1)S(1)}, u32[]{:S(2)}, u32[]{:S(2)}) %collective-permute-start.15) | collective-permute-done | bytes 262176 | tf_op jit(solution)/shard_map/ppermute | solution.py:430
  (145 shorter events, 28.0 us)
Async XLA Ops:
  0.6 2.6 %copy-start.2 = (f32[3,1536]{1,0:T(4,128)S(1)}, f32[3,1536]{1,0:T(4,128)}, u32[]{:S(2)}) copy-start(f32[3,1536]{1,0:T(4,128)} %gate_taps_ref.23) | copy-start | bytes 55300
  0.6 2.6 %copy-start.3 = (f32[3,1536]{1,0:T(4,128)S(1)}, f32[3,1536]{1,0:T(4,128)}, u32[]{:S(2)}) copy-start(f32[3,1536]{1,0:T(4,128)} %up_taps_ref.23) | copy-start | bytes 55300
  0.7 2.6 %copy-start.4 = (f32[1536]{0:T(1024)S(1)}, f32[1536]{0:T(1024)}, u32[]{:S(2)}) copy-start(f32[1536]{0:T(1024)} %gate_bias_ref.23) | copy-start | bytes 18436
  0.7 2.6 %copy-start.5 = (f32[1536]{0:T(1024)S(1)}, f32[1536]{0:T(1024)}, u32[]{:S(2)}) copy-start(f32[1536]{0:T(1024)} %up_bias_ref.23) | copy-start | bytes 18436
  4.9 11.6 %collective-permute-start.29 = (bf16[512,256]{1,0:T(8,128)(2,1)S(1)}, bf16[512,256]{1,0:T(8,128)(2,1)S(1)}, u32[]{:S(2)}, u32[]{:S(2)}) collective-permute-start(bf16[512,256]{1,0:T(8,128)(2,1)S(1)} %get-tuple-element.204.a_ref), channel_id=1, source_target_pairs={{0,8},{24,16},{1,9},{25,17},{2,10},{26,18},{3,11},{27,19},{4,12},{... | collective-permute-start | bytes 786440 | tf_op jit(solution)/shard_map/ppermute | solution.py:430
  9.9 12.3 %collective-permute-start.42 = (bf16[512,256]{1,0:T(8,128)(2,1)S(1)}, bf16[512,256]{1,0:T(8,128)(2,1)S(1)}, u32[]{:S(2)}, u32[]{:S(2)}) collective-permute-start(bf16[512,256]{1,0:T(8,128)(2,1)S(1)} %get-tuple-element.210.a_ref), channel_id=1, source_target_pairs={{0,8},{24,16},{1,9},{25,17},{2,10},{26,18},{3,11},{27,19},{4,12},{... | collective-permute-start | bytes 786440 | tf_op jit(solution)/shard_map/ppermute | solution.py:430
  12.8 15.0 %collective-permute-start.16 = (bf16[512,256]{1,0:T(8,128)(2,1)S(1)}, bf16[512,256]{1,0:T(8,128)(2,1)S(1)}, u32[]{:S(2)}, u32[]{:S(2)}) collective-permute-start(bf16[512,256]{1,0:T(8,128)(2,1)S(1)} %get-tuple-element.198.a_ref), channel_id=1, source_target_pairs={{0,8},{24,16},{1,9},{25,17},{2,10},{26,18},{3,11},{27,19},{4,12},{... | collective-permute-start | bytes 786440 | tf_op jit(solution)/shard_map/ppermute | solution.py:430
  14.1 18.1 %collective-permute-start.3 = (bf16[512,256]{1,0:T(8,128)(2,1)S(1)}, bf16[512,256]{1,0:T(8,128)(2,1)S(1)}, u32[]{:S(2)}, u32[]{:S(2)}) collective-permute-start(bf16[512,256]{1,0:T(8,128)(2,1)S(1)} %get-tuple-element.192.a_ref), channel_id=1, source_target_pairs={{0,8},{24,16},{1,9},{25,17},{2,10},{26,18},{3,11},{27,19},{4,12},{... | collective-permute-start | bytes 786440 | tf_op jit(solution)/shard_map/ppermute | solution.py:430
  16.6 22.9 %collective-permute-start.30 = (bf16[512,256]{1,0:T(8,128)(2,1)S(1)}, bf16[512,256]{1,0:T(8,128)(2,1)S(1)}, u32[]{:S(2)}, u32[]{:S(2)}) collective-permute-start(bf16[512,256]{1,0:T(8,128)(2,1)S(1)} %add.42.pair_ref), channel_id=1, source_target_pairs={{8,16},{16,8},{9,17},{17,9},{10,18},{18,10},{11,19},{19,11},{12,20... | collective-permute-start | bytes 786440 | tf_op jit(solution)/shard_map/ppermute | solution.py:434
  22.2 22.7 %collective-permute-start.43 = (bf16[512,256]{1,0:T(8,128)(2,1)S(1)}, bf16[512,256]{1,0:T(8,128)(2,1)S(1)}, u32[]{:S(2)}, u32[]{:S(2)}) collective-permute-start(bf16[512,256]{1,0:T(8,128)(2,1)S(1)} %add.48.pair_ref), channel_id=1, source_target_pairs={{8,16},{16,8},{9,17},{17,9},{10,18},{18,10},{11,19},{19,11},{12,20... | collective-permute-start | bytes 786440 | tf_op jit(solution)/shard_map/ppermute | solution.py:434
  27.9 22.1 %collective-permute-start.17 = (bf16[512,256]{1,0:T(8,128)(2,1)S(1)}, bf16[512,256]{1,0:T(8,128)(2,1)S(1)}, u32[]{:S(2)}, u32[]{:S(2)}) collective-permute-start(bf16[512,256]{1,0:T(8,128)(2,1)S(1)} %add.36.pair_ref), channel_id=1, source_target_pairs={{8,16},{16,8},{9,17},{17,9},{10,18},{18,10},{11,19},{19,11},{12,20... | collective-permute-start | bytes 786440 | tf_op jit(solution)/shard_map/ppermute | solution.py:434
  32.4 19.8 %collective-permute-start.4 = (bf16[512,256]{1,0:T(8,128)(2,1)S(1)}, bf16[512,256]{1,0:T(8,128)(2,1)S(1)}, u32[]{:S(2)}, u32[]{:S(2)}) collective-permute-start(bf16[512,256]{1,0:T(8,128)(2,1)S(1)} %add.30.pair_ref), channel_id=1, source_target_pairs={{8,16},{16,8},{9,17},{17,9},{10,18},{18,10},{11,19},{19,11},{12,20... | collective-permute-start | bytes 786440 | tf_op jit(solution)/shard_map/ppermute | solution.py:434
  39.6 18.9 %collective-permute-start.31 = (bf16[512,256]{1,0:T(8,128)(2,1)S(1)}, bf16[512,256]{1,0:T(8,128)(2,1)S(1)}, u32[]{:S(2)}, u32[]{:S(2)}) collective-permute-start(bf16[512,256]{1,0:T(8,128)(2,1)S(1)} %around.36.refs_4_), channel_id=1, source_target_pairs={{0,8},{24,16},{8,0},{16,24},{1,9},{25,17},{9,1},{17,25},{2,10},{26... | collective-permute-start | bytes 786440 | tf_op jit(solution)/shard_map/ppermute | solution.py:430
  45.0 12.7 %collective-permute-start.44 = (bf16[512,256]{1,0:T(8,128)(2,1)S(1)}, bf16[512,256]{1,0:T(8,128)(2,1)S(1)}, u32[]{:S(2)}, u32[]{:S(2)}) collective-permute-start(bf16[512,256]{1,0:T(8,128)(2,1)S(1)} %around.42.refs_5_), channel_id=1, source_target_pairs={{0,8},{24,16},{8,0},{16,24},{1,9},{25,17},{9,1},{17,25},{2,10},{26... | collective-permute-start | bytes 786440 | tf_op jit(solution)/shard_map/ppermute | solution.py:430
  48.4 3.9 %copy-start = (bf16[1024,1536]{1,0:T(8,128)(2,1)S(1)}, bf16[1024,1536]{1,0:T(8,128)(2,1)}, u32[]{:S(2)}) copy-start(bf16[1024,1536]{1,0:T(8,128)(2,1)} %refs_2_.11) | copy-start | bytes 9437188
  48.4 3.9 %copy-start.1 = (bf16[1024,1536]{1,0:T(8,128)(2,1)S(1)}, bf16[1024,1536]{1,0:T(8,128)(2,1)}, u32[]{:S(2)}) copy-start(bf16[1024,1536]{1,0:T(8,128)(2,1)} %refs_3_.11) | copy-start | bytes 9437188
  50.0 13.3 %collective-permute-start.18 = (bf16[512,256]{1,0:T(8,128)(2,1)S(1)}, bf16[512,256]{1,0:T(8,128)(2,1)S(1)}, u32[]{:S(2)}, u32[]{:S(2)}) collective-permute-start(bf16[512,256]{1,0:T(8,128)(2,1)S(1)} %around.30.refs_7_), channel_id=1, source_target_pairs={{0,8},{24,16},{8,0},{16,24},{1,9},{25,17},{9,1},{17,25},{2,10},{26... | collective-permute-start | bytes 786440 | tf_op jit(solution)/shard_map/ppermute | solution.py:430
  52.1 14.8 %collective-permute-start.5 = (bf16[512,256]{1,0:T(8,128)(2,1)S(1)}, bf16[512,256]{1,0:T(8,128)(2,1)S(1)}, u32[]{:S(2)}, u32[]{:S(2)}) collective-permute-start(bf16[512,256]{1,0:T(8,128)(2,1)S(1)} %around.24.refs_6_), channel_id=1, source_target_pairs={{0,8},{24,16},{8,0},{16,24},{1,9},{25,17},{9,1},{17,25},{2,10},{26... | collective-permute-start | bytes 786440 | tf_op jit(solution)/shard_map/ppermute | solution.py:430
  57.8 12.1 %collective-permute-start.45 = (bf16[512,256]{1,0:T(8,128)(2,1)S(1)}, bf16[512,256]{1,0:T(8,128)(2,1)S(1)}, u32[]{:S(2)}, u32[]{:S(2)}) collective-permute-start(bf16[512,256]{1,0:T(8,128)(2,1)S(1)} %add.49.pair_ref), channel_id=1, source_target_pairs={{8,16},{16,8},{9,17},{17,9},{10,18},{18,10},{11,19},{19,11},{12,20... | collective-permute-start | bytes 786440 | tf_op jit(solution)/shard_map/ppermute | solution.py:434
  58.6 18.3 %collective-permute-start.32 = (bf16[512,256]{1,0:T(8,128)(2,1)S(1)}, bf16[512,256]{1,0:T(8,128)(2,1)S(1)}, u32[]{:S(2)}, u32[]{:S(2)}) collective-permute-start(bf16[512,256]{1,0:T(8,128)(2,1)S(1)} %add.43.pair_ref), channel_id=1, source_target_pairs={{8,16},{16,8},{9,17},{17,9},{10,18},{18,10},{11,19},{19,11},{12,20... | collective-permute-start | bytes 786440 | tf_op jit(solution)/shard_map/ppermute | solution.py:434
  63.4 14.9 %collective-permute-start.19 = (bf16[512,256]{1,0:T(8,128)(2,1)S(1)}, bf16[512,256]{1,0:T(8,128)(2,1)S(1)}, u32[]{:S(2)}, u32[]{:S(2)}) collective-permute-start(bf16[512,256]{1,0:T(8,128)(2,1)S(1)} %add.37.pair_ref), channel_id=1, source_target_pairs={{8,16},{16,8},{9,17},{17,9},{10,18},{18,10},{11,19},{19,11},{12,20... | collective-permute-start | bytes 786440 | tf_op jit(solution)/shard_map/ppermute | solution.py:434
  67.0 13.4 %collective-permute-start.6 = (bf16[512,256]{1,0:T(8,128)(2,1)S(1)}, bf16[512,256]{1,0:T(8,128)(2,1)S(1)}, u32[]{:S(2)}, u32[]{:S(2)}) collective-permute-start(bf16[512,256]{1,0:T(8,128)(2,1)S(1)} %add.31.pair_ref), channel_id=1, source_target_pairs={{8,16},{16,8},{9,17},{17,9},{10,18},{18,10},{11,19},{19,11},{12,20... | collective-permute-start | bytes 786440 | tf_op jit(solution)/shard_map/ppermute | solution.py:434
  69.9 12.6 %collective-permute-start.46 = (bf16[512,256]{1,0:T(8,128)(2,1)S(1)}, bf16[512,256]{1,0:T(8,128)(2,1)S(1)}, u32[]{:S(2)}, u32[]{:S(2)}) collective-permute-start(bf16[512,256]{1,0:T(8,128)(2,1)S(1)} %around.43.refs_5_), channel_id=1, source_target_pairs={{0,8},{24,16},{8,0},{16,24},{1,9},{25,17},{9,1},{17,25},{2,10},{26... | collective-permute-start | bytes 786440 | tf_op jit(solution)/shard_map/ppermute | solution.py:430
  76.9 9.4 %collective-permute-start.33 = (bf16[512,256]{1,0:T(8,128)(2,1)S(1)}, bf16[512,256]{1,0:T(8,128)(2,1)S(1)}, u32[]{:S(2)}, u32[]{:S(2)}) collective-permute-start(bf16[512,256]{1,0:T(8,128)(2,1)S(1)} %around.37.refs_4_), channel_id=1, source_target_pairs={{0,8},{24,16},{8,0},{16,24},{1,9},{25,17},{9,1},{17,25},{2,10},{26... | collective-permute-start | bytes 786440 | tf_op jit(solution)/shard_map/ppermute | solution.py:430
  78.3 35.7 %collective-permute-start = (bf16[768,512]{1,0:T(8,128)(2,1)S(1)}, bf16[768,512]{1,0:T(8,128)(2,1)S(1)}, u32[]{:S(2)}, u32[]{:S(2)}) collective-permute-start(bf16[768,512]{1,0:T(8,128)(2,1)S(1)} %get-tuple-element.186), channel_id=1, source_target_pairs={{0,1},{1,0},{2,3},{3,2},{4,5},{5,4},{6,7},{7,6},{8,9},{9,8},{10,11... | collective-permute-start | bytes 2359304 | tf_op jit(solution)/shard_map/ppermute | solution.py:450
  78.4 13.6 %collective-permute-start.20 = (bf16[512,256]{1,0:T(8,128)(2,1)S(1)}, bf16[512,256]{1,0:T(8,128)(2,1)S(1)}, u32[]{:S(2)}, u32[]{:S(2)}) collective-permute-start(bf16[512,256]{1,0:T(8,128)(2,1)S(1)} %around.31.refs_7_), channel_id=1, source_target_pairs={{0,8},{24,16},{8,0},{16,24},{1,9},{25,17},{9,1},{17,25},{2,10},{26... | collective-permute-start | bytes 786440 | tf_op jit(solution)/shard_map/ppermute | solution.py:430
  80.5 14.8 %collective-permute-start.7 = (bf16[512,256]{1,0:T(8,128)(2,1)S(1)}, bf16[512,256]{1,0:T(8,128)(2,1)S(1)}, u32[]{:S(2)}, u32[]{:S(2)}) collective-permute-start(bf16[512,256]{1,0:T(8,128)(2,1)S(1)} %around.25.refs_6_), channel_id=1, source_target_pairs={{0,8},{24,16},{8,0},{16,24},{1,9},{25,17},{9,1},{17,25},{2,10},{26... | collective-permute-start | bytes 786440 | tf_op jit(solution)/shard_map/ppermute | solution.py:430
  82.5 13.5 %collective-permute-start.47 = (bf16[512,256]{1,0:T(8,128)(2,1)S(1)}, bf16[512,256]{1,0:T(8,128)(2,1)S(1)}, u32[]{:S(2)}, u32[]{:S(2)}) collective-permute-start(bf16[512,256]{1,0:T(8,128)(2,1)S(1)} %add.50.pair_ref), channel_id=1, source_target_pairs={{8,16},{16,8},{9,17},{17,9},{10,18},{18,10},{11,19},{19,11},{12,20... | collective-permute-start | bytes 786440 | tf_op jit(solution)/shard_map/ppermute | solution.py:434
  86.4 14.0 %collective-permute-start.34 = (bf16[512,256]{1,0:T(8,128)(2,1)S(1)}, bf16[512,256]{1,0:T(8,128)(2,1)S(1)}, u32[]{:S(2)}, u32[]{:S(2)}) collective-permute-start(bf16[512,256]{1,0:T(8,128)(2,1)S(1)} %add.44.pair_ref), channel_id=1, source_target_pairs={{8,16},{16,8},{9,17},{17,9},{10,18},{18,10},{11,19},{19,11},{12,20... | collective-permute-start | bytes 786440 | tf_op jit(solution)/shard_map/ppermute | solution.py:434
  92.0 8.6 %collective-permute-start.21 = (bf16[512,256]{1,0:T(8,128)(2,1)S(1)}, bf16[512,256]{1,0:T(8,128)(2,1)S(1)}, u32[]{:S(2)}, u32[]{:S(2)}) collective-permute-start(bf16[512,256]{1,0:T(8,128)(2,1)S(1)} %add.38.pair_ref), channel_id=1, source_target_pairs={{8,16},{16,8},{9,17},{17,9},{10,18},{18,10},{11,19},{19,11},{12,20... | collective-permute-start | bytes 786440 | tf_op jit(solution)/shard_map/ppermute | solution.py:434
  95.4 10.4 %collective-permute-start.8 = (bf16[512,256]{1,0:T(8,128)(2,1)S(1)}, bf16[512,256]{1,0:T(8,128)(2,1)S(1)}, u32[]{:S(2)}, u32[]{:S(2)}) collective-permute-start(bf16[512,256]{1,0:T(8,128)(2,1)S(1)} %add.32.pair_ref), channel_id=1, source_target_pairs={{8,16},{16,8},{9,17},{17,9},{10,18},{18,10},{11,19},{19,11},{12,20... | collective-permute-start | bytes 786440 | tf_op jit(solution)/shard_map/ppermute | solution.py:434
  96.1 13.5 %collective-permute-start.48 = (bf16[512,256]{1,0:T(8,128)(2,1)S(1)}, bf16[512,256]{1,0:T(8,128)(2,1)S(1)}, u32[]{:S(2)}, u32[]{:S(2)}) collective-permute-start(bf16[512,256]{1,0:T(8,128)(2,1)S(1)} %around.44.refs_5_), channel_id=1, source_target_pairs={{0,8},{24,16},{8,0},{16,24},{1,9},{25,17},{9,1},{17,25},{2,10},{26... | collective-permute-start | bytes 786440 | tf_op jit(solution)/shard_map/ppermute | solution.py:430
  100.5 12.7 %collective-permute-start.35 = (bf16[512,256]{1,0:T(8,128)(2,1)S(1)}, bf16[512,256]{1,0:T(8,128)(2,1)S(1)}, u32[]{:S(2)}, u32[]{:S(2)}) collective-permute-start(bf16[512,256]{1,0:T(8,128)(2,1)S(1)} %around.38.refs_4_), channel_id=1, source_target_pairs={{0,8},{24,16},{8,0},{16,24},{1,9},{25,17},{9,1},{17,25},{2,10},{26... | collective-permute-start | bytes 786440 | tf_op jit(solution)/shard_map/ppermute | solution.py:430
  100.6 17.1 %collective-permute-start.22 = (bf16[512,256]{1,0:T(8,128)(2,1)S(1)}, bf16[512,256]{1,0:T(8,128)(2,1)S(1)}, u32[]{:S(2)}, u32[]{:S(2)}) collective-permute-start(bf16[512,256]{1,0:T(8,128)(2,1)S(1)} %around.32.refs_7_), channel_id=1, source_target_pairs={{0,8},{24,16},{8,0},{16,24},{1,9},{25,17},{9,1},{17,25},{2,10},{26... | collective-permute-start | bytes 786440 | tf_op jit(solution)/shard_map/ppermute | solution.py:430
  105.8 14.7 %collective-permute-start.9 = (bf16[512,256]{1,0:T(8,128)(2,1)S(1)}, bf16[512,256]{1,0:T(8,128)(2,1)S(1)}, u32[]{:S(2)}, u32[]{:S(2)}) collective-permute-start(bf16[512,256]{1,0:T(8,128)(2,1)S(1)} %around.26.refs_6_), channel_id=1, source_target_pairs={{0,8},{24,16},{8,0},{16,24},{1,9},{25,17},{9,1},{17,25},{2,10},{26... | collective-permute-start | bytes 786440 | tf_op jit(solution)/shard_map/ppermute | solution.py:430
  109.7 11.5 %collective-permute-start.49 = (bf16[512,256]{1,0:T(8,128)(2,1)S(1)}, bf16[512,256]{1,0:T(8,128)(2,1)S(1)}, u32[]{:S(2)}, u32[]{:S(2)}) collective-permute-start(bf16[512,256]{1,0:T(8,128)(2,1)S(1)} %add.51.pair_ref), channel_id=1, source_target_pairs={{8,16},{16,8},{9,17},{17,9},{10,18},{18,10},{11,19},{19,11},{12,20... | collective-permute-start | bytes 786440 | tf_op jit(solution)/shard_map/ppermute | solution.py:434
  113.3 12.9 %collective-permute-start.36 = (bf16[512,256]{1,0:T(8,128)(2,1)S(1)}, bf16[512,256]{1,0:T(8,128)(2,1)S(1)}, u32[]{:S(2)}, u32[]{:S(2)}) collective-permute-start(bf16[512,256]{1,0:T(8,128)(2,1)S(1)} %add.45.pair_ref), channel_id=1, source_target_pairs={{8,16},{16,8},{9,17},{17,9},{10,18},{18,10},{11,19},{19,11},{12,20... | collective-permute-start | bytes 786440 | tf_op jit(solution)/shard_map/ppermute | solution.py:434
  114.2 38.3 %collective-permute-start.1 = (bf16[768,512]{1,0:T(8,128)(2,1)S(1)}, bf16[768,512]{1,0:T(8,128)(2,1)S(1)}, u32[]{:S(2)}, u32[]{:S(2)}) collective-permute-start(bf16[768,512]{1,0:T(8,128)(2,1)S(1)} %add.28.a_ref), channel_id=1, source_target_pairs={{0,2},{2,0},{1,3},{3,1},{4,6},{6,4},{5,7},{7,5},{8,10},{10,8},{9,1... | collective-permute-start | bytes 2359304 | tf_op jit(solution)/shard_map/ppermute | solution.py:452
  117.8 8.8 %collective-permute-start.23 = (bf16[512,256]{1,0:T(8,128)(2,1)S(1)}, bf16[512,256]{1,0:T(8,128)(2,1)S(1)}, u32[]{:S(2)}, u32[]{:S(2)}) collective-permute-start(bf16[512,256]{1,0:T(8,128)(2,1)S(1)} %add.39.pair_ref), channel_id=1, source_target_pairs={{8,16},{16,8},{9,17},{17,9},{10,18},{18,10},{11,19},{19,11},{12,20... | collective-permute-start | bytes 786440 | tf_op jit(solution)/shard_map/ppermute | solution.py:434
  120.6 11.6 %collective-permute-start.10 = (bf16[512,256]{1,0:T(8,128)(2,1)S(1)}, bf16[512,256]{1,0:T(8,128)(2,1)S(1)}, u32[]{:S(2)}, u32[]{:S(2)}) collective-permute-start(bf16[512,256]{1,0:T(8,128)(2,1)S(1)} %add.33.pair_ref), channel_id=1, source_target_pairs={{8,16},{16,8},{9,17},{17,9},{10,18},{18,10},{11,19},{19,11},{12,20... | collective-permute-start | bytes 786440 | tf_op jit(solution)/shard_map/ppermute | solution.py:434
  121.3 13.9 %collective-permute-start.50 = (bf16[512,256]{1,0:T(8,128)(2,1)S(1)}, bf16[512,256]{1,0:T(8,128)(2,1)S(1)}, u32[]{:S(2)}, u32[]{:S(2)}) collective-permute-start(bf16[512,256]{1,0:T(8,128)(2,1)S(1)} %around.45.refs_5_), channel_id=1, source_target_pairs={{0,8},{24,16},{8,0},{16,24},{1,9},{25,17},{9,1},{17,25},{2,10},{26... | collective-permute-start | bytes 786440 | tf_op jit(solution)/shard_map/ppermute | solution.py:430
  126.2 12.7 %collective-permute-start.37 = (bf16[512,256]{1,0:T(8,128)(2,1)S(1)}, bf16[512,256]{1,0:T(8,128)(2,1)S(1)}, u32[]{:S(2)}, u32[]{:S(2)}) collective-permute-start(bf16[512,256]{1,0:T(8,128)(2,1)S(1)} %around.39.refs_4_), channel_id=1, source_target_pairs={{0,8},{24,16},{8,0},{16,24},{1,9},{25,17},{9,1},{17,25},{2,10},{26... | collective-permute-start | bytes 786440 | tf_op jit(solution)/shard_map/ppermute | solution.py:430
  126.6 16.0 %collective-permute-start.24 = (bf16[512,256]{1,0:T(8,128)(2,1)S(1)}, bf16[512,256]{1,0:T(8,128)(2,1)S(1)}, u32[]{:S(2)}, u32[]{:S(2)}) collective-permute-start(bf16[512,256]{1,0:T(8,128)(2,1)S(1)} %around.33.refs_7_), channel_id=1, source_target_pairs={{0,8},{24,16},{8,0},{16,24},{1,9},{25,17},{9,1},{17,25},{2,10},{26... | collective-permute-start | bytes 786440 | tf_op jit(solution)/shard_map/ppermute | solution.py:430
  132.2 13.2 %collective-permute-start.11 = (bf16[512,256]{1,0:T(8,128)(2,1)S(1)}, bf16[512,256]{1,0:T(8,128)(2,1)S(1)}, u32[]{:S(2)}, u32[]{:S(2)}) collective-permute-start(bf16[512,256]{1,0:T(8,128)(2,1)S(1)} %around.27.refs_6_), channel_id=1, source_target_pairs={{0,8},{24,16},{8,0},{16,24},{1,9},{25,17},{9,1},{17,25},{2,10},{26... | collective-permute-start | bytes 786440 | tf_op jit(solution)/shard_map/ppermute | solution.py:430
  135.3 10.9 %collective-permute-start.51 = (bf16[512,256]{1,0:T(8,128)(2,1)S(1)}, bf16[512,256]{1,0:T(8,128)(2,1)S(1)}, u32[]{:S(2)}, u32[]{:S(2)}) collective-permute-start(bf16[512,256]{1,0:T(8,128)(2,1)S(1)} %add.52.pair_ref), channel_id=1, source_target_pairs={{8,16},{16,8},{9,17},{17,9},{10,18},{18,10},{11,19},{19,11},{12,20... | collective-permute-start | bytes 786440 | tf_op jit(solution)/shard_map/ppermute | solution.py:434
  139.0 13.3 %collective-permute-start.38 = (bf16[512,256]{1,0:T(8,128)(2,1)S(1)}, bf16[512,256]{1,0:T(8,128)(2,1)S(1)}, u32[]{:S(2)}, u32[]{:S(2)}) collective-permute-start(bf16[512,256]{1,0:T(8,128)(2,1)S(1)} %add.46.pair_ref), channel_id=1, source_target_pairs={{8,16},{16,8},{9,17},{17,9},{10,18},{18,10},{11,19},{19,11},{12,20... | collective-permute-start | bytes 786440 | tf_op jit(solution)/shard_map/ppermute | solution.py:434
  142.7 12.1 %collective-permute-start.25 = (bf16[512,256]{1,0:T(8,128)(2,1)S(1)}, bf16[512,256]{1,0:T(8,128)(2,1)S(1)}, u32[]{:S(2)}, u32[]{:S(2)}) collective-permute-start(bf16[512,256]{1,0:T(8,128)(2,1)S(1)} %add.40.pair_ref), channel_id=1, source_target_pairs={{8,16},{16,8},{9,17},{17,9},{10,18},{18,10},{11,19},{19,11},{12,20... | collective-permute-start | bytes 786440 | tf_op jit(solution)/shard_map/ppermute | solution.py:434
  145.5 9.4 %collective-permute-start.12 = (bf16[512,256]{1,0:T(8,128)(2,1)S(1)}, bf16[512,256]{1,0:T(8,128)(2,1)S(1)}, u32[]{:S(2)}, u32[]{:S(2)}) collective-permute-start(bf16[512,256]{1,0:T(8,128)(2,1)S(1)} %add.34.pair_ref), channel_id=1, source_target_pairs={{8,16},{16,8},{9,17},{17,9},{10,18},{18,10},{11,19},{19,11},{12,20... | collective-permute-start | bytes 786440 | tf_op jit(solution)/shard_map/ppermute | solution.py:434
  146.2 13.6 %collective-permute-start.55 = (bf16[8,3072]{1,0:T(8,128)(2,1)S(1)}, bf16[8,3072]{1,0:T(8,128)(2,1)S(1)}, u32[]{:S(2)}, u32[]{:S(2)}) collective-permute-start(bf16[8,3072]{1,0:T(8,128)(2,1)S(1)} %gather.1.a_ref), channel_id=1, source_target_pairs={{0,8},{24,16},{1,9},{25,17},{2,10},{26,18},{3,11},{27,19},{4,12},{... | collective-permute-start | bytes 147464 | tf_op jit(solution)/shard_map/ppermute | solution.py:414
  152.4 7.6 %collective-permute-start.52 = (bf16[512,256]{1,0:T(8,128)(2,1)S(1)}, bf16[512,256]{1,0:T(8,128)(2,1)S(1)}, u32[]{:S(2)}, u32[]{:S(2)}) collective-permute-start(bf16[512,256]{1,0:T(8,128)(2,1)S(1)} %around.46.refs_5_), channel_id=1, source_target_pairs={{0,8},{24,16},{8,0},{16,24},{1,9},{25,17},{9,1},{17,25},{2,10},{26... | collective-permute-start | bytes 786440 | tf_op jit(solution)/shard_map/ppermute | solution.py:430
  152.5 12.3 %collective-permute-start.39 = (bf16[512,256]{1,0:T(8,128)(2,1)S(1)}, bf16[512,256]{1,0:T(8,128)(2,1)S(1)}, u32[]{:S(2)}, u32[]{:S(2)}) collective-permute-start(bf16[512,256]{1,0:T(8,128)(2,1)S(1)} %around.40.refs_4_), channel_id=1, source_target_pairs={{0,8},{24,16},{8,0},{16,24},{1,9},{25,17},{9,1},{17,25},{2,10},{26... | collective-permute-start | bytes 786440 | tf_op jit(solution)/shard_map/ppermute | solution.py:430
  154.8 41.9 %collective-permute-start.2 = (bf16[768,512]{1,0:T(8,128)(2,1)S(1)}, bf16[768,512]{1,0:T(8,128)(2,1)S(1)}, u32[]{:S(2)}, u32[]{:S(2)}) collective-permute-start(bf16[768,512]{1,0:T(8,128)(2,1)S(1)} %add.29.own_ref), channel_id=1, source_target_pairs={{0,1},{1,0},{2,3},{3,2},{4,5},{5,4},{6,7},{7,6},{8,9},{9,8},{10,11... | collective-permute-start | bytes 2359304 | tf_op jit(solution)/shard_map/ppermute | solution.py:454
  154.9 15.1 %collective-permute-start.26 = (bf16[512,256]{1,0:T(8,128)(2,1)S(1)}, bf16[512,256]{1,0:T(8,128)(2,1)S(1)}, u32[]{:S(2)}, u32[]{:S(2)}) collective-permute-start(bf16[512,256]{1,0:T(8,128)(2,1)S(1)} %around.34.refs_7_), channel_id=1, source_target_pairs={{0,8},{24,16},{8,0},{16,24},{1,9},{25,17},{9,1},{17,25},{2,10},{26... | collective-permute-start | bytes 786440 | tf_op jit(solution)/shard_map/ppermute | solution.py:430
  159.8 13.1 %collective-permute-start.13 = (bf16[512,256]{1,0:T(8,128)(2,1)S(1)}, bf16[512,256]{1,0:T(8,128)(2,1)S(1)}, u32[]{:S(2)}, u32[]{:S(2)}) collective-permute-start(bf16[512,256]{1,0:T(8,128)(2,1)S(1)} %around.28.refs_6_), channel_id=1, source_target_pairs={{0,8},{24,16},{8,0},{16,24},{1,9},{25,17},{9,1},{17,25},{2,10},{26... | collective-permute-start | bytes 786440 | tf_op jit(solution)/shard_map/ppermute | solution.py:430
  159.9 13.7 %collective-permute-start.56 = (bf16[8,3072]{1,0:T(8,128)(2,1)S(1)}, bf16[8,3072]{1,0:T(8,128)(2,1)S(1)}, u32[]{:S(2)}, u32[]{:S(2)}) collective-permute-start(bf16[8,3072]{1,0:T(8,128)(2,1)S(1)} %add.54.a_ref), channel_id=1, source_target_pairs={{8,16},{16,8},{9,17},{17,9},{10,18},{18,10},{11,19},{19,11},{12,20... | collective-permute-start | bytes 147464 | tf_op jit(solution)/shard_map/ppermute | solution.py:416
  164.8 9.5 %collective-permute-start.53 = (bf16[512,256]{1,0:T(8,128)(2,1)S(1)}, bf16[512,256]{1,0:T(8,128)(2,1)S(1)}, u32[]{:S(2)}, u32[]{:S(2)}) collective-permute-start(bf16[512,256]{1,0:T(8,128)(2,1)S(1)} %add.53.pair_ref), channel_id=1, source_target_pairs={{8,16},{16,8},{9,17},{17,9},{10,18},{18,10},{11,19},{19,11},{12,20... | collective-permute-start | bytes 786440 | tf_op jit(solution)/shard_map/ppermute | solution.py:434
  170.0 5.6 %collective-permute-start.40 = (bf16[512,256]{1,0:T(8,128)(2,1)S(1)}, bf16[512,256]{1,0:T(8,128)(2,1)S(1)}, u32[]{:S(2)}, u32[]{:S(2)}) collective-permute-start(bf16[512,256]{1,0:T(8,128)(2,1)S(1)} %add.47.pair_ref), channel_id=1, source_target_pairs={{8,16},{16,8},{9,17},{17,9},{10,18},{18,10},{11,19},{19,11},{12,20... | collective-permute-start | bytes 786440 | tf_op jit(solution)/shard_map/ppermute | solution.py:434
  172.8 8.6 %collective-permute-start.27 = (bf16[512,256]{1,0:T(8,128)(2,1)S(1)}, bf16[512,256]{1,0:T(8,128)(2,1)S(1)}, u32[]{:S(2)}, u32[]{:S(2)}) collective-permute-start(bf16[512,256]{1,0:T(8,128)(2,1)S(1)} %add.41.pair_ref), channel_id=1, source_target_pairs={{8,16},{16,8},{9,17},{17,9},{10,18},{18,10},{11,19},{19,11},{12,20... | collective-permute-start | bytes 786440 | tf_op jit(solution)/shard_map/ppermute | solution.py:434
  173.6 13.5 %collective-permute-start.14 = (bf16[512,256]{1,0:T(8,128)(2,1)S(1)}, bf16[512,256]{1,0:T(8,128)(2,1)S(1)}, u32[]{:S(2)}, u32[]{:S(2)}) collective-permute-start(bf16[512,256]{1,0:T(8,128)(2,1)S(1)} %add.35.pair_ref), channel_id=1, source_target_pairs={{8,16},{16,8},{9,17},{17,9},{10,18},{18,10},{11,19},{19,11},{12,20... | collective-permute-start | bytes 786440 | tf_op jit(solution)/shard_map/ppermute | solution.py:434
  174.3 15.7 %collective-permute-start.57 = (bf16[8,3072]{1,0:T(8,128)(2,1)S(1)}, bf16[8,3072]{1,0:T(8,128)(2,1)S(1)}, u32[]{:S(2)}, u32[]{:S(2)}) collective-permute-start(bf16[8,3072]{1,0:T(8,128)(2,1)S(1)} %add.55.final_ref), channel_id=1, source_target_pairs={{8,0},{16,24},{9,1},{17,25},{10,2},{18,26},{11,3},{19,27},{12,4},{... | collective-permute-start | bytes 147464 | tf_op jit(solution)/shard_map/ppermute | solution.py:418
  175.7 23.8 %collective-permute-start.54 = (bf16[512,256]{1,0:T(8,128)(2,1)S(1)}, bf16[512,256]{1,0:T(8,128)(2,1)S(1)}, u32[]{:S(2)}, u32[]{:S(2)}) collective-permute-start(bf16[512,256]{1,0:T(8,128)(2,1)S(1)} %around.47.refs_3_), channel_id=1, source_target_pairs={{0,8},{24,16},{8,0},{16,24},{1,9},{25,17},{9,1},{17,25},{2,10},{26... | collective-permute-start | bytes 786440 | tf_op jit(solution)/shard_map/ppermute | solution.py:430
  181.5 18.0 %collective-permute-start.41 = (bf16[512,256]{1,0:T(8,128)(2,1)S(1)}, bf16[512,256]{1,0:T(8,128)(2,1)S(1)}, u32[]{:S(2)}, u32[]{:S(2)}) collective-permute-start(bf16[512,256]{1,0:T(8,128)(2,1)S(1)} %around.41.refs_2_), channel_id=1, source_target_pairs={{0,8},{24,16},{8,0},{16,24},{1,9},{25,17},{9,1},{17,25},{2,10},{26... | collective-permute-start | bytes 786440 | tf_op jit(solution)/shard_map/ppermute | solution.py:430
  187.1 13.4 %collective-permute-start.28 = (bf16[512,256]{1,0:T(8,128)(2,1)S(1)}, bf16[512,256]{1,0:T(8,128)(2,1)S(1)}, u32[]{:S(2)}, u32[]{:S(2)}) collective-permute-start(bf16[512,256]{1,0:T(8,128)(2,1)S(1)} %around.35.refs_3_), channel_id=1, source_target_pairs={{0,8},{24,16},{8,0},{16,24},{1,9},{25,17},{9,1},{17,25},{2,10},{26... | collective-permute-start | bytes 786440 | tf_op jit(solution)/shard_map/ppermute | solution.py:430
  190.0 12.6 %collective-permute-start.15 = (bf16[512,256]{1,0:T(8,128)(2,1)S(1)}, bf16[512,256]{1,0:T(8,128)(2,1)S(1)}, u32[]{:S(2)}, u32[]{:S(2)}) collective-permute-start(bf16[512,256]{1,0:T(8,128)(2,1)S(1)} %around.29.refs_2_), channel_id=1, source_target_pairs={{0,8},{24,16},{8,0},{16,24},{1,9},{25,17},{9,1},{17,25},{2,10},{26... | collective-permute-start | bytes 786440 | tf_op jit(solution)/shard_map/ppermute | solution.py:430

commit v3 on v2

--- a/solution.py
+++ b/solution.py
@@ -51,50 +51,50 @@
     return copies
 
 
-def turn_kernel(in_ref, gate_ref, up_ref, grad_ref, out_ref, gate_in, up_in, grad_in, sems):
-    copies = start_loads(0, (gate_ref, up_ref, grad_ref), (gate_in, up_in, grad_in), sems)
-    out_ref[...] = in_ref[...].T
-    for copy in copies:
-        copy.wait()
-
-
-def turn(tokens, signals):
-    length, features = tokens.shape
-    return pl.pallas_call(
-        turn_kernel,
-        in_specs=[VMEM, HBM, HBM, HBM],
-        out_specs=[VMEM] * 4,
-        out_shape=[pltpu.VMEM((features, length), tokens.dtype)]
-        + [pltpu.VMEM((length, BLOCK), tokens.dtype)] * 3,
-        scratch_shapes=[pltpu.SemaphoreType.DMA((3,))],
-        compiler_params=params(6),
-        name="turn",
-    )(off_chip(tokens), *(off_chip(x) for x in signals))
-
-
-def block_kernel(
-    index,
-    last,
-    aliased,
-    tokens_ref,
-    gate_pre_ref,
-    up_pre_ref,
-    grad_ref,
-    gate_in,
-    up_in,
-    grad_in,
-    gate_taps_ref,
-    up_taps_ref,
-    gate_bias_ref,
-    up_bias_ref,
-    *rest,
-):
-    gate_pad, up_pad, gate_delta, up_delta, back_ref, sems = rest[-6:]
-    outs = rest[aliased:-6]
-    top_ref, bottom_ref, extra_ref, gate_back_ref, up_back_ref = outs[:5]
+def block_kernel(index, last, aliased, *refs):
+    tokens_ref, gate_pre_ref, up_pre_ref, grad_ref, gate_in, up_in, grad_in = refs[:7]
+    params_refs = refs[7:11]
+    outs, scratch = refs[11 + aliased : -6], refs[-6:]
+    sems = scratch[5]
     copies = []
     if not last:
         copies = start_loads(index + 1, (gate_pre_ref, up_pre_ref, grad_ref), outs[5:], sems)
+    back_signals(index, (gate_in, up_in, grad_in), params_refs, outs, scratch)
+    weight_partial(tokens_ref[...], outs, scratch)
+    for copy in copies:
+        copy.wait()
+
+
+def first_kernel(ends, aliased, *refs):
+    tokens_ref, gate_pre_ref, up_pre_ref, grad_ref = refs[:4]
+    params_refs = refs[4:8]
+    outs, scratch = refs[8 + aliased : -11], refs[-11:]
+    tokens_in, gate_in, up_in, grad_in, token_sem = scratch[6:]
+    sems = scratch[5]
+    sources = (gate_pre_ref, up_pre_ref, grad_ref)
+
+    @pl.when(on_end() if ends else jnp.logical_not(on_end()))
+    def _():
+        copies = start_loads(0, sources, (gate_in, up_in, grad_in), sems)
+        tokens_copy = pltpu.make_async_copy(tokens_ref, tokens_in, token_sem)
+        tokens_copy.start()
+        for copy in copies:
+            copy.wait()
+        copies = start_loads(1, sources, outs[5:8], sems)
+        back_signals(0, (gate_in, up_in, grad_in), params_refs, outs, scratch)
+        tokens_copy.wait()
+        turned = tokens_in[...].T
+        outs[8][...] = turned
+        weight_partial(turned, outs, scratch)
+        for copy in copies:
+            copy.wait()
+
+
+def back_signals(index, inputs, params_refs, outs, scratch):
+    gate_in, up_in, grad_in = inputs
+    gate_taps_ref, up_taps_ref, gate_bias_ref, up_bias_ref = params_refs
+    extra_ref, gate_back_ref, up_back_ref = outs[2:5]
+    gate_pad, up_pad, gate_delta, up_delta, back_ref = scratch[:5]
     length, width = gate_in.shape
     taps = gate_taps_ref.shape[0]
     columns = slice(index * width, (index + 1) * width)
@@ -157,32 +157,73 @@
     begin = index * width % gate_back_ref.shape[1]
     gate_back_ref[:, begin : begin + width] = back_ref[:, 0:width]
     up_back_ref[:, begin : begin + width] = back_ref[:, width:]
-    product = jnp.dot(
-        tokens_ref[...], back_ref[...], preferred_element_type=jnp.float32
-    ).astype(jnp.bfloat16)
+
+
+def weight_partial(tokens_t, outs, scratch):
+    top_ref, bottom_ref = outs[:2]
+    product = jnp.dot(tokens_t, scratch[4][...], preferred_element_type=jnp.float32).astype(jnp.bfloat16)
     rows = top_ref.shape[0]
     top_ref[...] = product[:rows]
     bottom_ref[...] = product[rows:]
-    for copy in copies:
-        copy.wait()
+
+
+def block_shapes(features, length, hidden):
+    back = pltpu.VMEM((length, max(hidden // PIECES, BLOCK)), jnp.bfloat16)
+    half = pltpu.VMEM((features // 2, 2 * BLOCK), jnp.bfloat16)
+    ready = [pltpu.VMEM((length, BLOCK), jnp.bfloat16)] * 3
+    return [half, half, pltpu.VMEM((ROWS, 2 * BLOCK), jnp.float32), back, back], ready
+
+
+def block_scratch(length):
+    return [pltpu.VMEM((length + 8, BLOCK), jnp.float32)] * 4 + [
+        pltpu.VMEM((length, 2 * BLOCK), jnp.bfloat16),
+        pltpu.SemaphoreType.DMA((3,)),
+    ]
+
+
+def first_block(ends, earlier, tokens, signals, taps, biases):
+    length, features = tokens.shape
+    hidden = signals[0].shape[1]
+    outs, ready = block_shapes(features, length, hidden)
+    outs = outs + ready + [pltpu.VMEM((features, length), jnp.bfloat16)]
+    kept = list(earlier[2:])
+    return pl.pallas_call(
+        functools.partial(first_kernel, ends, len(kept)),
+        in_specs=[HBM] * 4 + [VMEM] * (4 + len(kept)),
+        out_specs=[VMEM] * len(outs),
+        out_shape=outs,
+        scratch_shapes=block_scratch(length)
+        + [pltpu.VMEM((length, features), jnp.bfloat16)]
+        + [pltpu.VMEM((length, BLOCK), jnp.bfloat16)] * 3
+        + [pltpu.SemaphoreType.DMA],
+        input_output_aliases={8 + k: 2 + k for k in range(len(kept))},
+        compiler_params=params(10),
+        cost_estimate=pl.CostEstimate(
+            flops=2 * features * length * 2 * BLOCK + 60 * length * BLOCK,
+            bytes_accessed=2 * length * features,
+            transcendentals=length * BLOCK,
+        ),
+        name="first",
+    )(
+        off_chip(tokens),
+        *(off_chip(x) for x in (*signals, *taps, *biases)),
+        *(on_chip(x) for x in kept),
+    )
 
 
 def make_block(index, backs, tokens_t, signals, ready, taps, biases):
     length, hidden = signals[0].shape
     features = tokens_t.shape[0]
     last = (index + 1) * BLOCK == hidden
-    back = pltpu.VMEM((length, max(hidden // PIECES, BLOCK)), jnp.bfloat16)
-    half = pltpu.VMEM((features // 2, 2 * BLOCK), jnp.bfloat16)
-    outs = [half, half, pltpu.VMEM((ROWS, 2 * BLOCK), jnp.float32), back, back]
+    outs, more_ready = block_shapes(features, length, hidden)
     if not last:
-        outs += [pltpu.VMEM((length, BLOCK), jnp.bfloat16)] * 3
+        outs = outs + more_ready
     top, bottom, extra, *more = pl.pallas_call(
         functools.partial(block_kernel, index, last, len(backs)),
         in_specs=[VMEM] + [HBM] * 3 + [VMEM] * (7 + len(backs)),
         out_specs=[VMEM] * len(outs),
         out_shape=outs,
-        scratch_shapes=[pltpu.VMEM((length + 8, BLOCK), jnp.float32)] * 4
-        + [pltpu.VMEM((length, 2 * BLOCK), jnp.bfloat16), pltpu.SemaphoreType.DMA((3,))],
+        scratch_shapes=block_scratch(length),
         input_output_aliases={11: 3, 12: 4} if backs else {},
         compiler_params=params(6),
         cost_estimate=pl.CostEstimate(
@@ -419,12 +460,14 @@
     return got, final
 
 
-def line_sums(parts):
+def line_sums(firsts, parts):
     count = len(parts)
     sums, came = [], []
     for j in range(count + LAG):
         if j < LAG:
-            send, pairs = parts[j], INWARD
+            send, pairs = (firsts[j] if j < len(firsts) else parts[j]), INWARD
+        elif j == count:
+            send, pairs = sums[j - LAG], OUTWARD
         else:
             send, pairs = sums[j - LAG], INWARD + OUTWARD
         got = lax.ppermute(send, "rep", pairs)
@@ -471,11 +514,16 @@
     count = hidden // BLOCK
     per = max(count // PIECES, 1)
     signals = (gate_pre, up_pre, hidden_grad)
-    tokens_t, *ready = turn(tokens, signals)
-    chunks, extras, backs, backs_at = [], [], (), []
-    for j in range(count):
+    mixes = ((gate_taps, up_taps), (gate_bias, up_bias))
+    lead = first_block(True, (), tokens, signals, *mixes)
+    follow = first_block(False, lead, tokens, signals, *mixes)
+    extras, backs, ready, tokens_t = [follow[2]], follow[3:5], follow[5:8], follow[8]
+    firsts, chunks, backs_at = lead[:2], list(follow[:2]), []
+    if per == 1:
+        backs_at, backs = [backs], ()
+    for j in range(1, count):
         pair, extra, backs, ready = make_block(
-            j, backs, tokens_t, signals, ready, (gate_taps, up_taps), (gate_bias, up_bias)
+            j, backs, tokens_t, signals, ready, *mixes
         )
         chunks.extend(pair)
         extras.append(extra)
@@ -488,7 +536,7 @@
         for piece in range(PIECES):
             total = feature_piece(piece, *backs_at[piece], gate_weight, up_weight, total)
         result = sum_over_four(*total)
-        came, sums = line_sums(chunks)
+        came, sums = line_sums(firsts, chunks)
         outs = ()
         for first, size in store_groups(count):
             mine = slice(2 * first, 2 * (first + size))
@@ -503,6 +551,7 @@
         ) + lax.dot_general(up_back, up_weight, dims, preferred_element_type=jnp.float32)
         own = lax.psum_scatter(partial.astype(jnp.bfloat16), "tp", scatter_dimension=1, tiled=True)
         result = lax.all_gather(own, "tp", axis=1, tiled=True)
+        chunks[:2] = [jnp.where(on_end(), a, b) for a, b in zip(lead, follow[:2])]
         sums = [lax.psum(c, "rep") for c in chunks]
         gate, up = (
             jnp.concatenate(

time: 205 us -> 203 us (level)
  waiting for transfers between devices: 57.1 us -> 52.4 us
    ppermute x28, waiting for transfers between devices: 57 us -> 52.3 us  [line_sums(): got = lax.ppermute(send, 'rep', pairs)]
    ppermute x28, starting transfers between devices: 76.5 us -> 79.5 us  [line_sums(): got = lax.ppermute(send, 'rep', pairs)]
    pallas_call x1 -> x2, Pallas kernels: 2.58 us -> 4.37 us  [first_block(): pl.pallas_call(functools.partial(first_kernel, ends, len(kept)), in_specs...]
    pallas_call x12 -> x11, Pallas kernels: 19.3 us -> 17.7 us  [make_block(): pl.pallas_call(functools.partial(block_kernel, index, last, len(backs)),...]
  transfers between devices with their start and end apart: 58 -> 58, of which waited for: 20 -> 19; matrix products, arithmetic and copies ran while one was open for 0% -> 0% of each run, Pallas kernels for 18% -> 19%
where the time goes in v3:
time: 203 us; the launch traced here: 202 us
  starting transfers between devices  105 us (52%)
  waiting for transfers between devices  52.4 us (26%)
  Pallas kernels  42.8 us (21%)
    ppermute x28, starting transfers between devices, line_sums(): got = lax.ppermute(send, 'rep', pairs)  79.5 us
    ppermute x28, waiting for transfers between devices, line_sums(): got = lax.ppermute(send, 'rep', pairs)  52.3 us
    pallas_call x11, Pallas kernels, make_block(): pl.pallas_call(functools.partial(block_kernel, index, last, len(backs)),...  17.7 us
    ppermute x24, starting transfers between devices, line_sums(): other = lax.ppermute(pair, 'rep', MIDDLE)  16.2 us
    pallas_call x7, Pallas kernels, store_blocks(): pl.pallas_call(functools.partial(store_kernel, blocks), grid=(1,), in_spe...  9.5 us
    pallas_call x6, Pallas kernels, feature_piece(): pl.pallas_call(functools.partial(feature_kernel, piece), in_specs=[VMEM]...  6.42 us
    ppermute x1, starting transfers between devices, line_chunk(): got = lax.ppermute(part, 'rep', INWARD)  6.09 us
    pallas_call x2, Pallas kernels, first_block(): pl.pallas_call(functools.partial(first_kernel, ends, len(kept)), in_specs...  4.37 us
  transfers between devices with their start and end apart: 58, of which 19 were waited for; matrix products, arithmetic and copies ran while one was open for 0% of the time, Pallas kernels for 19%

profile of v3, /device:TPU:0, one launch (start us, length us, event | category | flops | bytes accessed | tf_op | source)
XLA Modules:
  0.0 202.3 jit_solution(9326237194800975698)
XLA Ops:
  0.6 3.6 %first.2 = (bf16[512,256]{1,0:T(8,128)(2,1)S(1)}, bf16[512,256]{1,0:T(8,128)(2,1)S(1)}, f32[8,256]{1,0:T(8,128)S(1)}, bf16[768,256]{1,0:T(8,128)(2,1)S(1)}, bf16...) custom-call(bf16[768,1024]{1,0:T(8,128)(2,1)} %refs_0_.3, ...), custom_call_target="tpu_custom_call" | custom-call | flops 408551424 | bytes 1572864 | tf_op jit(solution)/shard_map/first/pallas_call | solution.py:190
  4.2 2.4 %collective-permute-start.29 = (bf16[512,256]{1,0:T(8,128)(2,1)S(1)}, bf16[512,256]{1,0:T(8,128)(2,1)S(1)}, u32[]{:S(2)}, u32[]{:S(2)}) collective-permute-start(bf16[512,256]{1,0:T(8,128)(2,1)S(1)} %get-tuple-element.215), channel_id=1, source_target_pairs={{0,8},{24,16},{1,9},{25,17},{2,10},{26,18},{3,11},{27,19},{4,12},{... | collective-permute-start | bytes 786440 | tf_op jit(solution)/shard_map/ppermute | solution.py:473
  6.6 1.3 collective-permute-start.42
  8.8 1.6 block.11
  10.4 4.0 %collective-permute-start.16 = (bf16[512,256]{1,0:T(8,128)(2,1)S(1)}, bf16[512,256]{1,0:T(8,128)(2,1)S(1)}, u32[]{:S(2)}, u32[]{:S(2)}) collective-permute-start(bf16[512,256]{1,0:T(8,128)(2,1)S(1)} %get-tuple-element.208.a_ref), channel_id=1, source_target_pairs={{0,8},{24,16},{1,9},{25,17},{2,10},{26,18},{3,11},{27,19},{4,12},{... | collective-permute-start | bytes 786440 | tf_op jit(solution)/shard_map/ppermute | solution.py:473
  14.4 1.3 collective-permute-start.3
  16.5 2.4 %collective-permute-done.42.b_ref = bf16[512,256]{1,0:T(8,128)(2,1)S(1)} collective-permute-done((bf16[512,256]{1,0:T(8,128)(2,1)S(1)}, bf16[512,256]{1,0:T(8,128)(2,1)S(1)}, u32[]{:S(2)}, u32[]{:S(2)}) %collective-permute-start.42) | collective-permute-done | bytes 262176 | tf_op jit(solution)/shard_map/ppermute | solution.py:473
  19.6 1.6 block.12
  21.3 1.6 block.13
  22.9 1.6 collective-permute-done.16.b_ref
  25.3 3.8 %collective-permute-done.3.b_ref = bf16[512,256]{1,0:T(8,128)(2,1)S(1)} collective-permute-done((bf16[512,256]{1,0:T(8,128)(2,1)S(1)}, bf16[512,256]{1,0:T(8,128)(2,1)S(1)}, u32[]{:S(2)}, u32[]{:S(2)}) %collective-permute-start.3) | collective-permute-done | bytes 262176 | tf_op jit(solution)/shard_map/ppermute | solution.py:473
  29.8 1.6 block.14
  31.4 1.6 block.15
  33.0 1.6 block.16
  34.6 1.6 block.17
  36.3 7.3 %collective-permute-start.31 = (bf16[512,256]{1,0:T(8,128)(2,1)S(1)}, bf16[512,256]{1,0:T(8,128)(2,1)S(1)}, u32[]{:S(2)}, u32[]{:S(2)}) collective-permute-start(bf16[512,256]{1,0:T(8,128)(2,1)S(1)} %around.36.refs_4_), channel_id=1, source_target_pairs={{0,8},{24,16},{8,0},{16,24},{1,9},{25,17},{9,1},{17,25},{2,10},{26... | collective-permute-start | bytes 786440 | tf_op jit(solution)/shard_map/ppermute | solution.py:473
  43.8 1.6 block.18
  45.4 1.6 block.19
  47.0 1.6 block.20
  48.7 2.1 %collective-permute-start.18 = (bf16[512,256]{1,0:T(8,128)(2,1)S(1)}, bf16[512,256]{1,0:T(8,128)(2,1)S(1)}, u32[]{:S(2)}, u32[]{:S(2)}) collective-permute-start(bf16[512,256]{1,0:T(8,128)(2,1)S(1)} %around.30.refs_7_), channel_id=1, source_target_pairs={{0,8},{24,16},{8,0},{16,24},{1,9},{25,17},{9,1},{17,25},{2,10},{26... | collective-permute-start | bytes 786440 | tf_op jit(solution)/shard_map/ppermute | solution.py:473
  52.2 1.1 feature.7.refs_4_
  53.2 3.2 %collective-permute-done.44.b_ref.refs_1_ = bf16[512,256]{1,0:T(8,128)(2,1)S(1)} collective-permute-done((bf16[512,256]{1,0:T(8,128)(2,1)S(1)}, bf16[512,256]{1,0:T(8,128)(2,1)S(1)}, u32[]{:S(2)}, u32[]{:S(2)}) %collective-permute-start.44) | collective-permute-done | bytes 262176 | tf_op jit(solution)/shard_map/ppermute | solution.py:473
  57.9 1.6 block.21
  60.6 1.4 collective-permute-done.18.b_ref.refs_3_
  62.8 3.2 %collective-permute-done.5.b_ref.refs_2_ = bf16[512,256]{1,0:T(8,128)(2,1)S(1)} collective-permute-done((bf16[512,256]{1,0:T(8,128)(2,1)S(1)}, bf16[512,256]{1,0:T(8,128)(2,1)S(1)}, u32[]{:S(2)}, u32[]{:S(2)}) %collective-permute-start.5) | collective-permute-done | bytes 262176 | tf_op jit(solution)/shard_map/ppermute | solution.py:473
  66.7 1.1 feature.9.refs_4_
  68.8 6.6 %collective-permute-start.46 = (bf16[512,256]{1,0:T(8,128)(2,1)S(1)}, bf16[512,256]{1,0:T(8,128)(2,1)S(1)}, u32[]{:S(2)}, u32[]{:S(2)}) collective-permute-start(bf16[512,256]{1,0:T(8,128)(2,1)S(1)} %around.43.refs_5_), channel_id=1, source_target_pairs={{0,8},{24,16},{8,0},{16,24},{1,9},{25,17},{9,1},{17,25},{2,10},{26... | collective-permute-start | bytes 786440 | tf_op jit(solution)/shard_map/ppermute | solution.py:473
  75.6 1.2 feature.11
  76.9 2.1 %collective-permute-start.20 = (bf16[512,256]{1,0:T(8,128)(2,1)S(1)}, bf16[512,256]{1,0:T(8,128)(2,1)S(1)}, u32[]{:S(2)}, u32[]{:S(2)}) collective-permute-start(bf16[512,256]{1,0:T(8,128)(2,1)S(1)} %around.31.refs_7_), channel_id=1, source_target_pairs={{0,8},{24,16},{8,0},{16,24},{1,9},{25,17},{9,1},{17,25},{2,10},{26... | collective-permute-start | bytes 786440 | tf_op jit(solution)/shard_map/ppermute | solution.py:473
  79.0 2.7 %collective-permute-start.7 = (bf16[512,256]{1,0:T(8,128)(2,1)S(1)}, bf16[512,256]{1,0:T(8,128)(2,1)S(1)}, u32[]{:S(2)}, u32[]{:S(2)}) collective-permute-start(bf16[512,256]{1,0:T(8,128)(2,1)S(1)} %around.25.refs_6_), channel_id=1, source_target_pairs={{0,8},{24,16},{8,0},{16,24},{1,9},{25,17},{9,1},{17,25},{2,10},{26... | collective-permute-start | bytes 786440 | tf_op jit(solution)/shard_map/ppermute | solution.py:473
  82.5 2.4 %collective-permute-done.33.b_ref.refs_0_ = bf16[512,256]{1,0:T(8,128)(2,1)S(1)} collective-permute-done((bf16[512,256]{1,0:T(8,128)(2,1)S(1)}, bf16[512,256]{1,0:T(8,128)(2,1)S(1)}, u32[]{:S(2)}, u32[]{:S(2)}) %collective-permute-start.33) | collective-permute-done | bytes 262176 | tf_op jit(solution)/shard_map/ppermute | solution.py:473
  85.6 4.9 %collective-permute-done.20.b_ref.refs_3_ = bf16[512,256]{1,0:T(8,128)(2,1)S(1)} collective-permute-done((bf16[512,256]{1,0:T(8,128)(2,1)S(1)}, bf16[512,256]{1,0:T(8,128)(2,1)S(1)}, u32[]{:S(2)}, u32[]{:S(2)}) %collective-permute-start.20) | collective-permute-done | bytes 262176 | tf_op jit(solution)/shard_map/ppermute | solution.py:473
  91.2 2.6 %collective-permute-done.7.b_ref.refs_2_ = bf16[512,256]{1,0:T(8,128)(2,1)S(1)} collective-permute-done((bf16[512,256]{1,0:T(8,128)(2,1)S(1)}, bf16[512,256]{1,0:T(8,128)(2,1)S(1)}, u32[]{:S(2)}, u32[]{:S(2)}) %collective-permute-start.7) | collective-permute-done | bytes 262176 | tf_op jit(solution)/shard_map/ppermute | solution.py:473
  94.6 4.4 %collective-permute-start.48 = (bf16[512,256]{1,0:T(8,128)(2,1)S(1)}, bf16[512,256]{1,0:T(8,128)(2,1)S(1)}, u32[]{:S(2)}, u32[]{:S(2)}) collective-permute-start(bf16[512,256]{1,0:T(8,128)(2,1)S(1)} %around.44.refs_5_), channel_id=1, source_target_pairs={{0,8},{24,16},{8,0},{16,24},{1,9},{25,17},{9,1},{17,25},{2,10},{26... | collective-permute-start | bytes 786440 | tf_op jit(solution)/shard_map/ppermute | solution.py:473
  99.2 5.1 %collective-permute-start.22 = (bf16[512,256]{1,0:T(8,128)(2,1)S(1)}, bf16[512,256]{1,0:T(8,128)(2,1)S(1)}, u32[]{:S(2)}, u32[]{:S(2)}) collective-permute-start(bf16[512,256]{1,0:T(8,128)(2,1)S(1)} %around.32.refs_7_), channel_id=1, source_target_pairs={{0,8},{24,16},{8,0},{16,24},{1,9},{25,17},{9,1},{17,25},{2,10},{26... | collective-permute-start | bytes 786440 | tf_op jit(solution)/shard_map/ppermute | solution.py:473
  104.3 3.8 %collective-permute-start.9 = (bf16[512,256]{1,0:T(8,128)(2,1)S(1)}, bf16[512,256]{1,0:T(8,128)(2,1)S(1)}, u32[]{:S(2)}, u32[]{:S(2)}) collective-permute-start(bf16[512,256]{1,0:T(8,128)(2,1)S(1)} %around.26.refs_6_), channel_id=1, source_target_pairs={{0,8},{24,16},{8,0},{16,24},{1,9},{25,17},{9,1},{17,25},{2,10},{26... | collective-permute-start | bytes 786440 | tf_op jit(solution)/shard_map/ppermute | solution.py:473
  108.9 2.9 %collective-permute-done.35.b_ref.refs_0_ = bf16[512,256]{1,0:T(8,128)(2,1)S(1)} collective-permute-done((bf16[512,256]{1,0:T(8,128)(2,1)S(1)}, bf16[512,256]{1,0:T(8,128)(2,1)S(1)}, u32[]{:S(2)}, u32[]{:S(2)}) %collective-permute-start.35) | collective-permute-done | bytes 262176 | tf_op jit(solution)/shard_map/ppermute | solution.py:473
  112.7 1.5 collective-permute-start.1
  114.3 1.8 collective-permute-done.22.b_ref.refs_3_
  116.8 2.1 %collective-permute-done.9.b_ref.refs_2_ = bf16[512,256]{1,0:T(8,128)(2,1)S(1)} collective-permute-done((bf16[512,256]{1,0:T(8,128)(2,1)S(1)}, bf16[512,256]{1,0:T(8,128)(2,1)S(1)}, u32[]{:S(2)}, u32[]{:S(2)}) %collective-permute-start.9) | collective-permute-done | bytes 262176 | tf_op jit(solution)/shard_map/ppermute | solution.py:473
  119.6 5.3 %collective-permute-start.50 = (bf16[512,256]{1,0:T(8,128)(2,1)S(1)}, bf16[512,256]{1,0:T(8,128)(2,1)S(1)}, u32[]{:S(2)}, u32[]{:S(2)}) collective-permute-start(bf16[512,256]{1,0:T(8,128)(2,1)S(1)} %around.45.refs_5_), channel_id=1, source_target_pairs={{0,8},{24,16},{8,0},{16,24},{1,9},{25,17},{9,1},{17,25},{2,10},{26... | collective-permute-start | bytes 786440 | tf_op jit(solution)/shard_map/ppermute | solution.py:473
  125.1 5.6 %collective-permute-start.24 = (bf16[512,256]{1,0:T(8,128)(2,1)S(1)}, bf16[512,256]{1,0:T(8,128)(2,1)S(1)}, u32[]{:S(2)}, u32[]{:S(2)}) collective-permute-start(bf16[512,256]{1,0:T(8,128)(2,1)S(1)} %around.33.refs_7_), channel_id=1, source_target_pairs={{0,8},{24,16},{8,0},{16,24},{1,9},{25,17},{9,1},{17,25},{2,10},{26... | collective-permute-start | bytes 786440 | tf_op jit(solution)/shard_map/ppermute | solution.py:473
  130.7 3.0 %collective-permute-start.11 = (bf16[512,256]{1,0:T(8,128)(2,1)S(1)}, bf16[512,256]{1,0:T(8,128)(2,1)S(1)}, u32[]{:S(2)}, u32[]{:S(2)}) collective-permute-start(bf16[512,256]{1,0:T(8,128)(2,1)S(1)} %around.27.refs_6_), channel_id=1, source_target_pairs={{0,8},{24,16},{8,0},{16,24},{1,9},{25,17},{9,1},{17,25},{2,10},{26... | collective-permute-start | bytes 786440 | tf_op jit(solution)/shard_map/ppermute | solution.py:473
  134.4 3.3 %collective-permute-done.37.b_ref.refs_0_ = bf16[512,256]{1,0:T(8,128)(2,1)S(1)} collective-permute-done((bf16[512,256]{1,0:T(8,128)(2,1)S(1)}, bf16[512,256]{1,0:T(8,128)(2,1)S(1)}, u32[]{:S(2)}, u32[]{:S(2)}) %collective-permute-start.37) | collective-permute-done | bytes 262176 | tf_op jit(solution)/shard_map/ppermute | solution.py:473
  138.4 2.4 %collective-permute-done.24.b_ref.refs_3_ = bf16[512,256]{1,0:T(8,128)(2,1)S(1)} collective-permute-done((bf16[512,256]{1,0:T(8,128)(2,1)S(1)}, bf16[512,256]{1,0:T(8,128)(2,1)S(1)}, u32[]{:S(2)}, u32[]{:S(2)}) %collective-permute-start.24) | collective-permute-done | bytes 262176 | tf_op jit(solution)/shard_map/ppermute | solution.py:473
  141.6 2.1 %collective-permute-done.11.b_ref.refs_2_ = bf16[512,256]{1,0:T(8,128)(2,1)S(1)} collective-permute-done((bf16[512,256]{1,0:T(8,128)(2,1)S(1)}, bf16[512,256]{1,0:T(8,128)(2,1)S(1)}, u32[]{:S(2)}, u32[]{:S(2)}) %collective-permute-start.11) | collective-permute-done | bytes 262176 | tf_op jit(solution)/shard_map/ppermute | solution.py:473
  144.5 6.1 %collective-permute-start.55 = (bf16[8,3072]{1,0:T(8,128)(2,1)S(1)}, bf16[8,3072]{1,0:T(8,128)(2,1)S(1)}, u32[]{:S(2)}, u32[]{:S(2)}) collective-permute-start(bf16[8,3072]{1,0:T(8,128)(2,1)S(1)} %gather.1.a_ref), channel_id=1, source_target_pairs={{0,8},{24,16},{1,9},{25,17},{2,10},{26,18},{3,11},{27,19},{4,12},{... | collective-permute-start | bytes 147464 | tf_op jit(solution)/shard_map/ppermute | solution.py:455
  150.9 2.0 collective-permute-start.39
  153.2 5.0 %collective-permute-start.26 = (bf16[512,256]{1,0:T(8,128)(2,1)S(1)}, bf16[512,256]{1,0:T(8,128)(2,1)S(1)}, u32[]{:S(2)}, u32[]{:S(2)}) collective-permute-start(bf16[512,256]{1,0:T(8,128)(2,1)S(1)} %around.34.refs_7_), channel_id=1, source_target_pairs={{0,8},{24,16},{8,0},{16,24},{1,9},{25,17},{9,1},{17,25},{2,10},{26... | collective-permute-start | bytes 786440 | tf_op jit(solution)/shard_map/ppermute | solution.py:473
  159.3 3.5 %collective-permute-done.39.b_ref.refs_0_ = bf16[512,256]{1,0:T(8,128)(2,1)S(1)} collective-permute-done((bf16[512,256]{1,0:T(8,128)(2,1)S(1)}, bf16[512,256]{1,0:T(8,128)(2,1)S(1)}, u32[]{:S(2)}, u32[]{:S(2)}) %collective-permute-start.39) | collective-permute-done | bytes 262176 | tf_op jit(solution)/shard_map/ppermute | solution.py:473
  163.5 4.7 %collective-permute-done.26.b_ref.refs_3_ = bf16[512,256]{1,0:T(8,128)(2,1)S(1)} collective-permute-done((bf16[512,256]{1,0:T(8,128)(2,1)S(1)}, bf16[512,256]{1,0:T(8,128)(2,1)S(1)}, u32[]{:S(2)}, u32[]{:S(2)}) %collective-permute-start.26) | collective-permute-done | bytes 262176 | tf_op jit(solution)/shard_map/ppermute | solution.py:473
  169.0 2.1 %collective-permute-done.13.b_ref.refs_2_ = bf16[512,256]{1,0:T(8,128)(2,1)S(1)} collective-permute-done((bf16[512,256]{1,0:T(8,128)(2,1)S(1)}, bf16[512,256]{1,0:T(8,128)(2,1)S(1)}, u32[]{:S(2)}, u32[]{:S(2)}) %collective-permute-start.13) | collective-permute-done | bytes 262176 | tf_op jit(solution)/shard_map/ppermute | solution.py:473
  172.6 1.3 collective-permute-start.57
  173.9 6.2 %collective-permute-start.54 = (bf16[512,256]{1,0:T(8,128)(2,1)S(1)}, bf16[512,256]{1,0:T(8,128)(2,1)S(1)}, u32[]{:S(2)}, u32[]{:S(2)}) collective-permute-start(bf16[512,256]{1,0:T(8,128)(2,1)S(1)} %around.47.refs_3_), channel_id=1, source_target_pairs={{0,8},{24,16},{8,0},{16,24},{1,9},{25,17},{9,1},{17,25},{2,10},{26... | collective-permute-start | bytes 786440 | tf_op jit(solution)/shard_map/ppermute | solution.py:473
  180.1 1.3 collective-permute-start.41
  181.5 7.0 %collective-permute-start.28 = (bf16[512,256]{1,0:T(8,128)(2,1)S(1)}, bf16[512,256]{1,0:T(8,128)(2,1)S(1)}, u32[]{:S(2)}, u32[]{:S(2)}) collective-permute-start(bf16[512,256]{1,0:T(8,128)(2,1)S(1)} %around.35.refs_3_), channel_id=1, source_target_pairs={{0,8},{24,16},{8,0},{16,24},{1,9},{25,17},{9,1},{17,25},{2,10},{26... | collective-permute-start | bytes 786440 | tf_op jit(solution)/shard_map/ppermute | solution.py:473
  189.3 1.5 store.7
  190.8 1.5 store.8
  192.3 1.5 store.9
  193.7 1.5 store.10
  195.2 1.3 join.1
  196.5 1.5 store.11
  198.0 1.1 store.12
  199.0 2.3 %collective-permute-done.15.refs_0_ = bf16[512,256]{1,0:T(8,128)(2,1)S(1)} collective-permute-done((bf16[512,256]{1,0:T(8,128)(2,1)S(1)}, bf16[512,256]{1,0:T(8,128)(2,1)S(1)}, u32[]{:S(2)}, u32[]{:S(2)}) %collective-permute-start.15) | collective-permute-done | bytes 262176 | tf_op jit(solution)/shard_map/ppermute | solution.py:473
  (145 shorter events, 26.9 us)
Async XLA Ops:
  4.2 4.6 %copy-start.2 = (f32[3,1536]{1,0:T(4,128)S(1)}, f32[3,1536]{1,0:T(4,128)}, u32[]{:S(2)}) copy-start(f32[3,1536]{1,0:T(4,128)} %refs_7_.25) | copy-start | bytes 55300
  4.2 4.5 %copy-start.3 = (f32[3,1536]{1,0:T(4,128)S(1)}, f32[3,1536]{1,0:T(4,128)}, u32[]{:S(2)}) copy-start(f32[3,1536]{1,0:T(4,128)} %refs_8_.21) | copy-start | bytes 55300
  4.2 4.5 %copy-start.4 = (f32[1536]{0:T(1024)S(1)}, f32[1536]{0:T(1024)}, u32[]{:S(2)}) copy-start(f32[1536]{0:T(1024)} %refs_9_.21) | copy-start | bytes 18436
  4.2 4.5 %copy-start.5 = (f32[1536]{0:T(1024)S(1)}, f32[1536]{0:T(1024)}, u32[]{:S(2)}) copy-start(f32[1536]{0:T(1024)} %refs_10_.21) | copy-start | bytes 18436
  4.2 11.5 %collective-permute-start.29 = (bf16[512,256]{1,0:T(8,128)(2,1)S(1)}, bf16[512,256]{1,0:T(8,128)(2,1)S(1)}, u32[]{:S(2)}, u32[]{:S(2)}) collective-permute-start(bf16[512,256]{1,0:T(8,128)(2,1)S(1)} %get-tuple-element.215), channel_id=1, source_target_pairs={{0,8},{24,16},{1,9},{25,17},{2,10},{26,18},{3,11},{27,19},{4,12},{... | collective-permute-start | bytes 786440 | tf_op jit(solution)/shard_map/ppermute | solution.py:473
  6.6 12.3 %collective-permute-start.42 = (bf16[512,256]{1,0:T(8,128)(2,1)S(1)}, bf16[512,256]{1,0:T(8,128)(2,1)S(1)}, u32[]{:S(2)}, u32[]{:S(2)}) collective-permute-start(bf16[512,256]{1,0:T(8,128)(2,1)S(1)} %get-tuple-element.222), channel_id=1, source_target_pairs={{0,8},{24,16},{1,9},{25,17},{2,10},{26,18},{3,11},{27,19},{4,12},{... | collective-permute-start | bytes 786440 | tf_op jit(solution)/shard_map/ppermute | solution.py:473
  10.4 14.1 %collective-permute-start.16 = (bf16[512,256]{1,0:T(8,128)(2,1)S(1)}, bf16[512,256]{1,0:T(8,128)(2,1)S(1)}, u32[]{:S(2)}, u32[]{:S(2)}) collective-permute-start(bf16[512,256]{1,0:T(8,128)(2,1)S(1)} %get-tuple-element.208.a_ref), channel_id=1, source_target_pairs={{0,8},{24,16},{1,9},{25,17},{2,10},{26,18},{3,11},{27,19},{4,12},{... | collective-permute-start | bytes 786440 | tf_op jit(solution)/shard_map/ppermute | solution.py:473
  14.4 14.6 %collective-permute-start.3 = (bf16[512,256]{1,0:T(8,128)(2,1)S(1)}, bf16[512,256]{1,0:T(8,128)(2,1)S(1)}, u32[]{:S(2)}, u32[]{:S(2)}) collective-permute-start(bf16[512,256]{1,0:T(8,128)(2,1)S(1)} %get-tuple-element.202.a_ref), channel_id=1, source_target_pairs={{0,8},{24,16},{1,9},{25,17},{2,10},{26,18},{3,11},{27,19},{4,12},{... | collective-permute-start | bytes 786440 | tf_op jit(solution)/shard_map/ppermute | solution.py:473
  15.8 20.4 %collective-permute-start.30 = (bf16[512,256]{1,0:T(8,128)(2,1)S(1)}, bf16[512,256]{1,0:T(8,128)(2,1)S(1)}, u32[]{:S(2)}, u32[]{:S(2)}) collective-permute-start(bf16[512,256]{1,0:T(8,128)(2,1)S(1)} %add.42.pair_ref), channel_id=1, source_target_pairs={{8,16},{16,8},{9,17},{17,9},{10,18},{18,10},{11,19},{19,11},{12,20... | collective-permute-start | bytes 786440 | tf_op jit(solution)/shard_map/ppermute | solution.py:477
  19.0 24.7 %collective-permute-start.43 = (bf16[512,256]{1,0:T(8,128)(2,1)S(1)}, bf16[512,256]{1,0:T(8,128)(2,1)S(1)}, u32[]{:S(2)}, u32[]{:S(2)}) collective-permute-start(bf16[512,256]{1,0:T(8,128)(2,1)S(1)} %add.48.pair_ref), channel_id=1, source_target_pairs={{8,16},{16,8},{9,17},{17,9},{10,18},{18,10},{11,19},{19,11},{12,20... | collective-permute-start | bytes 786440 | tf_op jit(solution)/shard_map/ppermute | solution.py:477
  24.6 24.1 %collective-permute-start.17 = (bf16[512,256]{1,0:T(8,128)(2,1)S(1)}, bf16[512,256]{1,0:T(8,128)(2,1)S(1)}, u32[]{:S(2)}, u32[]{:S(2)}) collective-permute-start(bf16[512,256]{1,0:T(8,128)(2,1)S(1)} %add.36.pair_ref), channel_id=1, source_target_pairs={{8,16},{16,8},{9,17},{17,9},{10,18},{18,10},{11,19},{19,11},{12,20... | collective-permute-start | bytes 786440 | tf_op jit(solution)/shard_map/ppermute | solution.py:477
  29.1 21.7 %collective-permute-start.4 = (bf16[512,256]{1,0:T(8,128)(2,1)S(1)}, bf16[512,256]{1,0:T(8,128)(2,1)S(1)}, u32[]{:S(2)}, u32[]{:S(2)}) collective-permute-start(bf16[512,256]{1,0:T(8,128)(2,1)S(1)} %add.30.pair_ref), channel_id=1, source_target_pairs={{8,16},{16,8},{9,17},{17,9},{10,18},{18,10},{11,19},{19,11},{12,20... | collective-permute-start | bytes 786440 | tf_op jit(solution)/shard_map/ppermute | solution.py:477
  36.3 20.9 %collective-permute-start.31 = (bf16[512,256]{1,0:T(8,128)(2,1)S(1)}, bf16[512,256]{1,0:T(8,128)(2,1)S(1)}, u32[]{:S(2)}, u32[]{:S(2)}) collective-permute-start(bf16[512,256]{1,0:T(8,128)(2,1)S(1)} %around.36.refs_4_), channel_id=1, source_target_pairs={{0,8},{24,16},{8,0},{16,24},{1,9},{25,17},{9,1},{17,25},{2,10},{26... | collective-permute-start | bytes 786440 | tf_op jit(solution)/shard_map/ppermute | solution.py:473
  43.6 12.7 %collective-permute-start.44 = (bf16[512,256]{1,0:T(8,128)(2,1)S(1)}, bf16[512,256]{1,0:T(8,128)(2,1)S(1)}, u32[]{:S(2)}, u32[]{:S(2)}) collective-permute-start(bf16[512,256]{1,0:T(8,128)(2,1)S(1)} %around.42.refs_5_), channel_id=1, source_target_pairs={{0,8},{24,16},{8,0},{16,24},{1,9},{25,17},{9,1},{17,25},{2,10},{26... | collective-permute-start | bytes 786440 | tf_op jit(solution)/shard_map/ppermute | solution.py:473
  47.0 4.1 %copy-start = (bf16[1024,1536]{1,0:T(8,128)(2,1)S(1)}, bf16[1024,1536]{1,0:T(8,128)(2,1)}, u32[]{:S(2)}) copy-start(bf16[1024,1536]{1,0:T(8,128)(2,1)} %refs_2_.37) | copy-start | bytes 9437188
  47.0 4.1 %copy-start.1 = (bf16[1024,1536]{1,0:T(8,128)(2,1)S(1)}, bf16[1024,1536]{1,0:T(8,128)(2,1)}, u32[]{:S(2)}) copy-start(bf16[1024,1536]{1,0:T(8,128)(2,1)} %refs_3_.37) | copy-start | bytes 9437188
  48.7 13.3 %collective-permute-start.18 = (bf16[512,256]{1,0:T(8,128)(2,1)S(1)}, bf16[512,256]{1,0:T(8,128)(2,1)S(1)}, u32[]{:S(2)}, u32[]{:S(2)}) collective-permute-start(bf16[512,256]{1,0:T(8,128)(2,1)S(1)} %around.30.refs_7_), channel_id=1, source_target_pairs={{0,8},{24,16},{8,0},{16,24},{1,9},{25,17},{9,1},{17,25},{2,10},{26... | collective-permute-start | bytes 786440 | tf_op jit(solution)/shard_map/ppermute | solution.py:473
  51.0 14.9 %collective-permute-start.5 = (bf16[512,256]{1,0:T(8,128)(2,1)S(1)}, bf16[512,256]{1,0:T(8,128)(2,1)S(1)}, u32[]{:S(2)}, u32[]{:S(2)}) collective-permute-start(bf16[512,256]{1,0:T(8,128)(2,1)S(1)} %around.24.refs_6_), channel_id=1, source_target_pairs={{0,8},{24,16},{8,0},{16,24},{1,9},{25,17},{9,1},{17,25},{2,10},{26... | collective-permute-start | bytes 786440 | tf_op jit(solution)/shard_map/ppermute | solution.py:473
  56.5 12.3 %collective-permute-start.45 = (bf16[512,256]{1,0:T(8,128)(2,1)S(1)}, bf16[512,256]{1,0:T(8,128)(2,1)S(1)}, u32[]{:S(2)}, u32[]{:S(2)}) collective-permute-start(bf16[512,256]{1,0:T(8,128)(2,1)S(1)} %add.49.pair_ref), channel_id=1, source_target_pairs={{8,16},{16,8},{9,17},{17,9},{10,18},{18,10},{11,19},{19,11},{12,20... | collective-permute-start | bytes 786440 | tf_op jit(solution)/shard_map/ppermute | solution.py:477
  57.2 18.2 %collective-permute-start.32 = (bf16[512,256]{1,0:T(8,128)(2,1)S(1)}, bf16[512,256]{1,0:T(8,128)(2,1)S(1)}, u32[]{:S(2)}, u32[]{:S(2)}) collective-permute-start(bf16[512,256]{1,0:T(8,128)(2,1)S(1)} %add.43.pair_ref), channel_id=1, source_target_pairs={{8,16},{16,8},{9,17},{17,9},{10,18},{18,10},{11,19},{19,11},{12,20... | collective-permute-start | bytes 786440 | tf_op jit(solution)/shard_map/ppermute | solution.py:477
  62.1 14.8 %collective-permute-start.19 = (bf16[512,256]{1,0:T(8,128)(2,1)S(1)}, bf16[512,256]{1,0:T(8,128)(2,1)S(1)}, u32[]{:S(2)}, u32[]{:S(2)}) collective-permute-start(bf16[512,256]{1,0:T(8,128)(2,1)S(1)} %add.37.pair_ref), channel_id=1, source_target_pairs={{8,16},{16,8},{9,17},{17,9},{10,18},{18,10},{11,19},{19,11},{12,20... | collective-permute-start | bytes 786440 | tf_op jit(solution)/shard_map/ppermute | solution.py:477
  66.0 13.0 %collective-permute-start.6 = (bf16[512,256]{1,0:T(8,128)(2,1)S(1)}, bf16[512,256]{1,0:T(8,128)(2,1)S(1)}, u32[]{:S(2)}, u32[]{:S(2)}) collective-permute-start(bf16[512,256]{1,0:T(8,128)(2,1)S(1)} %add.31.pair_ref), channel_id=1, source_target_pairs={{8,16},{16,8},{9,17},{17,9},{10,18},{18,10},{11,19},{19,11},{12,20... | collective-permute-start | bytes 786440 | tf_op jit(solution)/shard_map/ppermute | solution.py:477
  68.8 12.9 %collective-permute-start.46 = (bf16[512,256]{1,0:T(8,128)(2,1)S(1)}, bf16[512,256]{1,0:T(8,128)(2,1)S(1)}, u32[]{:S(2)}, u32[]{:S(2)}) collective-permute-start(bf16[512,256]{1,0:T(8,128)(2,1)S(1)} %around.43.refs_5_), channel_id=1, source_target_pairs={{0,8},{24,16},{8,0},{16,24},{1,9},{25,17},{9,1},{17,25},{2,10},{26... | collective-permute-start | bytes 786440 | tf_op jit(solution)/shard_map/ppermute | solution.py:473
  75.4 9.4 %collective-permute-start.33 = (bf16[512,256]{1,0:T(8,128)(2,1)S(1)}, bf16[512,256]{1,0:T(8,128)(2,1)S(1)}, u32[]{:S(2)}, u32[]{:S(2)}) collective-permute-start(bf16[512,256]{1,0:T(8,128)(2,1)S(1)} %around.37.refs_4_), channel_id=1, source_target_pairs={{0,8},{24,16},{8,0},{16,24},{1,9},{25,17},{9,1},{17,25},{2,10},{26... | collective-permute-start | bytes 786440 | tf_op jit(solution)/shard_map/ppermute | solution.py:473
  76.8 35.8 %collective-permute-start = (bf16[768,512]{1,0:T(8,128)(2,1)S(1)}, bf16[768,512]{1,0:T(8,128)(2,1)S(1)}, u32[]{:S(2)}, u32[]{:S(2)}) collective-permute-start(bf16[768,512]{1,0:T(8,128)(2,1)S(1)} %get-tuple-element.196), channel_id=1, source_target_pairs={{0,1},{1,0},{2,3},{3,2},{4,5},{5,4},{6,7},{7,6},{8,9},{9,8},{10,11... | collective-permute-start | bytes 2359304 | tf_op jit(solution)/shard_map/ppermute | solution.py:493
  76.9 13.6 %collective-permute-start.20 = (bf16[512,256]{1,0:T(8,128)(2,1)S(1)}, bf16[512,256]{1,0:T(8,128)(2,1)S(1)}, u32[]{:S(2)}, u32[]{:S(2)}) collective-permute-start(bf16[512,256]{1,0:T(8,128)(2,1)S(1)} %around.31.refs_7_), channel_id=1, source_target_pairs={{0,8},{24,16},{8,0},{16,24},{1,9},{25,17},{9,1},{17,25},{2,10},{26... | collective-permute-start | bytes 786440 | tf_op jit(solution)/shard_map/ppermute | solution.py:473
  79.0 14.8 %collective-permute-start.7 = (bf16[512,256]{1,0:T(8,128)(2,1)S(1)}, bf16[512,256]{1,0:T(8,128)(2,1)S(1)}, u32[]{:S(2)}, u32[]{:S(2)}) collective-permute-start(bf16[512,256]{1,0:T(8,128)(2,1)S(1)} %around.25.refs_6_), channel_id=1, source_target_pairs={{0,8},{24,16},{8,0},{16,24},{1,9},{25,17},{9,1},{17,25},{2,10},{26... | collective-permute-start | bytes 786440 | tf_op jit(solution)/shard_map/ppermute | solution.py:473
  81.8 12.8 %collective-permute-start.47 = (bf16[512,256]{1,0:T(8,128)(2,1)S(1)}, bf16[512,256]{1,0:T(8,128)(2,1)S(1)}, u32[]{:S(2)}, u32[]{:S(2)}) collective-permute-start(bf16[512,256]{1,0:T(8,128)(2,1)S(1)} %add.50.pair_ref), channel_id=1, source_target_pairs={{8,16},{16,8},{9,17},{17,9},{10,18},{18,10},{11,19},{19,11},{12,20... | collective-permute-start | bytes 786440 | tf_op jit(solution)/shard_map/ppermute | solution.py:477
  84.9 14.1 %collective-permute-start.34 = (bf16[512,256]{1,0:T(8,128)(2,1)S(1)}, bf16[512,256]{1,0:T(8,128)(2,1)S(1)}, u32[]{:S(2)}, u32[]{:S(2)}) collective-permute-start(bf16[512,256]{1,0:T(8,128)(2,1)S(1)} %add.44.pair_ref), channel_id=1, source_target_pairs={{8,16},{16,8},{9,17},{17,9},{10,18},{18,10},{11,19},{19,11},{12,20... | collective-permute-start | bytes 786440 | tf_op jit(solution)/shard_map/ppermute | solution.py:477
  90.5 8.7 %collective-permute-start.21 = (bf16[512,256]{1,0:T(8,128)(2,1)S(1)}, bf16[512,256]{1,0:T(8,128)(2,1)S(1)}, u32[]{:S(2)}, u32[]{:S(2)}) collective-permute-start(bf16[512,256]{1,0:T(8,128)(2,1)S(1)} %add.38.pair_ref), channel_id=1, source_target_pairs={{8,16},{16,8},{9,17},{17,9},{10,18},{18,10},{11,19},{19,11},{12,20... | collective-permute-start | bytes 786440 | tf_op jit(solution)/shard_map/ppermute | solution.py:477
  93.9 10.4 %collective-permute-start.8 = (bf16[512,256]{1,0:T(8,128)(2,1)S(1)}, bf16[512,256]{1,0:T(8,128)(2,1)S(1)}, u32[]{:S(2)}, u32[]{:S(2)}) collective-permute-start(bf16[512,256]{1,0:T(8,128)(2,1)S(1)} %add.32.pair_ref), channel_id=1, source_target_pairs={{8,16},{16,8},{9,17},{17,9},{10,18},{18,10},{11,19},{19,11},{12,20... | collective-permute-start | bytes 786440 | tf_op jit(solution)/shard_map/ppermute | solution.py:477
  94.6 13.5 %collective-permute-start.48 = (bf16[512,256]{1,0:T(8,128)(2,1)S(1)}, bf16[512,256]{1,0:T(8,128)(2,1)S(1)}, u32[]{:S(2)}, u32[]{:S(2)}) collective-permute-start(bf16[512,256]{1,0:T(8,128)(2,1)S(1)} %around.44.refs_5_), channel_id=1, source_target_pairs={{0,8},{24,16},{8,0},{16,24},{1,9},{25,17},{9,1},{17,25},{2,10},{26... | collective-permute-start | bytes 786440 | tf_op jit(solution)/shard_map/ppermute | solution.py:473
  99.0 12.7 %collective-permute-start.35 = (bf16[512,256]{1,0:T(8,128)(2,1)S(1)}, bf16[512,256]{1,0:T(8,128)(2,1)S(1)}, u32[]{:S(2)}, u32[]{:S(2)}) collective-permute-start(bf16[512,256]{1,0:T(8,128)(2,1)S(1)} %around.38.refs_4_), channel_id=1, source_target_pairs={{0,8},{24,16},{8,0},{16,24},{1,9},{25,17},{9,1},{17,25},{2,10},{26... | collective-permute-start | bytes 786440 | tf_op jit(solution)/shard_map/ppermute | solution.py:473
  99.2 16.8 %collective-permute-start.22 = (bf16[512,256]{1,0:T(8,128)(2,1)S(1)}, bf16[512,256]{1,0:T(8,128)(2,1)S(1)}, u32[]{:S(2)}, u32[]{:S(2)}) collective-permute-start(bf16[512,256]{1,0:T(8,128)(2,1)S(1)} %around.32.refs_7_), channel_id=1, source_target_pairs={{0,8},{24,16},{8,0},{16,24},{1,9},{25,17},{9,1},{17,25},{2,10},{26... | collective-permute-start | bytes 786440 | tf_op jit(solution)/shard_map/ppermute | solution.py:473
  104.3 14.5 %collective-permute-start.9 = (bf16[512,256]{1,0:T(8,128)(2,1)S(1)}, bf16[512,256]{1,0:T(8,128)(2,1)S(1)}, u32[]{:S(2)}, u32[]{:S(2)}) collective-permute-start(bf16[512,256]{1,0:T(8,128)(2,1)S(1)} %around.26.refs_6_), channel_id=1, source_target_pairs={{0,8},{24,16},{8,0},{16,24},{1,9},{25,17},{9,1},{17,25},{2,10},{26... | collective-permute-start | bytes 786440 | tf_op jit(solution)/shard_map/ppermute | solution.py:473
  108.2 11.4 %collective-permute-start.49 = (bf16[512,256]{1,0:T(8,128)(2,1)S(1)}, bf16[512,256]{1,0:T(8,128)(2,1)S(1)}, u32[]{:S(2)}, u32[]{:S(2)}) collective-permute-start(bf16[512,256]{1,0:T(8,128)(2,1)S(1)} %add.51.pair_ref), channel_id=1, source_target_pairs={{8,16},{16,8},{9,17},{17,9},{10,18},{18,10},{11,19},{19,11},{12,20... | collective-permute-start | bytes 786440 | tf_op jit(solution)/shard_map/ppermute | solution.py:477
  111.8 13.1 %collective-permute-start.36 = (bf16[512,256]{1,0:T(8,128)(2,1)S(1)}, bf16[512,256]{1,0:T(8,128)(2,1)S(1)}, u32[]{:S(2)}, u32[]{:S(2)}) collective-permute-start(bf16[512,256]{1,0:T(8,128)(2,1)S(1)} %add.45.pair_ref), channel_id=1, source_target_pairs={{8,16},{16,8},{9,17},{17,9},{10,18},{18,10},{11,19},{19,11},{12,20... | collective-permute-start | bytes 786440 | tf_op jit(solution)/shard_map/ppermute | solution.py:477
  112.7 38.1 %collective-permute-start.1 = (bf16[768,512]{1,0:T(8,128)(2,1)S(1)}, bf16[768,512]{1,0:T(8,128)(2,1)S(1)}, u32[]{:S(2)}, u32[]{:S(2)}) collective-permute-start(bf16[768,512]{1,0:T(8,128)(2,1)S(1)} %add.28.a_ref), channel_id=1, source_target_pairs={{0,2},{2,0},{1,3},{3,1},{4,6},{6,4},{5,7},{7,5},{8,10},{10,8},{9,1... | collective-permute-start | bytes 2359304 | tf_op jit(solution)/shard_map/ppermute | solution.py:495
  116.1 9.0 %collective-permute-start.23 = (bf16[512,256]{1,0:T(8,128)(2,1)S(1)}, bf16[512,256]{1,0:T(8,128)(2,1)S(1)}, u32[]{:S(2)}, u32[]{:S(2)}) collective-permute-start(bf16[512,256]{1,0:T(8,128)(2,1)S(1)} %add.39.pair_ref), channel_id=1, source_target_pairs={{8,16},{16,8},{9,17},{17,9},{10,18},{18,10},{11,19},{19,11},{12,20... | collective-permute-start | bytes 786440 | tf_op jit(solution)/shard_map/ppermute | solution.py:477
  118.9 11.8 %collective-permute-start.10 = (bf16[512,256]{1,0:T(8,128)(2,1)S(1)}, bf16[512,256]{1,0:T(8,128)(2,1)S(1)}, u32[]{:S(2)}, u32[]{:S(2)}) collective-permute-start(bf16[512,256]{1,0:T(8,128)(2,1)S(1)} %add.33.pair_ref), channel_id=1, source_target_pairs={{8,16},{16,8},{9,17},{17,9},{10,18},{18,10},{11,19},{19,11},{12,20... | collective-permute-start | bytes 786440 | tf_op jit(solution)/shard_map/ppermute | solution.py:477
  119.6 14.0 %collective-permute-start.50 = (bf16[512,256]{1,0:T(8,128)(2,1)S(1)}, bf16[512,256]{1,0:T(8,128)(2,1)S(1)}, u32[]{:S(2)}, u32[]{:S(2)}) collective-permute-start(bf16[512,256]{1,0:T(8,128)(2,1)S(1)} %around.45.refs_5_), channel_id=1, source_target_pairs={{0,8},{24,16},{8,0},{16,24},{1,9},{25,17},{9,1},{17,25},{2,10},{26... | collective-permute-start | bytes 786440 | tf_op jit(solution)/shard_map/ppermute | solution.py:473
  124.9 12.7 %collective-permute-start.37 = (bf16[512,256]{1,0:T(8,128)(2,1)S(1)}, bf16[512,256]{1,0:T(8,128)(2,1)S(1)}, u32[]{:S(2)}, u32[]{:S(2)}) collective-permute-start(bf16[512,256]{1,0:T(8,128)(2,1)S(1)} %around.39.refs_4_), channel_id=1, source_target_pairs={{0,8},{24,16},{8,0},{16,24},{1,9},{25,17},{9,1},{17,25},{2,10},{26... | collective-permute-start | bytes 786440 | tf_op jit(solution)/shard_map/ppermute | solution.py:473
  125.1 15.7 %collective-permute-start.24 = (bf16[512,256]{1,0:T(8,128)(2,1)S(1)}, bf16[512,256]{1,0:T(8,128)(2,1)S(1)}, u32[]{:S(2)}, u32[]{:S(2)}) collective-permute-start(bf16[512,256]{1,0:T(8,128)(2,1)S(1)} %around.33.refs_7_), channel_id=1, source_target_pairs={{0,8},{24,16},{8,0},{16,24},{1,9},{25,17},{9,1},{17,25},{2,10},{26... | collective-permute-start | bytes 786440 | tf_op jit(solution)/shard_map/ppermute | solution.py:473
  130.7 13.0 %collective-permute-start.11 = (bf16[512,256]{1,0:T(8,128)(2,1)S(1)}, bf16[512,256]{1,0:T(8,128)(2,1)S(1)}, u32[]{:S(2)}, u32[]{:S(2)}) collective-permute-start(bf16[512,256]{1,0:T(8,128)(2,1)S(1)} %around.27.refs_6_), channel_id=1, source_target_pairs={{0,8},{24,16},{8,0},{16,24},{1,9},{25,17},{9,1},{17,25},{2,10},{26... | collective-permute-start | bytes 786440 | tf_op jit(solution)/shard_map/ppermute | solution.py:473
  133.7 10.7 %collective-permute-start.51 = (bf16[512,256]{1,0:T(8,128)(2,1)S(1)}, bf16[512,256]{1,0:T(8,128)(2,1)S(1)}, u32[]{:S(2)}, u32[]{:S(2)}) collective-permute-start(bf16[512,256]{1,0:T(8,128)(2,1)S(1)} %add.52.pair_ref), channel_id=1, source_target_pairs={{8,16},{16,8},{9,17},{17,9},{10,18},{18,10},{11,19},{19,11},{12,20... | collective-permute-start | bytes 786440 | tf_op jit(solution)/shard_map/ppermute | solution.py:477
  137.8 12.8 %collective-permute-start.38 = (bf16[512,256]{1,0:T(8,128)(2,1)S(1)}, bf16[512,256]{1,0:T(8,128)(2,1)S(1)}, u32[]{:S(2)}, u32[]{:S(2)}) collective-permute-start(bf16[512,256]{1,0:T(8,128)(2,1)S(1)} %add.46.pair_ref), channel_id=1, source_target_pairs={{8,16},{16,8},{9,17},{17,9},{10,18},{18,10},{11,19},{19,11},{12,20... | collective-permute-start | bytes 786440 | tf_op jit(solution)/shard_map/ppermute | solution.py:477
  140.9 12.1 %collective-permute-start.25 = (bf16[512,256]{1,0:T(8,128)(2,1)S(1)}, bf16[512,256]{1,0:T(8,128)(2,1)S(1)}, u32[]{:S(2)}, u32[]{:S(2)}) collective-permute-start(bf16[512,256]{1,0:T(8,128)(2,1)S(1)} %add.40.pair_ref), channel_id=1, source_target_pairs={{8,16},{16,8},{9,17},{17,9},{10,18},{18,10},{11,19},{19,11},{12,20... | collective-permute-start | bytes 786440 | tf_op jit(solution)/shard_map/ppermute | solution.py:477
  143.7 9.4 %collective-permute-start.12 = (bf16[512,256]{1,0:T(8,128)(2,1)S(1)}, bf16[512,256]{1,0:T(8,128)(2,1)S(1)}, u32[]{:S(2)}, u32[]{:S(2)}) collective-permute-start(bf16[512,256]{1,0:T(8,128)(2,1)S(1)} %add.34.pair_ref), channel_id=1, source_target_pairs={{8,16},{16,8},{9,17},{17,9},{10,18},{18,10},{11,19},{19,11},{12,20... | collective-permute-start | bytes 786440 | tf_op jit(solution)/shard_map/ppermute | solution.py:477
  144.5 14.0 %collective-permute-start.55 = (bf16[8,3072]{1,0:T(8,128)(2,1)S(1)}, bf16[8,3072]{1,0:T(8,128)(2,1)S(1)}, u32[]{:S(2)}, u32[]{:S(2)}) collective-permute-start(bf16[8,3072]{1,0:T(8,128)(2,1)S(1)} %gather.1.a_ref), channel_id=1, source_target_pairs={{0,8},{24,16},{1,9},{25,17},{2,10},{26,18},{3,11},{27,19},{4,12},{... | collective-permute-start | bytes 147464 | tf_op jit(solution)/shard_map/ppermute | solution.py:455
  150.6 8.0 %collective-permute-start.52 = (bf16[512,256]{1,0:T(8,128)(2,1)S(1)}, bf16[512,256]{1,0:T(8,128)(2,1)S(1)}, u32[]{:S(2)}, u32[]{:S(2)}) collective-permute-start(bf16[512,256]{1,0:T(8,128)(2,1)S(1)} %around.46.refs_5_), channel_id=1, source_target_pairs={{0,8},{24,16},{8,0},{16,24},{1,9},{25,17},{9,1},{17,25},{2,10},{26... | collective-permute-start | bytes 786440 | tf_op jit(solution)/shard_map/ppermute | solution.py:473
  150.9 11.9 %collective-permute-start.39 = (bf16[512,256]{1,0:T(8,128)(2,1)S(1)}, bf16[512,256]{1,0:T(8,128)(2,1)S(1)}, u32[]{:S(2)}, u32[]{:S(2)}) collective-permute-start(bf16[512,256]{1,0:T(8,128)(2,1)S(1)} %around.40.refs_4_), channel_id=1, source_target_pairs={{0,8},{24,16},{8,0},{16,24},{1,9},{25,17},{9,1},{17,25},{2,10},{26... | collective-permute-start | bytes 786440 | tf_op jit(solution)/shard_map/ppermute | solution.py:473
  153.0 42.2 %collective-permute-start.2 = (bf16[768,512]{1,0:T(8,128)(2,1)S(1)}, bf16[768,512]{1,0:T(8,128)(2,1)S(1)}, u32[]{:S(2)}, u32[]{:S(2)}) collective-permute-start(bf16[768,512]{1,0:T(8,128)(2,1)S(1)} %add.29.own_ref), channel_id=1, source_target_pairs={{0,1},{1,0},{2,3},{3,2},{4,5},{5,4},{6,7},{7,6},{8,9},{9,8},{10,11... | collective-permute-start | bytes 2359304 | tf_op jit(solution)/shard_map/ppermute | solution.py:497
  153.2 15.1 %collective-permute-start.26 = (bf16[512,256]{1,0:T(8,128)(2,1)S(1)}, bf16[512,256]{1,0:T(8,128)(2,1)S(1)}, u32[]{:S(2)}, u32[]{:S(2)}) collective-permute-start(bf16[512,256]{1,0:T(8,128)(2,1)S(1)} %around.34.refs_7_), channel_id=1, source_target_pairs={{0,8},{24,16},{8,0},{16,24},{1,9},{25,17},{9,1},{17,25},{2,10},{26... | collective-permute-start | bytes 786440 | tf_op jit(solution)/shard_map/ppermute | solution.py:473
  158.5 12.6 %collective-permute-start.13 = (bf16[512,256]{1,0:T(8,128)(2,1)S(1)}, bf16[512,256]{1,0:T(8,128)(2,1)S(1)}, u32[]{:S(2)}, u32[]{:S(2)}) collective-permute-start(bf16[512,256]{1,0:T(8,128)(2,1)S(1)} %around.28.refs_6_), channel_id=1, source_target_pairs={{0,8},{24,16},{8,0},{16,24},{1,9},{25,17},{9,1},{17,25},{2,10},{26... | collective-permute-start | bytes 786440 | tf_op jit(solution)/shard_map/ppermute | solution.py:473
  158.6 13.2 %collective-permute-start.56 = (bf16[8,3072]{1,0:T(8,128)(2,1)S(1)}, bf16[8,3072]{1,0:T(8,128)(2,1)S(1)}, u32[]{:S(2)}, u32[]{:S(2)}) collective-permute-start(bf16[8,3072]{1,0:T(8,128)(2,1)S(1)} %add.54.a_ref), channel_id=1, source_target_pairs={{8,16},{16,8},{9,17},{17,9},{10,18},{18,10},{11,19},{19,11},{12,20... | collective-permute-start | bytes 147464 | tf_op jit(solution)/shard_map/ppermute | solution.py:457
  162.8 9.8 %collective-permute-start.53 = (bf16[512,256]{1,0:T(8,128)(2,1)S(1)}, bf16[512,256]{1,0:T(8,128)(2,1)S(1)}, u32[]{:S(2)}, u32[]{:S(2)}) collective-permute-start(bf16[512,256]{1,0:T(8,128)(2,1)S(1)} %add.53.pair_ref), channel_id=1, source_target_pairs={{8,16},{16,8},{9,17},{17,9},{10,18},{18,10},{11,19},{19,11},{12,20... | collective-permute-start | bytes 786440 | tf_op jit(solution)/shard_map/ppermute | solution.py:477
  168.3 5.6 %collective-permute-start.40 = (bf16[512,256]{1,0:T(8,128)(2,1)S(1)}, bf16[512,256]{1,0:T(8,128)(2,1)S(1)}, u32[]{:S(2)}, u32[]{:S(2)}) collective-permute-start(bf16[512,256]{1,0:T(8,128)(2,1)S(1)} %add.47.pair_ref), channel_id=1, source_target_pairs={{8,16},{16,8},{9,17},{17,9},{10,18},{18,10},{11,19},{19,11},{12,20... | collective-permute-start | bytes 786440 | tf_op jit(solution)/shard_map/ppermute | solution.py:477
  171.1 9.0 %collective-permute-start.27 = (bf16[512,256]{1,0:T(8,128)(2,1)S(1)}, bf16[512,256]{1,0:T(8,128)(2,1)S(1)}, u32[]{:S(2)}, u32[]{:S(2)}) collective-permute-start(bf16[512,256]{1,0:T(8,128)(2,1)S(1)} %add.41.pair_ref), channel_id=1, source_target_pairs={{8,16},{16,8},{9,17},{17,9},{10,18},{18,10},{11,19},{19,11},{12,20... | collective-permute-start | bytes 786440 | tf_op jit(solution)/shard_map/ppermute | solution.py:477
  171.8 9.6 %collective-permute-start.14 = (bf16[512,256]{1,0:T(8,128)(2,1)S(1)}, bf16[512,256]{1,0:T(8,128)(2,1)S(1)}, u32[]{:S(2)}, u32[]{:S(2)}) collective-permute-start(bf16[512,256]{1,0:T(8,128)(2,1)S(1)} %add.35.pair_ref), channel_id=1, source_target_pairs={{8,16},{16,8},{9,17},{17,9},{10,18},{18,10},{11,19},{19,11},{12,20... | collective-permute-start | bytes 786440 | tf_op jit(solution)/shard_map/ppermute | solution.py:477
  172.6 16.0 %collective-permute-start.57 = (bf16[8,3072]{1,0:T(8,128)(2,1)S(1)}, bf16[8,3072]{1,0:T(8,128)(2,1)S(1)}, u32[]{:S(2)}, u32[]{:S(2)}) collective-permute-start(bf16[8,3072]{1,0:T(8,128)(2,1)S(1)} %add.55.final_ref), channel_id=1, source_target_pairs={{8,0},{16,24},{9,1},{17,25},{10,2},{18,26},{11,3},{19,27},{12,4},{... | collective-permute-start | bytes 147464 | tf_op jit(solution)/shard_map/ppermute | solution.py:459
  173.9 24.1 %collective-permute-start.54 = (bf16[512,256]{1,0:T(8,128)(2,1)S(1)}, bf16[512,256]{1,0:T(8,128)(2,1)S(1)}, u32[]{:S(2)}, u32[]{:S(2)}) collective-permute-start(bf16[512,256]{1,0:T(8,128)(2,1)S(1)} %around.47.refs_3_), channel_id=1, source_target_pairs={{0,8},{24,16},{8,0},{16,24},{1,9},{25,17},{9,1},{17,25},{2,10},{26... | collective-permute-start | bytes 786440 | tf_op jit(solution)/shard_map/ppermute | solution.py:473
  180.1 17.9 %collective-permute-start.41 = (bf16[512,256]{1,0:T(8,128)(2,1)S(1)}, bf16[512,256]{1,0:T(8,128)(2,1)S(1)}, u32[]{:S(2)}, u32[]{:S(2)}) collective-permute-start(bf16[512,256]{1,0:T(8,128)(2,1)S(1)} %around.41.refs_2_), channel_id=1, source_target_pairs={{8,0},{16,24},{9,1},{17,25},{10,2},{18,26},{11,3},{19,27},{12,4},{... | collective-permute-start | bytes 786440 | tf_op jit(solution)/shard_map/ppermute | solution.py:473
  181.5 17.6 %collective-permute-start.28 = (bf16[512,256]{1,0:T(8,128)(2,1)S(1)}, bf16[512,256]{1,0:T(8,128)(2,1)S(1)}, u32[]{:S(2)}, u32[]{:S(2)}) collective-permute-start(bf16[512,256]{1,0:T(8,128)(2,1)S(1)} %around.35.refs_3_), channel_id=1, source_target_pairs={{0,8},{24,16},{8,0},{16,24},{1,9},{25,17},{9,1},{17,25},{2,10},{26... | collective-permute-start | bytes 786440 | tf_op jit(solution)/shard_map/ppermute | solution.py:473
  188.5 12.7 %collective-permute-start.15 = (bf16[512,256]{1,0:T(8,128)(2,1)S(1)}, bf16[512,256]{1,0:T(8,128)(2,1)S(1)}, u32[]{:S(2)}, u32[]{:S(2)}) collective-permute-start(bf16[512,256]{1,0:T(8,128)(2,1)S(1)} %around.29.refs_2_), channel_id=1, source_target_pairs={{0,8},{24,16},{8,0},{16,24},{1,9},{25,17},{9,1},{17,25},{2,10},{26... | collective-permute-start | bytes 786440 | tf_op jit(solution)/shard_map/ppermute | solution.py:473
